TPU v7x, 128 devices: a whole 4x4x4 slice. The times are simulated.
128 devices in a mesh: sp: 16 (over z, y), tp: 8 (over x, core).
Axes of the slice: x: 4, y: 4, z: 4, core: 2. Of those that a mesh axis runs over, the one named last changes fastest.
Arguments:
- queries: bfloat16 [16384, 512], P('sp', 'tp'), may hold values from -6 to 6
- keys: bfloat16 [16384, 512], P('sp', 'tp'), may hold values from -6 to 6
- values: bfloat16 [16384, 1024], P('sp', 'tp'), may hold values from -6 to 6
- out_gate: bfloat16 [16384, 1024], P('sp', 'tp'), may hold values from -6 to 6
- decay_logit: float32 [2, 16384, 512], P(None, 'sp', 'tp'), may hold values from -8 to 16
- head_gain: float32 [1024], P('tp'), may hold values from 0.1 to 1.9
- out_weight: bfloat16 [1024, 2048], replicated, may hold values from -0.1875 to 0.1875
- stream: bfloat16 [16384, 2048], P(('sp', 'tp')), may hold values from -6 to 6
- mlp_gain: float32 [2048], replicated, may hold values from 0.1 to 1.9
- up_weight: bfloat16 [2048, 8192], P('sp', 'tp'), may hold values from -0.125 to 0.125
- down_weight: bfloat16 [8192, 2048], P('tp', 'sp'), may hold values from -0.0625 to 0.0625
Outputs:
- output: bfloat16 [16384, 2048], P(('sp', 'tp'))
All inputs are finite; a program needn't handle non-finite values.
Results may differ from a plain program's by a relative error of at most 0.018.
Values may be sent and summed in bfloat16 or wider, within the bound.
No kernel may reach another device: no remote copies, remote signals or barrier semaphores. Data moves between devices by JAX's collectives and lax.ppermute only.
A program may use at most 128 MiB of HBM per device.

v0:
```python
import functools

import jax
import jax.numpy as jnp
from jax import lax
from jax.experimental import pallas as pl
from jax.experimental.pallas import tpu as pltpu
from jax.sharding import Mesh
from jax.sharding import PartitionSpec as P


HEAD_K = 64
HEAD_V = 128
BLOCK = 128
D = 2048
ROWS = 128
SP = ("z", "y")
TP = ("x", "c")
PEERS = 16
FOLD = 80

gate_temper = 16.0
norm_eps = 1e-06
f32 = jnp.float32
bf16 = jnp.bfloat16
NEAR = (0, -1, 1, 2)

VMEM = pl.BlockSpec(memory_space=pltpu.VMEM)
SMEM = pl.BlockSpec(memory_space=pltpu.SMEM)
ANY = pl.BlockSpec(memory_space=pl.ANY)
HBM = pl.BlockSpec(memory_space=pltpu.HBM)


def dot(a, b, dims=((1,), (0,)), precision=None):
    return lax.dot_general(a, b, (dims, ((), ())), precision=precision, preferred_element_type=f32)


def attend_kernel(pos, q_ref, k_ref, v_ref, ld_ref, local_ref, carry_ref, send_ref, qd_s, tot_s, inc_s):
    length = q_ref.shape[1]
    count = length // BLOCK
    me = pos[0] * 4 + pos[1]
    row = lax.broadcasted_iota(jnp.int32, (BLOCK, BLOCK), 0)
    col = lax.broadcasted_iota(jnp.int32, (BLOCK, BLOCK), 1)
    ahead = col < HEAD_K
    lower = jnp.where(row >= col, 1.0, 0.0).astype(bf16)

    for b in range(count):
        rows = slice(b * BLOCK, (b + 1) * BLOCK)
        logit = jnp.concatenate([ld_ref[0, :, rows], ld_ref[1, :, rows]], axis=0).T
        decay = (jnp.minimum(logit, 0.0) - jnp.log1p(jnp.exp(-jnp.abs(logit)))) / gate_temper
        high = decay.astype(bf16)
        low = (decay - high.astype(f32)).astype(bf16)
        run = dot(lower, high) + dot(lower, low)
        total = run[BLOCK - 1 : BLOCK]
        within = jnp.where(ahead, run, total - run + decay)
        grow = jnp.exp(-within)
        q_blk, k_blk = q_ref[:, rows].astype(f32), k_ref[:, rows].astype(f32)
        q2 = jnp.concatenate([q_blk, q_blk], axis=0).T
        k2 = jnp.concatenate([k_blk, k_blk], axis=0).T
        q_dec = q2 * (jnp.exp(within) * HEAD_K ** (-0.5))
        k_inv = k2 * grow
        k_end = (k2 * jnp.exp(total - within)).astype(bf16)
        k_low = k_inv.astype(bf16)
        v_blk = v_ref[rows]
        fwd = dot(jnp.where(ahead, q_dec, 0.0).astype(bf16), k_low, ((1,), (1,)))
        bwd = dot(jnp.where(ahead, 0.0, q_dec).astype(bf16), k_low, ((1,), (1,)))
        scores = jnp.where(row >= col, fwd, 0.0) + jnp.where(row <= col, bwd, 0.0)
        local_ref[rows] = dot(scores.astype(bf16), v_blk)
        inc_s[b] = dot(v_blk, k_end, ((0,), (0,)))
        qd_s[rows] = q_dec
        tot_s[b : b + 1] = total

    totals = [tot_s[b : b + 1] for b in range(count)]
    ends = [jnp.exp(t) for t in totals]
    ahead1 = ahead[:1]
    forward = [jnp.zeros((HEAD_V, 2 * HEAD_K), f32)]
    before = [jnp.zeros_like(totals[0])]
    for b in range(count):
        forward.append(forward[b] * ends[b] + inc_s[b])
        before.append(before[b] + totals[b])
    backward = [jnp.zeros((HEAD_V, 2 * HEAD_K), f32)]
    after = [jnp.zeros_like(totals[0])]
    for b in reversed(range(count)):
        backward.append(backward[-1] * ends[b] + inc_s[b])
        after.append(after[-1] + totals[b])
    for b in range(count):
        rows = slice(b * BLOCK, (b + 1) * BLOCK)
        state = jnp.where(ahead, forward[b], backward[count - 1 - b]).astype(bf16)
        q_dec = qd_s[rows]
        local_ref[rows] = local_ref[rows] + dot(q_dec.astype(bf16), state, ((1,), (1,)))
        reach = jnp.exp(jnp.where(ahead1, before[b], after[count - 1 - b]))
        carry_ref[rows] = (q_dec * reach).astype(bf16)

    whole = jnp.exp(before[count])
    half = HEAD_V // 2

    def folded(state, lanes):
        wide = jnp.concatenate([state[:half, lanes], state[half:, lanes]], axis=1)
        decay = jnp.concatenate([whole[:, lanes], whole[:, lanes]], axis=1)
        return wide.astype(bf16), jnp.broadcast_to(decay, (FOLD - half, 2 * HEAD_K)).astype(bf16)

    to_later = folded(forward[count], slice(0, HEAD_K))
    to_earlier = folded(backward[count], slice(HEAD_K, 2 * HEAD_K))
    for peer in range(PEERS):
        later = peer > me
        send_ref[peer, :half] = jnp.where(later, to_later[0], to_earlier[0])
        send_ref[peer, half:] = jnp.where(later, to_later[1], to_earlier[1])


def gate_kernel(pos, got_ref, local_hbm, carry_hbm, gate_hbm, gain_ref, keep_ref, give_ref, both_s, local_ref, carry_ref, gate_ref, sems):
    loads = ((carry_hbm, carry_ref), (local_hbm, local_ref), (gate_hbm, gate_ref))
    loads = [pltpu.make_async_copy(src, dst, sems.at[n]) for n, (src, dst) in enumerate(loads)]
    for load in loads:
        load.start()
    me = pos[0] * 4 + pos[1]
    half = HEAD_V // 2
    fwd = jnp.zeros((half, 2 * HEAD_K), f32)
    bwd = jnp.zeros((half, 2 * HEAD_K), f32)
    for peer in range(PEERS):
        state = got_ref[peer, :half].astype(f32)
        decay = got_ref[peer, half : half + 16].astype(f32)[:1]
        fwd = jnp.where(peer < me, fwd * decay + state, fwd)
    for peer in reversed(range(PEERS)):
        state = got_ref[peer, :half].astype(f32)
        decay = got_ref[peer, half : half + 16].astype(f32)[:1]
        bwd = jnp.where(peer > me, bwd * decay + state, bwd)
    top = jnp.concatenate([fwd[:, :HEAD_K], bwd[:, :HEAD_K]], axis=1)
    low = jnp.concatenate([fwd[:, HEAD_K:], bwd[:, HEAD_K:]], axis=1)
    state = jnp.concatenate([top, low], axis=0).astype(bf16)
    for load in loads:
        load.wait()
    for group in range(8):
        rows = slice(group * ROWS, (group + 1) * ROWS)
        out = local_ref[rows] + dot(carry_ref[rows], state, ((1,), (1,)))
        scale = lax.rsqrt(jnp.mean(out * out, axis=-1, keepdims=True) + norm_eps)
        gate = gate_ref[rows].astype(f32)
        gate = gate / (1.0 + jnp.exp(-gate))
        both_s[lax.bitwise_xor(pos[3], group % 2), group // 2] = (out * scale * gain_ref[...] * gate).astype(bf16)
    keep_ref[...] = both_s[0]
    give_ref[...] = both_s[1]


def mix_kernel(pos, g0, g1, g2, g3, s0, s1, s2, s3, w_hbm, gain_ref, near_ref, far_ref, own_ref, xs, res, w_ref, sems):
    wide = 512
    loads = []
    for n in range(D // wide):
        cols = pl.ds(n * wide, wide)
        loads.append(pltpu.make_async_copy(w_hbm.at[:, cols], w_ref.at[:, cols], sems.at[n]))
    for load in loads:
        load.start()
    first = pos[3] == 0
    for d, g in enumerate((g0, g1, g2, g3)):
        for k in range(4):
            at = lax.rem(pos[2] + (NEAR[k] + 4), 4)
            a, b = g[0, at], g[1, at]
            xs[k * ROWS : (k + 1) * ROWS, d * 256 : d * 256 + 128] = jnp.where(first, a, b)
            xs[k * ROWS : (k + 1) * ROWS, d * 256 + 128 : (d + 1) * 256] = jnp.where(first, b, a)
    squares = jnp.zeros((4 * ROWS, 128), f32)
    for n in range(D // wide):
        cols = slice(n * wide, (n + 1) * wide)
        acc = None
        loads[n].wait()
        for d in range(4):
            at = pl.multiple_of(lax.rem(pos[2] + (NEAR[d] + 4), 4) * 256, 256)
            part = dot(xs[:, d * 256 : (d + 1) * 256], w_ref[pl.ds(at, 256), cols])
            acc = part if acc is None else acc + part
        for k, s in enumerate((s0, s1, s2, s3)):
            rows = slice(k * ROWS, (k + 1) * ROWS)
            res[rows, cols] = (s[:, cols].astype(f32) + acc[rows]).astype(bf16)
        line = res[:, cols].astype(f32)
        line = line * line
        for j in range(wide // 128):
            squares = squares + line[:, j * 128 : (j + 1) * 128]
    scale = lax.rsqrt(jnp.sum(squares, axis=-1, keepdims=True) / D + norm_eps)
    e = 2 * pos[3] - 1
    steps = (0, e, -e, 2)
    for j in range(4):
        for i in range(4):
            sp = lax.rem(pos[0] + steps[j] + 4, 4) * 4 + lax.rem(pos[1] + steps[i] + 4, 4)
            cols = pl.ds(pl.multiple_of(sp * 128, 128), 128)
            line = (res[:, cols].astype(f32) * scale * gain_ref[:, cols]).astype(bf16)
            if j < 3:
                near_ref[:, (4 * j + i) * 128 : (4 * j + i + 1) * 128] = line
            else:
                far_ref[:, i * 128 : (i + 1) * 128] = line
    own_ref[...] = res[:ROWS]


TURNED = (0, 2, 1, 3)


def up_copies(pairs, wu, sems, base):
    copies = []
    for j, pair in enumerate(pairs):
        for half in range(2):
            for i in range(4):
                dst = wu.at[pl.ds((4 * j + i) * 128, 128), pl.ds(half * 1024, 1024)]
                src = pair[half].at[TURNED[i] if half else i]
                copies.append(pltpu.make_async_copy(src, dst, sems.at[base + len(copies)]))
    return copies


def down_copies(pairs, wd, sems, base):
    copies = []
    for j, pair in enumerate(pairs):
        for half in range(2):
            for i in range(4):
                dst = wd.at[pl.ds(half * 1024, 1024), pl.ds(j * 512 + i * 128, 128)]
                src = pair[half].at[TURNED[i] if half else i]
                copies.append(pltpu.make_async_copy(src, dst, sems.at[base + len(copies)]))
    return copies


def up_kernel(x_ref, *refs):
    pairs, (acc_ref, wu, sems) = [refs[2 * j : 2 * j + 2] for j in range(3)], refs[6:]
    copies = up_copies(pairs, wu, sems, 0)
    for copy in copies:
        copy.start()
    for copy in copies:
        copy.wait()
    wide = 512
    for n in range(2048 // wide):
        cols = slice(n * wide, (n + 1) * wide)
        acc_ref[:, cols] = dot(x_ref[...], wu[:, cols])


def turn_kernel(x_ref, acc_ref, u0, u1, d0, d1, hid_ref, o0, o1, o2, o3, wu, wd, sems):
    ups = up_copies([(u0, u1)], wu, sems, 0)
    downs = down_copies([(d0, d1)], wd, sems, 8)
    for copy in ups + downs:
        copy.start()
    for copy in ups:
        copy.wait()
    wide = 512
    for n in range(2048 // wide):
        cols = slice(n * wide, (n + 1) * wide)
        h = jnp.maximum(acc_ref[:, cols] + dot(x_ref[...], wu[:, cols]), 0.0)
        hid_ref[:, cols] = (h * h).astype(bf16)
    for copy in downs:
        copy.wait()
    part = dot(hid_ref[...], wd[...]).astype(bf16)
    for k, o in enumerate((o0, o1, o2, o3)):
        o[...] = part[k * ROWS : (k + 1) * ROWS]


def down_kernel(hid_ref, *refs, count):
    pairs, outs = [refs[2 * j : 2 * j + 2] for j in range(count)], refs[2 * count : 2 * count + 4]
    wd, sems = refs[2 * count + 4 :]
    copies = down_copies(pairs, wd, sems, 0)
    for copy in copies:
        copy.start()
    for j in range(count):
        for copy in copies[8 * j : 8 * j + 8]:
            copy.wait()
        cols = slice(j * 512, (j + 1) * 512)
        part = dot(hid_ref[...], wd[:, cols]).astype(bf16)
        for k, o in enumerate(outs):
            o[:, cols] = part[k * ROWS : (k + 1) * ROWS]


def end_kernel(pos, res_ref, *refs):
    parts, out_ref = [refs[4 * n : 4 * n + 4] for n in range(3)], refs[12]
    e = 2 * pos[3] - 1
    steps = (0, e, -e, 2)
    for j in range(4):
        for i in range(4):
            sp = lax.rem(pos[0] + steps[i] + 4, 4) * 4 + lax.rem(pos[1] + steps[j] + 4, 4)
            at = pl.ds(pl.multiple_of(sp * 128, 128), 128)
            src, off = ((parts[0], 0), (parts[1], 0), (parts[1], 512), (parts[2], 0))[j]
            cols = slice(off + i * 128, off + (i + 1) * 128)
            total = src[0][:, cols].astype(f32) + src[1][:, cols].astype(f32)
            total = total + src[2][:, cols].astype(f32) + src[3][:, cols].astype(f32)
            out_ref[:, at] = (res_ref[:, at].astype(f32) + total).astype(bf16)


def join_kernel(*refs):
    out_ref, sems = refs[4:]
    copies = [pltpu.make_async_copy(refs[i], out_ref.at[i], sems.at[i]) for i in range(4)]
    for copy in copies:
        copy.start()
    for copy in copies:
        copy.wait()


def mark_kernel(pos, out_ref):
    for i in range(4):
        out_ref[i] = pos[i]


def call(kernel, ins, outs, scratch, args, flops, nbytes, limit, spec=VMEM):
    return launched(kernel, ins, outs, scratch, args, flops, nbytes, limit, spec)


def launched(kernel, ins, outs, scratch, args, flops, nbytes, limit, spec):
    return pl.pallas_call(
        kernel,
        in_specs=ins,
        out_specs=[spec] * len(outs),
        out_shape=[jax.ShapeDtypeStruct(s, t) for s, t in outs],
        scratch_shapes=scratch,
        cost_estimate=pl.CostEstimate(flops=flops, bytes_accessed=nbytes, transcendentals=0),
        compiler_params=pltpu.CompilerParams(vmem_limit_bytes=limit * 1024 * 1024),
    )(*args)


def shifted(v, axis, by, n=4):
    return lax.ppermute(v, axis, [(i, (i + by) % n) for i in range(n)])


def swapped(v):
    return lax.ppermute(v, "c", [(0, 1), (1, 0)])


def both_ways(v, axis, sign):
    pairs = [(2 * i + c, 2 * ((i + sign * (1 - 2 * c)) % 4) + c) for i in range(4) for c in range(2)]
    return lax.ppermute(v, (axis, "c"), pairs)


def joined(blocks):
    shape = (4, *blocks[0].shape)
    scratch = [pltpu.SemaphoreType.DMA((4,))]
    return call(join_kernel, [VMEM] * 4, [(shape, bf16)], scratch, blocks, 800_000_000, 2_000_000, 4, HBM)[0]


def local(
    queries,
    keys,
    values,
    out_gate,
    decay_logit,
    head_gain,
    out_weight,
    stream,
    mlp_gain,
    up_weight,
    down_weight,
):
    length = queries.shape[0]
    pos = jnp.stack([lax.axis_index(a) for a in ("z", "y", "x", "c")]).astype(jnp.int32)

    up_a, up_b = both_ways(up_weight, "y", 1), both_ways(up_weight, "y", -1)
    down_a, down_b = both_ways(down_weight, "z", 1), both_ways(down_weight, "z", -1)

    rows_out, carry, sent = call(
        attend_kernel,
        [SMEM] + [VMEM] * 4,
        [((length, HEAD_V), f32), ((length, 2 * HEAD_K), bf16), ((PEERS, FOLD, 128), bf16)],
        [
            pltpu.VMEM((length, 2 * HEAD_K), f32),
            pltpu.VMEM((length // BLOCK, 2 * HEAD_K), f32),
            pltpu.VMEM((length // BLOCK, HEAD_V, 2 * HEAD_K), f32),
        ],
        (pos, queries.T, keys.T, values, decay_logit.transpose(0, 2, 1)),
        2_000_000_000,
        2_000_000,
        60,
    )
    up_2 = both_ways(up_a, "y", 1)
    down_2 = both_ways(down_a, "z", 1)
    streams = [stream] + [shifted(stream, "x", NEAR[k]) for k in (3, 2, 1)]
    streams = [streams[0], streams[2], streams[3], streams[1]]
    got = lax.all_to_all(sent, SP, 0, 0, tiled=True)
    up_line = joined((up_weight, up_a, up_b, up_2))
    down_line = joined((down_weight, down_a, down_b, down_2))
    up_na, up_nb = both_ways(up_line, "z", 1), both_ways(up_line, "z", -1)
    down_na, down_nb = both_ways(down_line, "y", 1), both_ways(down_line, "y", -1)
    up_n2 = both_ways(up_na, "z", 1)
    down_n2 = both_ways(down_na, "y", 1)
    ups = [up_line, up_na, up_nb, up_n2]
    ups_s = [swapped(v) for v in ups]
    downs = [down_line, down_na, down_nb, down_n2]
    downs_s = [swapped(v) for v in downs]
    keep, give = call(
        gate_kernel,
        [SMEM, VMEM, HBM, HBM, HBM, VMEM],
        [((4, ROWS, HEAD_V), bf16)] * 2,
        [
            pltpu.VMEM((2, 4, ROWS, HEAD_V), bf16),
            pltpu.VMEM((length, HEAD_V), f32),
            pltpu.VMEM((length, 2 * HEAD_K), bf16),
            pltpu.VMEM((length, HEAD_V), bf16),
            pltpu.SemaphoreType.DMA((3,)),
        ],
        (pos, got, rows_out, carry, out_gate, head_gain.reshape(1, HEAD_V)),
        1_000_000_000,
        2_000_000,
        8,
    )
    pair = jnp.stack([keep, swapped(give)])
    heads = {k: shifted(pair, "x", NEAR[k]) for k in (1, 2, 3)}
    heads = [pair, heads[2], heads[1], heads[3]]
    pos2 = pl.pallas_call(
        mark_kernel, in_specs=[SMEM], out_specs=SMEM, out_shape=jax.ShapeDtypeStruct((4,), jnp.int32)
    )(pos)
    near, far, residual = call(
        mix_kernel,
        [SMEM] + [VMEM] * 8 + [HBM, VMEM],
        [((4 * ROWS, 1536), bf16), ((4 * ROWS, 512), bf16), ((ROWS, D), bf16)],
        [
            pltpu.VMEM((4 * ROWS, 1024), bf16),
            pltpu.VMEM((4 * ROWS, D), bf16),
            pltpu.VMEM((1024, D), bf16),
            pltpu.SemaphoreType.DMA((4,)),
        ],
        (pos2, *heads, *streams, out_weight, mlp_gain.reshape(1, D)),
        2 * 512 * 1024 * 2048,
        12_000_000,
        24,
    )
    gathered = call(
        up_kernel,
        [VMEM] + [ANY] * 6,
        [((4 * ROWS, 2048), f32)],
        [pltpu.VMEM((1536, 2048), bf16), pltpu.SemaphoreType.DMA((24,))],
        (near, *[w for j in range(3) for w in (ups[j], ups_s[TURNED[j]])]),
        2 * 512 * 1536 * 2048,
        10_000_000,
        20,
    )[0]
    turned = call(
        turn_kernel,
        [VMEM] * 2 + [ANY] * 4,
        [((4 * ROWS, 2048), bf16)] + [((ROWS, 512), bf16)] * 4,
        [pltpu.VMEM((512, 2048), bf16), pltpu.VMEM((2048, 512), bf16), pltpu.SemaphoreType.DMA((16,))],
        (far, gathered, ups[3], ups_s[3], downs[0], downs_s[0]),
        4 * 512 * 512 * 2048,
        8_000_000,
        24,
    )
    hidden, first = turned[0], turned[1:]

    def down(js):
        count = len(js)
        return call(
            functools.partial(down_kernel, count=count),
            [VMEM] + [ANY] * (2 * count),
            [((ROWS, count * 512), bf16)] * 4,
            [pltpu.VMEM((2048, count * 512), bf16), pltpu.SemaphoreType.DMA((8 * count,))],
            (hidden, *[w for j in js for w in (downs[j], downs_s[TURNED[j]])]),
            count * 512 * 2048 * 1024,
            count * 3_000_000,
            20,
        )

    def sent_back(parts):
        return [parts[0]] + [shifted(parts[k], "x", NEAR[k]) for k in (1, 2, 3)]

    first = sent_back(first)
    second = sent_back(down((1, 2)))
    third = sent_back(down((3,)))
    return call(
        end_kernel,
        [SMEM] + [VMEM] * 13,
        [((ROWS, D), bf16)],
        [],
        (pos, residual, *first, *second, *third),
        100_000_000,
        3_000_000,
        8,
    )[0]


def solution(mesh):
    split = Mesh(mesh.devices.reshape(4, 4, 4, 2), ("z", "y", "x", "c"))
    both = SP + TP
    in_specs = (
        P(SP, TP),
        P(SP, TP),
        P(SP, TP),
        P(SP, TP),
        P(None, SP, TP),
        P(TP),
        P(),
        P(both, None),
        P(),
        P(SP, TP),
        P(TP, SP),
    )
    return jax.shard_map(local, mesh=split, in_specs=in_specs, out_specs=P(both, None), check_vma=False)
```

profile of v0, /device:TPU:1, one launch (start us, length us, event | category | flops | bytes accessed | tf_op | source)
XLA Modules:
  0.0 162.2 jit_solution(8714488809735935803)
XLA Ops:
  0.0 3.6 %collective-permute-start.7 = (bf16[128,1024]{1,0:T(8,128)(2,1)}, bf16[128,1024]{1,0:T(8,128)(2,1)S(1)}, u32[]{:S(2)}, u32[]{:S(2)}) collective-permute-start(bf16[128,1024]{1,0:T(8,128)(2,1)} %refs_0_.2), channel_id=1, source_target_pairs={{0,8},{1,25},{8,16},{9,1},{16,24},{17,9},{24,0},{25,17},{2,10},{3,... | collective-permute-start | bytes 786440 | tf_op jit(solution)/shard_map/ppermute | solution.py:316
  4.3 4.9 %shard_map.110 = (f32[1024,128]{1,0:T(8,128)}, bf16[1024,128]{1,0:T(8,128)(2,1)}, bf16[16,80,128]{2,1,0:T(8,128)(2,1)}) custom-call(s32[4]{0:T(128)} %pad_add_fusion.pos, bf16[64,1024]{1,0:T(8,128)(2,1)} %bitcast.16, bf16[64,1024]{1,0:T(8,128)(2,1)} %bitcast.17, bf16[1024,128]{1,0:T(8,128)(2,1)} %v_ref.1, f32[2,64,1024]{2,1,0:T(8,128)} %bitcast.15), custom_call_target="tpu_custom_call" | custom-call | flops 2000000000 | bytes 2000000 | tf_op jit(solution)/shard_map/pallas_call | solution.py:295
  9.2 7.5 %all-to-all-start = ((bf16[16,80,128]{2,1,0:T(8,128)(2,1)}), bf16[16,80,128]{2,1,0:T(8,128)(2,1)S(1)}, u32[]{:S(2)}, u32[]{:S(2)}) async-start(bf16[16,80,128]{2,1,0:T(8,128)(2,1)} %get-tuple-element.26), calls=%async_computation | async-start | bytes 655360 | tf_op jit(solution)/shard_map/all_to_all | solution.py:362
  16.8 2.6 %collective-permute-start.17 = (bf16[1024,128]{1,0:T(8,128)(2,1)S(1)}, bf16[1024,128]{1,0:T(8,128)(2,1)}, u32[]{:S(2)}, u32[]{:S(2)}) collective-permute-start(bf16[1024,128]{1,0:T(8,128)(2,1)S(1)} %copy-done.15), channel_id=1, source_target_pairs={{0,32},{1,97},{32,64},{33,1},{64,96},{65,33},{96,0},{97,65},{2,34}... | collective-permute-start | bytes 786440 | tf_op jit(solution)/shard_map/ppermute | solution.py:316
  19.4 1.2 collective-permute-start.4
  20.6 1.5 collective-permute-start.5
  22.1 2.4 %collective-permute-start.9 = (bf16[128,1024]{1,0:T(8,128)(2,1)S(1)}, bf16[128,1024]{1,0:T(8,128)(2,1)S(1)}, u32[]{:S(2)}, u32[]{:S(2)}) collective-permute-start(bf16[128,1024]{1,0:T(8,128)(2,1)S(1)} %collective-permute-done.7.refs_1_), channel_id=1, source_target_pairs={{0,8},{1,25},{8,16},{9,1},{16,24},{17,9},{24,0},{25,17},{2,10},{3,... | collective-permute-start | bytes 786440 | tf_op jit(solution)/shard_map/ppermute | solution.py:316
  24.5 1.3 all-to-all-done.got_ref
  25.8 1.0 copy-done.28
  26.8 0.9 copy-done.29
  27.8 1.4 shard_map.111
  29.2 1.4 collective-permute-start
  30.6 2.7 %collective-permute-start.6 = (bf16[128,2048]{1,0:T(8,128)(2,1)}, bf16[128,2048]{1,0:T(8,128)(2,1)S(1)}, u32[]{:S(2)}, u32[]{:S(2)}) collective-permute-start(bf16[128,2048]{1,0:T(8,128)(2,1)} %s0.1), channel_id=1, source_target_pairs={{0,4},{2,6},{4,0},{6,2},{1,5},{3,7},{5,1},{7,3},{8,12},{10,14},{12... | collective-permute-start | bytes 1572872 | tf_op jit(solution)/shard_map/ppermute | solution.py:307
  36.0 1.4 collective-permute-start.12
  37.4 1.6 %collective-permute-done.19.refs_3_ = bf16[1024,128]{1,0:T(8,128)(2,1)S(1)} collective-permute-done((bf16[1024,128]{1,0:T(8,128)(2,1)}, bf16[1024,128]{1,0:T(8,128)(2,1)S(1)}, u32[]{:S(2)}, u32[]{:S(2)}) %collective-permute-start.19) | collective-permute-done | bytes 262176 | tf_op jit(solution)/shard_map/ppermute | solution.py:316
  41.3 2.0 %shard_map.115.d0 = bf16[4,1024,128]{2,1,0:T(8,128)(2,1)} custom-call(bf16[1024,128]{1,0:T(8,128)(2,1)S(1)} %copy-done.16, bf16[1024,128]{1,0:T(8,128)(2,1)} %collective-permute-done.17.refs_1_, bf16[1024,128]{1,0:T(8,128)(2,1)S(1)} %copy-done.20, bf16[1024,128]{1,0:T(8,128)(2,1)S(1)} %collective-permute-done.19.refs_3_), custom_call_target="tpu_custom_call" | custom-call | flops 800000000 | bytes 2000000 | tf_op jit(solution)/shard_map/pallas_call | solution.py:295
  43.2 3.0 %collective-permute-done.6.s3 = bf16[128,2048]{1,0:T(8,128)(2,1)S(1)} collective-permute-done((bf16[128,2048]{1,0:T(8,128)(2,1)}, bf16[128,2048]{1,0:T(8,128)(2,1)S(1)}, u32[]{:S(2)}, u32[]{:S(2)}) %collective-permute-start.6) | collective-permute-done | bytes 524320 | tf_op jit(solution)/shard_map/ppermute | solution.py:307
  47.1 2.5 %collective-permute-start.24 = (bf16[4,1024,128]{2,1,0:T(8,128)(2,1)}, bf16[4,1024,128]{2,1,0:T(8,128)(2,1)}, u32[]{:S(2)}, u32[]{:S(2)}) collective-permute-start(bf16[4,1024,128]{2,1,0:T(8,128)(2,1)} %shard_map.115.d0), channel_id=1, source_target_pairs={{0,8},{1,25},{8,16},{9,1},{16,24},{17,9},{24,0},{25,17},{2,10},{3,... | collective-permute-start | bytes 3145736 | tf_op jit(solution)/shard_map/ppermute | solution.py:316
  50.5 1.7 %collective-permute-start.2 = (bf16[2,4,128,128]{3,2,1,0:T(8,128)(2,1)S(1)}, bf16[2,4,128,128]{3,2,1,0:T(8,128)(2,1)S(1)}, u32[]{:S(2)}, u32[]{:S(2)}) collective-permute-start(bf16[2,4,128,128]{3,2,1,0:T(8,128)(2,1)S(1)} %pad_maximum_fusion.g0), channel_id=1, source_target_pairs={{0,6},{2,0},{4,2},{6,4},{1,7},{3,1},{5,3},{7,5},{8,14},{10,8},{12,... | collective-permute-start | bytes 786440 | tf_op jit(solution)/shard_map/ppermute | solution.py:307
  52.2 4.5 %collective-permute-done.2.g2 = bf16[2,4,128,128]{3,2,1,0:T(8,128)(2,1)S(1)} collective-permute-done((bf16[2,4,128,128]{3,2,1,0:T(8,128)(2,1)S(1)}, bf16[2,4,128,128]{3,2,1,0:T(8,128)(2,1)S(1)}, u32[]{:S(2)}, u32[]{:S(2)}) %collective-permute-start.2) | collective-permute-done | bytes 262176 | tf_op jit(solution)/shard_map/ppermute | solution.py:307
  57.4 4.0 %collective-permute-start.3 = (bf16[2,4,128,128]{3,2,1,0:T(8,128)(2,1)S(1)}, bf16[2,4,128,128]{3,2,1,0:T(8,128)(2,1)S(1)}, u32[]{:S(2)}, u32[]{:S(2)}) collective-permute-start(bf16[2,4,128,128]{3,2,1,0:T(8,128)(2,1)S(1)} %pad_maximum_fusion.g0), channel_id=1, source_target_pairs={{0,4},{2,6},{4,0},{6,2},{1,5},{3,7},{5,1},{7,3},{8,12},{10,14},{12... | collective-permute-start | bytes 786440 | tf_op jit(solution)/shard_map/ppermute | solution.py:307
  61.4 3.8 %collective-permute-done.3.g3 = bf16[2,4,128,128]{3,2,1,0:T(8,128)(2,1)S(1)} collective-permute-done((bf16[2,4,128,128]{3,2,1,0:T(8,128)(2,1)S(1)}, bf16[2,4,128,128]{3,2,1,0:T(8,128)(2,1)S(1)}, u32[]{:S(2)}, u32[]{:S(2)}) %collective-permute-start.3) | collective-permute-done | bytes 262176 | tf_op jit(solution)/shard_map/ppermute | solution.py:307
  65.9 1.2 collective-permute-start.25
  67.1 1.3 collective-permute-start.15
  68.4 9.9 %collective-permute-start.13 = (bf16[4,128,1024]{2,1,0:T(8,128)(2,1)S(1)}, bf16[4,128,1024]{2,1,0:T(8,128)(2,1)S(1)}, u32[]{:S(2)}, u32[]{:S(2)}) collective-permute-start(bf16[4,128,1024]{2,1,0:T(8,128)(2,1)S(1)} %collective-permute-done.12.refs_4_), channel_id=1, source_target_pairs={{0,1},{1,0},{2,3},{3,2},{4,5},{5,4},{6,7},{7,6},{8,9},{9,8},{10,11... | collective-permute-start | bytes 3145736 | tf_op jit(solution)/shard_map/ppermute | solution.py:311
  78.4 1.0 copy-done
  80.0 1.0 collective-permute-done.25.refs_2_
  81.1 19.5 %collective-permute-start.20 = (bf16[4,1024,128]{2,1,0:T(8,128)(2,1)}, bf16[4,1024,128]{2,1,0:T(8,128)(2,1)}, u32[]{:S(2)}, u32[]{:S(2)}) collective-permute-start(bf16[4,1024,128]{2,1,0:T(8,128)(2,1)} %shard_map.115.d0), channel_id=1, source_target_pairs={{0,1},{1,0},{2,3},{3,2},{4,5},{5,4},{6,7},{7,6},{8,9},{9,8},{10,11... | collective-permute-start | bytes 3145736 | tf_op jit(solution)/shard_map/ppermute | solution.py:311
  100.6 1.0 copy-done.2
  102.1 1.0 copy-done.4
  103.6 1.2 shard_map.109.pos
  104.9 2.3 %copy-done.8 = bf16[1024,2048]{1,0:T(8,128)(2,1)S(1)} copy-done((bf16[1024,2048]{1,0:T(8,128)(2,1)S(1)}, bf16[1024,2048]{1,0:T(8,128)(2,1)}, u32[]{:S(2)}) %copy-start.8) | copy-done | bytes 4194328
  107.2 1.0 copy-done.10
  108.3 1.0 copy-done.12
  112.8 6.0 %shard_map.112 = (bf16[512,1536]{1,0:T(8,128)(2,1)S(1)}, bf16[512,512]{1,0:T(8,128)(2,1)S(1)}, bf16[128,2048]{1,0:T(8,128)(2,1)S(1)}) custom-call(s32[4]{0:T(128)S(1)} %copy-done.27, bf16[2,4,128,128]{3,2,1,0:T(8,128)(2,1)S(1)} %pad_maximum_fusion.g0, bf16[2,4,128,128]{3,2,1,0:T(8,128)(2,1)S(1)} %copy-done.18, bf16[2,4,128,128]{3,2,1,0:T(8,128)(2,1)S(1)} %copy-done.22, ...), custom_call_target="tpu_custom_call" | custom-call | flops 2147483648 | bytes 12000000 | tf_op jit(solution)/shard_map/pallas_call | solution.py:295
  118.9 4.2 %shard_map.114.acc_ref = f32[512,2048]{1,0:T(8,128)S(1)} custom-call(bf16[512,1536]{1,0:T(8,128)(2,1)S(1)} %get-tuple-element.33.x_ref, bf16[4,128,1024]{2,1,0:T(8,128)(2,1)S(1)} %shard_map.113.refs_0_, bf16[4,128,1024]{2,1,0:T(8,128)(2,1)S(1)} %collective-permute-done.10.refs_1_, bf16[4,128,1024]{2,1,0:T(8,128)(2,1)S(1)} %collective-permute-done.11.refs_2_, ...), custom_call_target="tpu_custom_call" | custom-call | flops 3221225472 | bytes 10000000 | tf_op jit(solution)/shard_map/pallas_call | solution.py:295
  123.1 4.2 %shard_map.116 = (bf16[512,2048]{1,0:T(8,128)(2,1)S(1)}, bf16[128,512]{1,0:T(8,128)(2,1)S(1)}, bf16[128,512]{1,0:T(8,128)(2,1)S(1)}, bf16[128,512]{1,0:T(8,128)(2,1)S(1)}, bf16[128,512]{1,0:T(8,128)(2,1)S(1)}) custom-call(bf16[512,512]{1,0:T(8,128)(2,1)S(1)} %get-tuple-element.32.x_ref, f32[512,2048]{1,0:T(8,128)S(1)} %shard_map.114.acc_ref, ...), custom_call_target="tpu_custom_call" | custom-call | flops 2147483648 | bytes 8000000 | tf_op jit(solution)/shard_map/pallas_call | solution.py:295
  127.2 3.5 %collective-permute-start.21 = (bf16[128,512]{1,0:T(8,128)(2,1)S(1)}, bf16[128,512]{1,0:T(8,128)(2,1)S(1)}, u32[]{:S(2)}, u32[]{:S(2)}) collective-permute-start(bf16[128,512]{1,0:T(8,128)(2,1)S(1)} %get-tuple-element.35), channel_id=1, source_target_pairs={{0,6},{2,0},{4,2},{6,4},{1,7},{3,1},{5,3},{7,5},{8,14},{10,8},{12,... | collective-permute-start | bytes 393224 | tf_op jit(solution)/shard_map/ppermute | solution.py:307
  130.7 1.3 collective-permute-start.23
  132.0 4.2 %shard_map.117 = (bf16[128,1024]{1,0:T(8,128)(2,1)S(1)}, bf16[128,1024]{1,0:T(8,128)(2,1)S(1)}, bf16[128,1024]{1,0:T(8,128)(2,1)S(1)}, bf16[128,1024]{1,0:T(8,128)(2,1)S(1)}) custom-call(bf16[512,2048]{1,0:T(8,128)(2,1)S(1)} %get-tuple-element.38.hid_ref, bf16[4,1024,128]{2,1,0:T(8,128)(2,1)} %collective-permute-done.24.refs_0_, ...), custom_call_target="tpu_custom_call" | custom-call | flops 2147483648 | bytes 6000000 | tf_op jit(solution)/shard_map/pallas_call | solution.py:295
  136.1 1.5 collective-permute-start.28
  137.6 2.8 %shard_map.118 = (bf16[128,512]{1,0:T(8,128)(2,1)S(1)}, bf16[128,512]{1,0:T(8,128)(2,1)S(1)}, bf16[128,512]{1,0:T(8,128)(2,1)S(1)}, bf16[128,512]{1,0:T(8,128)(2,1)S(1)}) custom-call(bf16[512,2048]{1,0:T(8,128)(2,1)S(1)} %get-tuple-element.38.hid_ref, bf16[4,1024,128]{2,1,0:T(8,128)(2,1)} %collective-permute-done.31.refs_0_, ...), custom_call_target="tpu_custom_call" | custom-call | flops 1073741824 | bytes 3000000 | tf_op jit(solution)/shard_map/pallas_call | solution.py:295
  142.0 2.3 %collective-permute-start.30 = (bf16[128,1024]{1,0:T(8,128)(2,1)S(1)}, bf16[128,1024]{1,0:T(8,128)(2,1)S(1)}, u32[]{:S(2)}, u32[]{:S(2)}) collective-permute-start(bf16[128,1024]{1,0:T(8,128)(2,1)S(1)} %get-tuple-element.42), channel_id=1, source_target_pairs={{0,4},{2,6},{4,0},{6,2},{1,5},{3,7},{5,1},{7,3},{8,12},{10,14},{12... | collective-permute-start | bytes 786440 | tf_op jit(solution)/shard_map/ppermute | solution.py:307
  144.3 2.5 %collective-permute-done.33.refs_9_ = bf16[128,512]{1,0:T(8,128)(2,1)S(1)} collective-permute-done((bf16[128,512]{1,0:T(8,128)(2,1)S(1)}, bf16[128,512]{1,0:T(8,128)(2,1)S(1)}, u32[]{:S(2)}, u32[]{:S(2)}) %collective-permute-start.33) | collective-permute-done | bytes 131104 | tf_op jit(solution)/shard_map/ppermute | solution.py:307
  146.8 1.3 collective-permute-start.35
  148.1 8.1 %collective-permute-done.34.refs_10_ = bf16[128,512]{1,0:T(8,128)(2,1)S(1)} collective-permute-done((bf16[128,512]{1,0:T(8,128)(2,1)S(1)}, bf16[128,512]{1,0:T(8,128)(2,1)S(1)}, u32[]{:S(2)}, u32[]{:S(2)}) %collective-permute-start.34) | collective-permute-done | bytes 131104 | tf_op jit(solution)/shard_map/ppermute | solution.py:307
  156.2 4.1 %collective-permute-done.35.refs_11_ = bf16[128,512]{1,0:T(8,128)(2,1)S(1)} collective-permute-done((bf16[128,512]{1,0:T(8,128)(2,1)S(1)}, bf16[128,512]{1,0:T(8,128)(2,1)S(1)}, u32[]{:S(2)}, u32[]{:S(2)}) %collective-permute-start.35) | collective-permute-done | bytes 131104 | tf_op jit(solution)/shard_map/ppermute | solution.py:307
  160.3 1.8 %shard_map.119 = bf16[128,2048]{1,0:T(8,128)(2,1)} custom-call(s32[4]{0:T(128)S(1)} %copy-done.7, bf16[128,2048]{1,0:T(8,128)(2,1)S(1)} %get-tuple-element.31.res_ref, bf16[128,512]{1,0:T(8,128)(2,1)S(1)} %get-tuple-element.34.refs_0_, bf16[128,512]{1,0:T(8,128)(2,1)S(1)} %collective-permute-done.21.refs_1_, ...), custom_call_target="tpu_custom_call" | custom-call | flops 100000000 | bytes 3000000 | tf_op jit(solution)/shard_map/pallas_call | solution.py:295
  (99 shorter events, 15.4 us)
Async XLA Ops:
  0.0 16.8 %copy-start.15 = (bf16[1024,128]{1,0:T(8,128)(2,1)S(1)}, bf16[1024,128]{1,0:T(8,128)(2,1)}, u32[]{:S(2)}) copy-start(bf16[1024,128]{1,0:T(8,128)(2,1)} %refs_0_.3) | copy-start | bytes 786436
  0.0 25.8 %copy-start.13 = (bf16[1024,128]{1,0:T(8,128)(2,1)S(1)}, bf16[1024,128]{1,0:T(8,128)(2,1)}, u32[]{:S(2)}) copy-start(bf16[1024,128]{1,0:T(8,128)(2,1)} %gate_hbm.1) | copy-start | bytes 786436
  0.0 25.8 %copy-start.26 = (f32[128]{0:T(128)S(1)}, f32[128]{0:T(128)}, u32[]{:S(2)}) copy-start(f32[128]{0:T(128)} %param.16) | copy-start | bytes 1540
  0.0 20.6 %collective-permute-start.7 = (bf16[128,1024]{1,0:T(8,128)(2,1)}, bf16[128,1024]{1,0:T(8,128)(2,1)S(1)}, u32[]{:S(2)}, u32[]{:S(2)}) collective-permute-start(bf16[128,1024]{1,0:T(8,128)(2,1)} %refs_0_.2), channel_id=1, source_target_pairs={{0,8},{1,25},{8,16},{9,1},{16,24},{17,9},{24,0},{25,17},{2,10},{3,... | collective-permute-start | bytes 786440 | tf_op jit(solution)/shard_map/ppermute | solution.py:316
  3.6 18.5 %collective-permute-start.8 = (bf16[128,1024]{1,0:T(8,128)(2,1)}, bf16[128,1024]{1,0:T(8,128)(2,1)S(1)}, u32[]{:S(2)}, u32[]{:S(2)}) collective-permute-start(bf16[128,1024]{1,0:T(8,128)(2,1)} %refs_0_.2), channel_id=1, source_target_pairs={{0,24},{1,9},{8,0},{9,17},{16,8},{17,25},{24,16},{25,1},{2,26},{3,... | collective-permute-start | bytes 786440 | tf_op jit(solution)/shard_map/ppermute | solution.py:316
  4.3 21.5 %copy-start.6 = (s32[4]{0:T(128)S(1)}, s32[4]{0:T(128)}, u32[]{:S(2)}) copy-start(s32[4]{0:T(128)} %pad_add_fusion.pos) | copy-start | bytes 52
  4.3 29.9 %copy-start.14 = (bf16[128,1024]{1,0:T(8,128)(2,1)S(1)}, bf16[128,1024]{1,0:T(8,128)(2,1)}, u32[]{:S(2)}) copy-start(bf16[128,1024]{1,0:T(8,128)(2,1)} %refs_0_.2) | copy-start | bytes 786436
  9.2 16.5 %all-to-all-start = ((bf16[16,80,128]{2,1,0:T(8,128)(2,1)}), bf16[16,80,128]{2,1,0:T(8,128)(2,1)S(1)}, u32[]{:S(2)}, u32[]{:S(2)}) async-start(bf16[16,80,128]{2,1,0:T(8,128)(2,1)} %get-tuple-element.26), calls=%async_computation | async-start | bytes 655360 | tf_op jit(solution)/shard_map/all_to_all | solution.py:362
  16.8 12.4 %collective-permute-start.17 = (bf16[1024,128]{1,0:T(8,128)(2,1)S(1)}, bf16[1024,128]{1,0:T(8,128)(2,1)}, u32[]{:S(2)}, u32[]{:S(2)}) collective-permute-start(bf16[1024,128]{1,0:T(8,128)(2,1)S(1)} %copy-done.15), channel_id=1, source_target_pairs={{0,32},{1,97},{32,64},{33,1},{64,96},{65,33},{96,0},{97,65},{2,34}... | collective-permute-start | bytes 786440 | tf_op jit(solution)/shard_map/ppermute | solution.py:316
  19.4 11.2 %collective-permute-start.18 = (bf16[1024,128]{1,0:T(8,128)(2,1)S(1)}, bf16[1024,128]{1,0:T(8,128)(2,1)S(1)}, u32[]{:S(2)}, u32[]{:S(2)}) collective-permute-start(bf16[1024,128]{1,0:T(8,128)(2,1)S(1)} %copy-done.15), channel_id=1, source_target_pairs={{0,96},{1,33},{32,0},{33,65},{64,32},{65,97},{96,64},{97,1},{2,98}... | collective-permute-start | bytes 786440 | tf_op jit(solution)/shard_map/ppermute | solution.py:316
  19.4 15.3 %collective-permute-start.4 = (bf16[128,2048]{1,0:T(8,128)(2,1)}, bf16[128,2048]{1,0:T(8,128)(2,1)S(1)}, u32[]{:S(2)}, u32[]{:S(2)}) collective-permute-start(bf16[128,2048]{1,0:T(8,128)(2,1)} %s0.1), channel_id=1, source_target_pairs={{0,2},{2,4},{4,6},{6,0},{1,3},{3,5},{5,7},{7,1},{8,10},{10,12},{12... | collective-permute-start | bytes 1572872 | tf_op jit(solution)/shard_map/ppermute | solution.py:307
  20.6 15.3 %collective-permute-start.5 = (bf16[128,2048]{1,0:T(8,128)(2,1)}, bf16[128,2048]{1,0:T(8,128)(2,1)}, u32[]{:S(2)}, u32[]{:S(2)}) collective-permute-start(bf16[128,2048]{1,0:T(8,128)(2,1)} %s0.1), channel_id=1, source_target_pairs={{0,6},{2,0},{4,2},{6,4},{1,7},{3,1},{5,3},{7,5},{8,14},{10,8},{12,... | collective-permute-start | bytes 1572872 | tf_op jit(solution)/shard_map/ppermute | solution.py:307
  22.1 11.2 %collective-permute-start.9 = (bf16[128,1024]{1,0:T(8,128)(2,1)S(1)}, bf16[128,1024]{1,0:T(8,128)(2,1)S(1)}, u32[]{:S(2)}, u32[]{:S(2)}) collective-permute-start(bf16[128,1024]{1,0:T(8,128)(2,1)S(1)} %collective-permute-done.7.refs_1_), channel_id=1, source_target_pairs={{0,8},{1,25},{8,16},{9,1},{16,24},{17,9},{24,0},{25,17},{2,10},{3,... | collective-permute-start | bytes 786440 | tf_op jit(solution)/shard_map/ppermute | solution.py:316
  27.8 77.1 %copy-start.25 = (f32[2048]{0:T(1024)S(1)}, f32[2048]{0:T(1024)}, u32[]{:S(2)}) copy-start(f32[2048]{0:T(1024)} %param.19) | copy-start | bytes 24580
  29.2 5.2 %collective-permute-start = (bf16[4,128,128]{2,1,0:T(8,128)(2,1)S(1)}, bf16[4,128,128]{2,1,0:T(8,128)(2,1)S(1)}, u32[]{:S(2)}, u32[]{:S(2)}) collective-permute-start(bf16[4,128,128]{2,1,0:T(8,128)(2,1)S(1)} %get-tuple-element.30), channel_id=1, source_target_pairs={{0,1},{1,0},{2,3},{3,2},{4,5},{5,4},{6,7},{7,6},{8,9},{9,8},{10,11... | collective-permute-start | bytes 393224 | tf_op jit(solution)/shard_map/ppermute | solution.py:311
  30.6 3.8 %copy-start.19 = (bf16[1024,128]{1,0:T(8,128)(2,1)}, bf16[1024,128]{1,0:T(8,128)(2,1)S(1)}, u32[]{:S(2)}) copy-start(bf16[1024,128]{1,0:T(8,128)(2,1)S(1)} %collective-permute-done.18.refs_2_) | copy-start | bytes 786436
  30.6 15.7 %collective-permute-start.6 = (bf16[128,2048]{1,0:T(8,128)(2,1)}, bf16[128,2048]{1,0:T(8,128)(2,1)S(1)}, u32[]{:S(2)}, u32[]{:S(2)}) collective-permute-start(bf16[128,2048]{1,0:T(8,128)(2,1)} %s0.1), channel_id=1, source_target_pairs={{0,4},{2,6},{4,0},{6,2},{1,5},{3,7},{5,1},{7,3},{8,12},{10,14},{12... | collective-permute-start | bytes 1572872 | tf_op jit(solution)/shard_map/ppermute | solution.py:307
  33.3 5.7 %collective-permute-start.19 = (bf16[1024,128]{1,0:T(8,128)(2,1)}, bf16[1024,128]{1,0:T(8,128)(2,1)S(1)}, u32[]{:S(2)}, u32[]{:S(2)}) collective-permute-start(bf16[1024,128]{1,0:T(8,128)(2,1)} %collective-permute-done.17.refs_1_), channel_id=1, source_target_pairs={{0,32},{1,97},{32,64},{33,1},{64,96},{65,33},{96,0},{97,65},{2,34}... | collective-permute-start | bytes 786440 | tf_op jit(solution)/shard_map/ppermute | solution.py:316
  34.4 32.7 %collective-permute-start.11 = (bf16[4,128,1024]{2,1,0:T(8,128)(2,1)S(1)}, bf16[4,128,1024]{2,1,0:T(8,128)(2,1)S(1)}, u32[]{:S(2)}, u32[]{:S(2)}) collective-permute-start(bf16[4,128,1024]{2,1,0:T(8,128)(2,1)S(1)} %shard_map.113.refs_0_), channel_id=1, source_target_pairs={{0,32},{1,97},{32,64},{33,1},{64,96},{65,33},{96,0},{97,65},{2,34}... | collective-permute-start | bytes 3145736 | tf_op jit(solution)/shard_map/ppermute | solution.py:316
  35.5 43.9 %collective-permute-start.10 = (bf16[4,128,1024]{2,1,0:T(8,128)(2,1)S(1)}, bf16[4,128,1024]{2,1,0:T(8,128)(2,1)S(1)}, u32[]{:S(2)}, u32[]{:S(2)}) collective-permute-start(bf16[4,128,1024]{2,1,0:T(8,128)(2,1)S(1)} %shard_map.113.refs_0_), channel_id=1, source_target_pairs={{0,1},{1,0},{2,3},{3,2},{4,5},{5,4},{6,7},{7,6},{8,9},{9,8},{10,11... | collective-permute-start | bytes 3145736 | tf_op jit(solution)/shard_map/ppermute | solution.py:311
  36.0 32.5 %collective-permute-start.12 = (bf16[4,128,1024]{2,1,0:T(8,128)(2,1)S(1)}, bf16[4,128,1024]{2,1,0:T(8,128)(2,1)S(1)}, u32[]{:S(2)}, u32[]{:S(2)}) collective-permute-start(bf16[4,128,1024]{2,1,0:T(8,128)(2,1)S(1)} %shard_map.113.refs_0_), channel_id=1, source_target_pairs={{0,96},{1,33},{32,0},{33,65},{64,32},{65,97},{96,64},{97,1},{2,98}... | collective-permute-start | bytes 3145736 | tf_op jit(solution)/shard_map/ppermute | solution.py:316
  39.1 10.7 %collective-permute-start.1 = (bf16[2,4,128,128]{3,2,1,0:T(8,128)(2,1)S(1)}, bf16[2,4,128,128]{3,2,1,0:T(8,128)(2,1)S(1)}, u32[]{:S(2)}, u32[]{:S(2)}) collective-permute-start(bf16[2,4,128,128]{3,2,1,0:T(8,128)(2,1)S(1)} %pad_maximum_fusion.g0), channel_id=1, source_target_pairs={{0,2},{2,4},{4,6},{6,0},{1,3},{3,5},{5,7},{7,1},{8,10},{10,12},{12... | collective-permute-start | bytes 786440 | tf_op jit(solution)/shard_map/ppermute | solution.py:307
  47.1 32.3 %collective-permute-start.24 = (bf16[4,1024,128]{2,1,0:T(8,128)(2,1)}, bf16[4,1024,128]{2,1,0:T(8,128)(2,1)}, u32[]{:S(2)}, u32[]{:S(2)}) collective-permute-start(bf16[4,1024,128]{2,1,0:T(8,128)(2,1)} %shard_map.115.d0), channel_id=1, source_target_pairs={{0,8},{1,25},{8,16},{9,1},{16,24},{17,9},{24,0},{25,17},{2,10},{3,... | collective-permute-start | bytes 3145736 | tf_op jit(solution)/shard_map/ppermute | solution.py:316
  50.5 6.2 %collective-permute-start.2 = (bf16[2,4,128,128]{3,2,1,0:T(8,128)(2,1)S(1)}, bf16[2,4,128,128]{3,2,1,0:T(8,128)(2,1)S(1)}, u32[]{:S(2)}, u32[]{:S(2)}) collective-permute-start(bf16[2,4,128,128]{3,2,1,0:T(8,128)(2,1)S(1)} %pad_maximum_fusion.g0), channel_id=1, source_target_pairs={{0,6},{2,0},{4,2},{6,4},{1,7},{3,1},{5,3},{7,5},{8,14},{10,8},{12,... | collective-permute-start | bytes 786440 | tf_op jit(solution)/shard_map/ppermute | solution.py:307
  57.4 7.7 %collective-permute-start.3 = (bf16[2,4,128,128]{3,2,1,0:T(8,128)(2,1)S(1)}, bf16[2,4,128,128]{3,2,1,0:T(8,128)(2,1)S(1)}, u32[]{:S(2)}, u32[]{:S(2)}) collective-permute-start(bf16[2,4,128,128]{3,2,1,0:T(8,128)(2,1)S(1)} %pad_maximum_fusion.g0), channel_id=1, source_target_pairs={{0,4},{2,6},{4,0},{6,2},{1,5},{3,7},{5,1},{7,3},{8,12},{10,14},{12... | collective-permute-start | bytes 786440 | tf_op jit(solution)/shard_map/ppermute | solution.py:307
  65.9 15.2 %collective-permute-start.25 = (bf16[4,1024,128]{2,1,0:T(8,128)(2,1)}, bf16[4,1024,128]{2,1,0:T(8,128)(2,1)}, u32[]{:S(2)}, u32[]{:S(2)}) collective-permute-start(bf16[4,1024,128]{2,1,0:T(8,128)(2,1)} %shard_map.115.d0), channel_id=1, source_target_pairs={{0,24},{1,9},{8,0},{9,17},{16,8},{17,25},{24,16},{25,1},{2,26},{3,... | collective-permute-start | bytes 3145736 | tf_op jit(solution)/shard_map/ppermute | solution.py:316
  67.1 33.5 %collective-permute-start.15 = (bf16[4,128,1024]{2,1,0:T(8,128)(2,1)S(1)}, bf16[4,128,1024]{2,1,0:T(8,128)(2,1)}, u32[]{:S(2)}, u32[]{:S(2)}) collective-permute-start(bf16[4,128,1024]{2,1,0:T(8,128)(2,1)S(1)} %collective-permute-done.11.refs_2_), channel_id=1, source_target_pairs={{0,32},{1,97},{32,64},{33,1},{64,96},{65,33},{96,0},{97,65},{2,34}... | collective-permute-start | bytes 3145736 | tf_op jit(solution)/shard_map/ppermute | solution.py:316
  68.4 32.2 %collective-permute-start.13 = (bf16[4,128,1024]{2,1,0:T(8,128)(2,1)S(1)}, bf16[4,128,1024]{2,1,0:T(8,128)(2,1)S(1)}, u32[]{:S(2)}, u32[]{:S(2)}) collective-permute-start(bf16[4,128,1024]{2,1,0:T(8,128)(2,1)S(1)} %collective-permute-done.12.refs_4_), channel_id=1, source_target_pairs={{0,1},{1,0},{2,3},{3,2},{4,5},{5,4},{6,7},{7,6},{8,9},{9,8},{10,11... | collective-permute-start | bytes 3145736 | tf_op jit(solution)/shard_map/ppermute | solution.py:311
  79.4 22.7 %collective-permute-start.14 = (bf16[4,128,1024]{2,1,0:T(8,128)(2,1)S(1)}, bf16[4,128,1024]{2,1,0:T(8,128)(2,1)S(1)}, u32[]{:S(2)}, u32[]{:S(2)}) collective-permute-start(bf16[4,128,1024]{2,1,0:T(8,128)(2,1)S(1)} %collective-permute-done.11.refs_2_), channel_id=1, source_target_pairs={{0,1},{1,0},{2,3},{3,2},{4,5},{5,4},{6,7},{7,6},{8,9},{9,8},{10,11... | collective-permute-start | bytes 3145736 | tf_op jit(solution)/shard_map/ppermute | solution.py:311
  79.4 23.7 %collective-permute-start.31 = (bf16[4,1024,128]{2,1,0:T(8,128)(2,1)}, bf16[4,1024,128]{2,1,0:T(8,128)(2,1)}, u32[]{:S(2)}, u32[]{:S(2)}) collective-permute-start(bf16[4,1024,128]{2,1,0:T(8,128)(2,1)} %collective-permute-done.24.refs_0_), channel_id=1, source_target_pairs={{0,8},{1,25},{8,16},{9,1},{16,24},{17,9},{24,0},{25,17},{2,10},{3,... | collective-permute-start | bytes 3145736 | tf_op jit(solution)/shard_map/ppermute | solution.py:316
  81.1 42.0 %collective-permute-start.20 = (bf16[4,1024,128]{2,1,0:T(8,128)(2,1)}, bf16[4,1024,128]{2,1,0:T(8,128)(2,1)}, u32[]{:S(2)}, u32[]{:S(2)}) collective-permute-start(bf16[4,1024,128]{2,1,0:T(8,128)(2,1)} %shard_map.115.d0), channel_id=1, source_target_pairs={{0,1},{1,0},{2,3},{3,2},{4,5},{5,4},{6,7},{7,6},{8,9},{9,8},{10,11... | collective-permute-start | bytes 3145736 | tf_op jit(solution)/shard_map/ppermute | solution.py:311
  100.6 22.5 %collective-permute-start.16 = (bf16[4,128,1024]{2,1,0:T(8,128)(2,1)}, bf16[4,128,1024]{2,1,0:T(8,128)(2,1)}, u32[]{:S(2)}, u32[]{:S(2)}) collective-permute-start(bf16[4,128,1024]{2,1,0:T(8,128)(2,1)} %collective-permute-done.15.u0), channel_id=1, source_target_pairs={{0,1},{1,0},{2,3},{3,2},{4,5},{5,4},{6,7},{7,6},{8,9},{9,8},{10,11... | collective-permute-start | bytes 3145736 | tf_op jit(solution)/shard_map/ppermute | solution.py:311
  101.6 29.1 %collective-permute-start.26 = (bf16[4,1024,128]{2,1,0:T(8,128)(2,1)}, bf16[4,1024,128]{2,1,0:T(8,128)(2,1)}, u32[]{:S(2)}, u32[]{:S(2)}) collective-permute-start(bf16[4,1024,128]{2,1,0:T(8,128)(2,1)} %collective-permute-done.25.refs_2_), channel_id=1, source_target_pairs={{0,1},{1,0},{2,3},{3,2},{4,5},{5,4},{6,7},{7,6},{8,9},{9,8},{10,11... | collective-permute-start | bytes 3145736 | tf_op jit(solution)/shard_map/ppermute | solution.py:311
  103.1 28.8 %collective-permute-start.27 = (bf16[4,1024,128]{2,1,0:T(8,128)(2,1)}, bf16[4,1024,128]{2,1,0:T(8,128)(2,1)}, u32[]{:S(2)}, u32[]{:S(2)}) collective-permute-start(bf16[4,1024,128]{2,1,0:T(8,128)(2,1)} %collective-permute-done.24.refs_0_), channel_id=1, source_target_pairs={{0,1},{1,0},{2,3},{3,2},{4,5},{5,4},{6,7},{7,6},{8,9},{9,8},{10,11... | collective-permute-start | bytes 3145736 | tf_op jit(solution)/shard_map/ppermute | solution.py:311
  103.1 34.5 %collective-permute-start.32 = (bf16[4,1024,128]{2,1,0:T(8,128)(2,1)}, bf16[4,1024,128]{2,1,0:T(8,128)(2,1)}, u32[]{:S(2)}, u32[]{:S(2)}) collective-permute-start(bf16[4,1024,128]{2,1,0:T(8,128)(2,1)} %collective-permute-done.31.refs_0_), channel_id=1, source_target_pairs={{0,1},{1,0},{2,3},{3,2},{4,5},{5,4},{6,7},{7,6},{8,9},{9,8},{10,11... | collective-permute-start | bytes 3145736 | tf_op jit(solution)/shard_map/ppermute | solution.py:311
  104.8 14.0 %copy-start.1 = (bf16[4,128,1024]{2,1,0:T(8,128)(2,1)S(1)}, bf16[4,128,1024]{2,1,0:T(8,128)(2,1)}, u32[]{:S(2)}) copy-start(bf16[4,128,1024]{2,1,0:T(8,128)(2,1)} %copy-done) | copy-start | bytes 3145732
  104.8 14.0 %copy-start.3 = (bf16[4,128,1024]{2,1,0:T(8,128)(2,1)S(1)}, bf16[4,128,1024]{2,1,0:T(8,128)(2,1)}, u32[]{:S(2)}) copy-start(bf16[4,128,1024]{2,1,0:T(8,128)(2,1)} %copy-done.2) | copy-start | bytes 3145732
  104.8 14.0 %copy-start.5 = (bf16[4,128,1024]{2,1,0:T(8,128)(2,1)S(1)}, bf16[4,128,1024]{2,1,0:T(8,128)(2,1)}, u32[]{:S(2)}) copy-start(bf16[4,128,1024]{2,1,0:T(8,128)(2,1)} %copy-done.4) | copy-start | bytes 3145732
  127.2 13.9 %collective-permute-start.21 = (bf16[128,512]{1,0:T(8,128)(2,1)S(1)}, bf16[128,512]{1,0:T(8,128)(2,1)S(1)}, u32[]{:S(2)}, u32[]{:S(2)}) collective-permute-start(bf16[128,512]{1,0:T(8,128)(2,1)S(1)} %get-tuple-element.35), channel_id=1, source_target_pairs={{0,6},{2,0},{4,2},{6,4},{1,7},{3,1},{5,3},{7,5},{8,14},{10,8},{12,... | collective-permute-start | bytes 393224 | tf_op jit(solution)/shard_map/ppermute | solution.py:307
  130.7 11.3 %collective-permute-start.22 = (bf16[128,512]{1,0:T(8,128)(2,1)S(1)}, bf16[128,512]{1,0:T(8,128)(2,1)S(1)}, u32[]{:S(2)}, u32[]{:S(2)}) collective-permute-start(bf16[128,512]{1,0:T(8,128)(2,1)S(1)} %get-tuple-element.36), channel_id=1, source_target_pairs={{0,2},{2,4},{4,6},{6,0},{1,3},{3,5},{5,7},{7,1},{8,10},{10,12},{12... | collective-permute-start | bytes 393224 | tf_op jit(solution)/shard_map/ppermute | solution.py:307
  130.7 13.7 %collective-permute-start.23 = (bf16[128,512]{1,0:T(8,128)(2,1)S(1)}, bf16[128,512]{1,0:T(8,128)(2,1)S(1)}, u32[]{:S(2)}, u32[]{:S(2)}) collective-permute-start(bf16[128,512]{1,0:T(8,128)(2,1)S(1)} %get-tuple-element.37), channel_id=1, source_target_pairs={{0,4},{2,6},{4,0},{6,2},{1,5},{3,7},{5,1},{7,3},{8,12},{10,14},{12... | collective-permute-start | bytes 393224 | tf_op jit(solution)/shard_map/ppermute | solution.py:307
  132.0 28.4 %copy-start.7 = (s32[4]{0:T(128)S(1)}, s32[4]{0:T(128)}, u32[]{:S(2)}) copy-start(s32[4]{0:T(128)} %pad_add_fusion.pos) | copy-start | bytes 52
  136.1 24.2 %collective-permute-start.28 = (bf16[128,1024]{1,0:T(8,128)(2,1)S(1)}, bf16[128,1024]{1,0:T(8,128)(2,1)S(1)}, u32[]{:S(2)}, u32[]{:S(2)}) collective-permute-start(bf16[128,1024]{1,0:T(8,128)(2,1)S(1)} %get-tuple-element.40), channel_id=1, source_target_pairs={{0,6},{2,0},{4,2},{6,4},{1,7},{3,1},{5,3},{7,5},{8,14},{10,8},{12,... | collective-permute-start | bytes 786440 | tf_op jit(solution)/shard_map/ppermute | solution.py:307
  140.4 6.4 %collective-permute-start.33 = (bf16[128,512]{1,0:T(8,128)(2,1)S(1)}, bf16[128,512]{1,0:T(8,128)(2,1)S(1)}, u32[]{:S(2)}, u32[]{:S(2)}) collective-permute-start(bf16[128,512]{1,0:T(8,128)(2,1)S(1)} %get-tuple-element.44), channel_id=1, source_target_pairs={{0,6},{2,0},{4,2},{6,4},{1,7},{3,1},{5,3},{7,5},{8,14},{10,8},{12,... | collective-permute-start | bytes 393224 | tf_op jit(solution)/shard_map/ppermute | solution.py:307
  141.1 19.2 %collective-permute-start.29 = (bf16[128,1024]{1,0:T(8,128)(2,1)S(1)}, bf16[128,1024]{1,0:T(8,128)(2,1)S(1)}, u32[]{:S(2)}, u32[]{:S(2)}) collective-permute-start(bf16[128,1024]{1,0:T(8,128)(2,1)S(1)} %get-tuple-element.41), channel_id=1, source_target_pairs={{0,2},{2,4},{4,6},{6,0},{1,3},{3,5},{5,7},{7,1},{8,10},{10,12},{12... | collective-permute-start | bytes 786440 | tf_op jit(solution)/shard_map/ppermute | solution.py:307
  142.0 18.3 %collective-permute-start.30 = (bf16[128,1024]{1,0:T(8,128)(2,1)S(1)}, bf16[128,1024]{1,0:T(8,128)(2,1)S(1)}, u32[]{:S(2)}, u32[]{:S(2)}) collective-permute-start(bf16[128,1024]{1,0:T(8,128)(2,1)S(1)} %get-tuple-element.42), channel_id=1, source_target_pairs={{0,4},{2,6},{4,0},{6,2},{1,5},{3,7},{5,1},{7,3},{8,12},{10,14},{12... | collective-permute-start | bytes 786440 | tf_op jit(solution)/shard_map/ppermute | solution.py:307
  144.3 11.8 %collective-permute-start.34 = (bf16[128,512]{1,0:T(8,128)(2,1)S(1)}, bf16[128,512]{1,0:T(8,128)(2,1)S(1)}, u32[]{:S(2)}, u32[]{:S(2)}) collective-permute-start(bf16[128,512]{1,0:T(8,128)(2,1)S(1)} %get-tuple-element.45), channel_id=1, source_target_pairs={{0,2},{2,4},{4,6},{6,0},{1,3},{3,5},{5,7},{7,1},{8,10},{10,12},{12... | collective-permute-start | bytes 393224 | tf_op jit(solution)/shard_map/ppermute | solution.py:307
  146.8 13.5 %collective-permute-start.35 = (bf16[128,512]{1,0:T(8,128)(2,1)S(1)}, bf16[128,512]{1,0:T(8,128)(2,1)S(1)}, u32[]{:S(2)}, u32[]{:S(2)}) collective-permute-start(bf16[128,512]{1,0:T(8,128)(2,1)S(1)} %get-tuple-element.46), channel_id=1, source_target_pairs={{0,4},{2,6},{4,0},{6,2},{1,5},{3,7},{5,1},{7,3},{8,12},{10,14},{12... | collective-permute-start | bytes 393224 | tf_op jit(solution)/shard_map/ppermute | solution.py:307
  (19 other events, 18.5 us)
where the time goes:
time: 165 us; the launch traced here: 162 us
  starting transfers between devices  79.7 us (48%)
  Pallas kernels  32.7 us (20%)
  waiting for transfers between devices  30.2 us (18%)
  local copies, waits for them, and re-layouts  18.5 us (11%)
    ppermute x9, starting transfers between devices, swapped(): return lax.ppermute(v, 'c', [(0, 1), (1, 0)])  32.4 us
    pallas_call x10, Pallas kernels, launched(): pl.pallas_call(kernel, in_specs=ins, out_specs=[spec] * len(outs), out_sh...  31.5 us
    ppermute x15, waiting for transfers between devices, shifted(): return lax.ppermute(v, axis, [(i, (i + by) % n) for i in range(n)])  26.3 us
    ppermute x15, starting transfers between devices, shifted(): return lax.ppermute(v, axis, [(i, (i + by) % n) for i in range(n)])  22.8 us
    unnamed x60, local copies, waits for them, and re-layouts  18.5 us
    ppermute x12, starting transfers between devices, both_ways(): return lax.ppermute(v, (axis, 'c'), pairs)  17 us
    all_to_all x1, starting transfers between devices, local(): got = lax.all_to_all(sent, SP, 0, 0, tiled=True)  7.53 us
  transfers between devices with their start and end apart: 37, of which 10 were waited for; matrix products, arithmetic and copies ran while one was open for 0% of the time, Pallas kernels for 19%

commit v1 on v0

--- a/solution.py
+++ b/solution.py
@@ -26,7 +26,6 @@
 NEAR = (0, -1, 1, 2)
 
 VMEM = pl.BlockSpec(memory_space=pltpu.VMEM)
-SMEM = pl.BlockSpec(memory_space=pltpu.SMEM)
 ANY = pl.BlockSpec(memory_space=pl.ANY)
 HBM = pl.BlockSpec(memory_space=pltpu.HBM)
 
@@ -35,7 +34,12 @@
     return lax.dot_general(a, b, (dims, ((), ())), precision=precision, preferred_element_type=f32)
 
 
-def attend_kernel(pos, q_ref, k_ref, v_ref, ld_ref, local_ref, carry_ref, send_ref, qd_s, tot_s, inc_s):
+def position():
+    return tuple(lax.axis_index(a) for a in SP + TP)
+
+
+def attend_kernel(q_ref, k_ref, v_ref, ld_ref, local_ref, carry_ref, send_ref, qd_s, tot_s, inc_s):
+    pos = position()
     length = q_ref.shape[1]
     count = length // BLOCK
     me = pos[0] * 4 + pos[1]
@@ -107,7 +111,8 @@
         send_ref[peer, half:] = jnp.where(later, to_later[1], to_earlier[1])
 
 
-def gate_kernel(pos, got_ref, local_hbm, carry_hbm, gate_hbm, gain_ref, keep_ref, give_ref, both_s, local_ref, carry_ref, gate_ref, sems):
+def gate_kernel(got_ref, local_hbm, carry_hbm, gate_hbm, gain_ref, keep_ref, give_ref, both_s, local_ref, carry_ref, gate_ref, sems):
+    pos = position()
     loads = ((carry_hbm, carry_ref), (local_hbm, local_ref), (gate_hbm, gate_ref))
     loads = [pltpu.make_async_copy(src, dst, sems.at[n]) for n, (src, dst) in enumerate(loads)]
     for load in loads:
@@ -140,14 +145,9 @@
     give_ref[...] = both_s[1]
 
 
-def mix_kernel(pos, g0, g1, g2, g3, s0, s1, s2, s3, w_hbm, gain_ref, near_ref, far_ref, own_ref, xs, res, w_ref, sems):
+def mix_kernel(g0, g1, g2, g3, s0, s1, s2, s3, w_ref, gain_ref, near_ref, far_ref, own_ref, xs, res):
+    pos = position()
     wide = 512
-    loads = []
-    for n in range(D // wide):
-        cols = pl.ds(n * wide, wide)
-        loads.append(pltpu.make_async_copy(w_hbm.at[:, cols], w_ref.at[:, cols], sems.at[n]))
-    for load in loads:
-        load.start()
     first = pos[3] == 0
     for d, g in enumerate((g0, g1, g2, g3)):
         for k in range(4):
@@ -159,7 +159,6 @@
     for n in range(D // wide):
         cols = slice(n * wide, (n + 1) * wide)
         acc = None
-        loads[n].wait()
         for d in range(4):
             at = pl.multiple_of(lax.rem(pos[2] + (NEAR[d] + 4), 4) * 256, 256)
             part = dot(xs[:, d * 256 : (d + 1) * 256], w_ref[pl.ds(at, 256), cols])
@@ -258,7 +257,8 @@
             o[:, cols] = part[k * ROWS : (k + 1) * ROWS]
 
 
-def end_kernel(pos, res_ref, *refs):
+def end_kernel(res_ref, *refs):
+    pos = position()
     parts, out_ref = [refs[4 * n : 4 * n + 4] for n in range(3)], refs[12]
     e = 2 * pos[3] - 1
     steps = (0, e, -e, 2)
@@ -273,6 +273,19 @@
             out_ref[:, at] = (res_ref[:, at].astype(f32) + total).astype(bf16)
 
 
+def relay_kernel(*refs):
+    out_ref, held, sems = refs[4:]
+    inward = [pltpu.make_async_copy(refs[i], held.at[i], sems.at[i]) for i in range(4)]
+    outward = [pltpu.make_async_copy(held.at[i], out_ref.at[i], sems.at[4 + i]) for i in range(4)]
+    for copy in inward:
+        copy.start()
+    for i in range(4):
+        inward[i].wait()
+        outward[i].start()
+    for copy in outward:
+        copy.wait()
+
+
 def join_kernel(*refs):
     out_ref, sems = refs[4:]
     copies = [pltpu.make_async_copy(refs[i], out_ref.at[i], sems.at[i]) for i in range(4)]
@@ -282,9 +295,10 @@
         copy.wait()
 
 
-def mark_kernel(pos, out_ref):
-    for i in range(4):
-        out_ref[i] = pos[i]
+def load_kernel(w_ref, out_ref, sem):
+    copy = pltpu.make_async_copy(w_ref, out_ref, sem)
+    copy.start()
+    copy.wait()
 
 
 def call(kernel, ins, outs, scratch, args, flops, nbytes, limit, spec=VMEM):
@@ -314,6 +328,12 @@
 def both_ways(v, axis, sign):
     pairs = [(2 * i + c, 2 * ((i + sign * (1 - 2 * c)) % 4) + c) for i in range(4) for c in range(2)]
     return lax.ppermute(v, (axis, "c"), pairs)
+
+
+def relayed(blocks):
+    shape = (4, *blocks[0].shape)
+    scratch = [pltpu.VMEM(shape, bf16), pltpu.SemaphoreType.DMA((8,))]
+    return call(relay_kernel, [HBM] * 4, [(shape, bf16)], scratch, blocks, 800_000_000, 2_000_000, 60, HBM)[0]
 
 
 def joined(blocks):
@@ -336,21 +356,20 @@
     down_weight,
 ):
     length = queries.shape[0]
-    pos = jnp.stack([lax.axis_index(a) for a in ("z", "y", "x", "c")]).astype(jnp.int32)
 
     up_a, up_b = both_ways(up_weight, "y", 1), both_ways(up_weight, "y", -1)
     down_a, down_b = both_ways(down_weight, "z", 1), both_ways(down_weight, "z", -1)
 
     rows_out, carry, sent = call(
         attend_kernel,
-        [SMEM] + [VMEM] * 4,
+        [VMEM] * 4,
         [((length, HEAD_V), f32), ((length, 2 * HEAD_K), bf16), ((PEERS, FOLD, 128), bf16)],
         [
             pltpu.VMEM((length, 2 * HEAD_K), f32),
             pltpu.VMEM((length // BLOCK, 2 * HEAD_K), f32),
             pltpu.VMEM((length // BLOCK, HEAD_V, 2 * HEAD_K), f32),
         ],
-        (pos, queries.T, keys.T, values, decay_logit.transpose(0, 2, 1)),
+        (queries.T, keys.T, values, decay_logit.transpose(0, 2, 1)),
         2_000_000_000,
         2_000_000,
         60,
@@ -361,7 +380,7 @@
     streams = [streams[0], streams[2], streams[3], streams[1]]
     got = lax.all_to_all(sent, SP, 0, 0, tiled=True)
     up_line = joined((up_weight, up_a, up_b, up_2))
-    down_line = joined((down_weight, down_a, down_b, down_2))
+    down_line = relayed((down_weight, down_a, down_b, down_2))
     up_na, up_nb = both_ways(up_line, "z", 1), both_ways(up_line, "z", -1)
     down_na, down_nb = both_ways(down_line, "y", 1), both_ways(down_line, "y", -1)
     up_n2 = both_ways(up_na, "z", 1)
@@ -372,7 +391,7 @@
     downs_s = [swapped(v) for v in downs]
     keep, give = call(
         gate_kernel,
-        [SMEM, VMEM, HBM, HBM, HBM, VMEM],
+        [VMEM, HBM, HBM, HBM, VMEM],
         [((4, ROWS, HEAD_V), bf16)] * 2,
         [
             pltpu.VMEM((2, 4, ROWS, HEAD_V), bf16),
@@ -381,28 +400,33 @@
             pltpu.VMEM((length, HEAD_V), bf16),
             pltpu.SemaphoreType.DMA((3,)),
         ],
-        (pos, got, rows_out, carry, out_gate, head_gain.reshape(1, HEAD_V)),
+        (got, rows_out, carry, out_gate, head_gain.reshape(1, HEAD_V)),
         1_000_000_000,
         2_000_000,
-        8,
+        60,
     )
     pair = jnp.stack([keep, swapped(give)])
     heads = {k: shifted(pair, "x", NEAR[k]) for k in (1, 2, 3)}
     heads = [pair, heads[2], heads[1], heads[3]]
-    pos2 = pl.pallas_call(
-        mark_kernel, in_specs=[SMEM], out_specs=SMEM, out_shape=jax.ShapeDtypeStruct((4,), jnp.int32)
-    )(pos)
+    mixing = call(
+        load_kernel,
+        [HBM],
+        [(out_weight.shape, bf16)],
+        [pltpu.SemaphoreType.DMA],
+        (out_weight,),
+        1000,
+        10000,
+        1,
+    )[0]
     near, far, residual = call(
         mix_kernel,
-        [SMEM] + [VMEM] * 8 + [HBM, VMEM],
+        [VMEM] * 10,
         [((4 * ROWS, 1536), bf16), ((4 * ROWS, 512), bf16), ((ROWS, D), bf16)],
         [
             pltpu.VMEM((4 * ROWS, 1024), bf16),
             pltpu.VMEM((4 * ROWS, D), bf16),
-            pltpu.VMEM((1024, D), bf16),
-            pltpu.SemaphoreType.DMA((4,)),
         ],
-        (pos2, *heads, *streams, out_weight, mlp_gain.reshape(1, D)),
+        (*heads, *streams, mixing, mlp_gain.reshape(1, D)),
         2 * 512 * 1024 * 2048,
         12_000_000,
         24,
@@ -450,10 +474,10 @@
     third = sent_back(down((3,)))
     return call(
         end_kernel,
-        [SMEM] + [VMEM] * 13,
+        [VMEM] * 13,
         [((ROWS, D), bf16)],
         [],
-        (pos, residual, *first, *second, *third),
+        (residual, *first, *second, *third),
         100_000_000,
         3_000_000,
         8,

time: 165 us -> 151 us (0.915)
  local copies, waits for them, and re-layouts: 18.5 us -> 5.18 us
  waiting for transfers between devices: 30.2 us -> 33.8 us
  Pallas kernels: 32.7 us -> 30.6 us
    unnamed x60 -> x22, local copies, waits for them, and re-layouts: 18.5 us -> 5.18 us
    ppermute x15, waiting for transfers between devices: 26.3 us -> 28.6 us  [shifted(): return lax.ppermute(v, axis, [(i, (i + by) % n) for i in range(n)])]
    ppermute x12, starting transfers between devices: 17 us -> 15.4 us  [both_ways(): return lax.ppermute(v, (axis, 'c'), pairs)]
    pallas_call x10 -> x11, Pallas kernels: 31.5 us -> 30.6 us  [launched(): pl.pallas_call(kernel, in_specs=ins, out_specs=[spec] * len(outs), out_sh...]
  transfers between devices with their start and end apart: 37 -> 37, of which waited for: 10 -> 10; matrix products, arithmetic and copies ran while one was open for 0% -> 1% of each run, Pallas kernels for 19% -> 20%
where the time goes in v1:
time: 151 us; the launch traced here: 149 us
  starting transfers between devices  78.2 us (52%)
  waiting for transfers between devices  33.8 us (22%)
  Pallas kernels  30.6 us (20%)
  local copies, waits for them, and re-layouts  5.18 us (3%)
    ppermute x9, starting transfers between devices, swapped(): return lax.ppermute(v, 'c', [(0, 1), (1, 0)])  33.7 us
    pallas_call x11, Pallas kernels, launched(): pl.pallas_call(kernel, in_specs=ins, out_specs=[spec] * len(outs), out_sh...  30.6 us
    ppermute x15, waiting for transfers between devices, shifted(): return lax.ppermute(v, axis, [(i, (i + by) % n) for i in range(n)])  28.6 us
    ppermute x15, starting transfers between devices, shifted(): return lax.ppermute(v, axis, [(i, (i + by) % n) for i in range(n)])  21.6 us
    ppermute x12, starting transfers between devices, both_ways(): return lax.ppermute(v, (axis, 'c'), pairs)  15.4 us
    all_to_all x1, starting transfers between devices, local(): got = lax.all_to_all(sent, SP, 0, 0, tiled=True)  7.53 us
    unnamed x22, local copies, waits for them, and re-layouts  5.18 us
    ppermute x12, waiting for transfers between devices, both_ways(): return lax.ppermute(v, (axis, 'c'), pairs)  3.92 us
  transfers between devices with their start and end apart: 37, of which 10 were waited for; matrix products, arithmetic and copies ran while one was open for 1% of the time, Pallas kernels for 20%

profile of v1, /device:TPU:1, one launch (start us, length us, event | category | flops | bytes accessed | tf_op | source)
XLA Modules:
  0.0 148.9 jit_solution(12754653301153110249)
XLA Ops:
  0.0 3.6 %collective-permute-start.7 = (bf16[128,1024]{1,0:T(8,128)(2,1)}, bf16[128,1024]{1,0:T(8,128)(2,1)S(1)}, u32[]{:S(2)}, u32[]{:S(2)}) collective-permute-start(bf16[128,1024]{1,0:T(8,128)(2,1)} %refs_0_.2), channel_id=1, source_target_pairs={{0,8},{1,25},{8,16},{9,1},{16,24},{17,9},{24,0},{25,17},{2,10},{3,... | collective-permute-start | bytes 786440 | tf_op jit(solution)/shard_map/ppermute | solution.py:330
  3.6 4.9 %shard_map.109 = (f32[1024,128]{1,0:T(8,128)}, bf16[1024,128]{1,0:T(8,128)(2,1)}, bf16[16,80,128]{2,1,0:T(8,128)(2,1)}) custom-call(bf16[64,1024]{1,0:T(8,128)(2,1)} %bitcast.11, bf16[64,1024]{1,0:T(8,128)(2,1)} %bitcast.12, bf16[1024,128]{1,0:T(8,128)(2,1)} %v_ref.1, f32[2,64,1024]{2,1,0:T(8,128)} %bitcast.10), custom_call_target="tpu_custom_call" | custom-call | flops 2000000000 | bytes 2000000 | tf_op jit(solution)/shard_map/pallas_call | solution.py:309
  8.5 7.5 %all-to-all-start = ((bf16[16,80,128]{2,1,0:T(8,128)(2,1)}), bf16[16,80,128]{2,1,0:T(8,128)(2,1)S(1)}, u32[]{:S(2)}, u32[]{:S(2)}) async-start(bf16[16,80,128]{2,1,0:T(8,128)(2,1)} %get-tuple-element.26), calls=%async_computation | async-start | bytes 655360 | tf_op jit(solution)/shard_map/all_to_all | solution.py:381
  16.0 2.6 %collective-permute-start.17 = (bf16[1024,128]{1,0:T(8,128)(2,1)S(1)}, bf16[1024,128]{1,0:T(8,128)(2,1)}, u32[]{:S(2)}, u32[]{:S(2)}) collective-permute-start(bf16[1024,128]{1,0:T(8,128)(2,1)S(1)} %copy-done.8), channel_id=1, source_target_pairs={{0,32},{1,97},{32,64},{33,1},{64,96},{65,33},{96,0},{97,65},{2,34}... | collective-permute-start | bytes 786440 | tf_op jit(solution)/shard_map/ppermute | solution.py:330
  18.7 1.2 collective-permute-start.4
  19.9 1.5 collective-permute-start.5
  21.4 2.4 %collective-permute-start.9 = (bf16[128,1024]{1,0:T(8,128)(2,1)S(1)}, bf16[128,1024]{1,0:T(8,128)(2,1)S(1)}, u32[]{:S(2)}, u32[]{:S(2)}) collective-permute-start(bf16[128,1024]{1,0:T(8,128)(2,1)S(1)} %collective-permute-done.7.refs_1_), channel_id=1, source_target_pairs={{0,8},{1,25},{8,16},{9,1},{16,24},{17,9},{24,0},{25,17},{2,10},{3,... | collective-permute-start | bytes 786440 | tf_op jit(solution)/shard_map/ppermute | solution.py:330
  23.7 1.3 all-to-all-done.got_ref
  25.0 0.7 copy-done.7
  25.7 3.4 %shard_map.110 = (bf16[4,128,128]{2,1,0:T(8,128)(2,1)}, bf16[4,128,128]{2,1,0:T(8,128)(2,1)}) custom-call(bf16[16,80,128]{2,1,0:T(8,128)(2,1)} %copy-done.7, f32[1024,128]{1,0:T(8,128)} %get-tuple-element.27.local_hbm, bf16[1024,128]{1,0:T(8,128)(2,1)} %get-tuple-element.28.carry_hbm, bf16[1024,128]{1,0:T(8,128)(2,1)} %gate_hbm.1, f32[1,128]{1,0:T(1,128)} %bitcast.13), custom_call_target="tpu_custom_call" | custom-call | flops 1000000000 | bytes 2000000 | tf_op jit(solution)/shard_map/pallas_call | solution.py:309
  29.2 1.4 collective-permute-start
  30.6 2.7 %collective-permute-start.6 = (bf16[128,2048]{1,0:T(8,128)(2,1)S(1)}, bf16[128,2048]{1,0:T(8,128)(2,1)}, u32[]{:S(2)}, u32[]{:S(2)}) collective-permute-start(bf16[128,2048]{1,0:T(8,128)(2,1)S(1)} %copy-done.2), channel_id=1, source_target_pairs={{0,4},{2,6},{4,0},{6,2},{1,5},{3,7},{5,1},{7,3},{8,12},{10,14},{12... | collective-permute-start | bytes 1572872 | tf_op jit(solution)/shard_map/ppermute | solution.py:321
  33.3 0.7 collective-permute-start.19
  34.5 0.8 copy-done.3
  35.6 1.2 collective-permute-start.12
  36.8 0.9 pad_maximum_fusion.g0
  37.8 1.5 %collective-permute-done.19.refs_3_ = bf16[1024,128]{1,0:T(8,128)(2,1)S(1)} collective-permute-done((bf16[1024,128]{1,0:T(8,128)(2,1)}, bf16[1024,128]{1,0:T(8,128)(2,1)S(1)}, u32[]{:S(2)}, u32[]{:S(2)}) %collective-permute-start.19) | collective-permute-done | bytes 262176 | tf_op jit(solution)/shard_map/ppermute | solution.py:330
  39.3 0.7 copy-done.10
  40.3 2.0 %shard_map.115.d0 = bf16[4,1024,128]{2,1,0:T(8,128)(2,1)} custom-call(bf16[1024,128]{1,0:T(8,128)(2,1)} %refs_0_.3, bf16[1024,128]{1,0:T(8,128)(2,1)} %collective-permute-done.17.refs_1_, bf16[1024,128]{1,0:T(8,128)(2,1)} %copy-done.9, bf16[1024,128]{1,0:T(8,128)(2,1)} %copy-done.10), custom_call_target="tpu_custom_call" | custom-call | flops 800000000 | bytes 2000000 | tf_op jit(solution)/shard_map/pallas_call | solution.py:309
  42.3 3.3 %collective-permute-done.6.s3 = bf16[128,2048]{1,0:T(8,128)(2,1)} collective-permute-done((bf16[128,2048]{1,0:T(8,128)(2,1)S(1)}, bf16[128,2048]{1,0:T(8,128)(2,1)}, u32[]{:S(2)}, u32[]{:S(2)}) %collective-permute-start.6) | collective-permute-done | bytes 524320 | tf_op jit(solution)/shard_map/ppermute | solution.py:321
  45.6 2.4 %collective-permute-start.24 = (bf16[4,1024,128]{2,1,0:T(8,128)(2,1)}, bf16[4,1024,128]{2,1,0:T(8,128)(2,1)S(1)}, u32[]{:S(2)}, u32[]{:S(2)}) collective-permute-start(bf16[4,1024,128]{2,1,0:T(8,128)(2,1)} %shard_map.115.d0), channel_id=1, source_target_pairs={{0,8},{1,25},{8,16},{9,1},{16,24},{17,9},{24,0},{25,17},{2,10},{3,... | collective-permute-start | bytes 3145736 | tf_op jit(solution)/shard_map/ppermute | solution.py:330
  47.9 0.9 collective-permute-done.1.g1
  48.9 1.0 collective-permute-start.2
  49.8 6.1 %collective-permute-done.2.g2 = bf16[2,4,128,128]{3,2,1,0:T(8,128)(2,1)S(1)} collective-permute-done((bf16[2,4,128,128]{3,2,1,0:T(8,128)(2,1)S(1)}, bf16[2,4,128,128]{3,2,1,0:T(8,128)(2,1)S(1)}, u32[]{:S(2)}, u32[]{:S(2)}) %collective-permute-start.2) | collective-permute-done | bytes 262176 | tf_op jit(solution)/shard_map/ppermute | solution.py:321
  55.9 4.1 %collective-permute-start.3 = (bf16[2,4,128,128]{3,2,1,0:T(8,128)(2,1)S(1)}, bf16[2,4,128,128]{3,2,1,0:T(8,128)(2,1)S(1)}, u32[]{:S(2)}, u32[]{:S(2)}) collective-permute-start(bf16[2,4,128,128]{3,2,1,0:T(8,128)(2,1)S(1)} %pad_maximum_fusion.g0), channel_id=1, source_target_pairs={{0,4},{2,6},{4,0},{6,2},{1,5},{3,7},{5,1},{7,3},{8,12},{10,14},{12... | collective-permute-start | bytes 786440 | tf_op jit(solution)/shard_map/ppermute | solution.py:321
  60.0 3.8 %collective-permute-done.3.g3 = bf16[2,4,128,128]{3,2,1,0:T(8,128)(2,1)S(1)} collective-permute-done((bf16[2,4,128,128]{3,2,1,0:T(8,128)(2,1)S(1)}, bf16[2,4,128,128]{3,2,1,0:T(8,128)(2,1)S(1)}, u32[]{:S(2)}, u32[]{:S(2)}) %collective-permute-start.3) | collective-permute-done | bytes 262176 | tf_op jit(solution)/shard_map/ppermute | solution.py:321
  64.3 1.2 collective-permute-start.15
  65.5 10.4 %collective-permute-start.13 = (bf16[4,128,1024]{2,1,0:T(8,128)(2,1)}, bf16[4,128,1024]{2,1,0:T(8,128)(2,1)S(1)}, u32[]{:S(2)}, u32[]{:S(2)}) collective-permute-start(bf16[4,128,1024]{2,1,0:T(8,128)(2,1)} %collective-permute-done.12.refs_4_), channel_id=1, source_target_pairs={{0,1},{1,0},{2,3},{3,2},{4,5},{5,4},{6,7},{7,6},{8,9},{9,8},{10,11... | collective-permute-start | bytes 3145736 | tf_op jit(solution)/shard_map/ppermute | solution.py:325
  76.5 2.4 %collective-permute-done.25.refs_2_ = bf16[4,1024,128]{2,1,0:T(8,128)(2,1)S(1)} collective-permute-done((bf16[4,1024,128]{2,1,0:T(8,128)(2,1)}, bf16[4,1024,128]{2,1,0:T(8,128)(2,1)S(1)}, u32[]{:S(2)}, u32[]{:S(2)}) %collective-permute-start.25) | collective-permute-done | bytes 1048608 | tf_op jit(solution)/shard_map/ppermute | solution.py:330
  78.9 20.5 %collective-permute-start.20 = (bf16[4,1024,128]{2,1,0:T(8,128)(2,1)}, bf16[4,1024,128]{2,1,0:T(8,128)(2,1)S(1)}, u32[]{:S(2)}, u32[]{:S(2)}) collective-permute-start(bf16[4,1024,128]{2,1,0:T(8,128)(2,1)} %shard_map.115.d0), channel_id=1, source_target_pairs={{0,1},{1,0},{2,3},{3,2},{4,5},{5,4},{6,7},{7,6},{8,9},{9,8},{10,11... | collective-permute-start | bytes 3145736 | tf_op jit(solution)/shard_map/ppermute | solution.py:325
  100.4 2.2 %copy-done = bf16[1024,2048]{1,0:T(8,128)(2,1)S(1)} copy-done((bf16[1024,2048]{1,0:T(8,128)(2,1)S(1)}, bf16[1024,2048]{1,0:T(8,128)(2,1)}, u32[]{:S(2)}) %copy-start) | copy-done | bytes 4194328
  102.9 0.7 copy-done.4
  103.6 4.6 %shard_map.112 = (bf16[512,1536]{1,0:T(8,128)(2,1)S(1)}, bf16[512,512]{1,0:T(8,128)(2,1)S(1)}, bf16[128,2048]{1,0:T(8,128)(2,1)S(1)}) custom-call(bf16[2,4,128,128]{3,2,1,0:T(8,128)(2,1)S(1)} %pad_maximum_fusion.g0, bf16[2,4,128,128]{3,2,1,0:T(8,128)(2,1)} %collective-permute-done.1.g1, bf16[2,4,128,128]{3,2,1,0:T(8,128)(2,1)S(1)} %collective-permute-done.2.g2, ...), custom_call_target="tpu_custom_call" | custom-call | flops 2147483648 | bytes 12000000 | tf_op jit(solution)/shard_map/pallas_call | solution.py:309
  108.2 5.1 %shard_map.114.acc_ref = f32[512,2048]{1,0:T(8,128)S(1)} custom-call(bf16[512,1536]{1,0:T(8,128)(2,1)S(1)} %get-tuple-element.33.x_ref, bf16[4,128,1024]{2,1,0:T(8,128)(2,1)S(1)} %shard_map.113.refs_0_, bf16[4,128,1024]{2,1,0:T(8,128)(2,1)S(1)} %collective-permute-done.10.refs_1_, bf16[4,128,1024]{2,1,0:T(8,128)(2,1)S(1)} %collective-permute-done.11.refs_2_, ...), custom_call_target="tpu_custom_call" | custom-call | flops 3221225472 | bytes 10000000 | tf_op jit(solution)/shard_map/pallas_call | solution.py:309
  113.4 3.2 %shard_map.116 = (bf16[512,2048]{1,0:T(8,128)(2,1)S(1)}, bf16[128,512]{1,0:T(8,128)(2,1)S(1)}, bf16[128,512]{1,0:T(8,128)(2,1)S(1)}, bf16[128,512]{1,0:T(8,128)(2,1)S(1)}, bf16[128,512]{1,0:T(8,128)(2,1)S(1)}) custom-call(bf16[512,512]{1,0:T(8,128)(2,1)S(1)} %get-tuple-element.32.x_ref, f32[512,2048]{1,0:T(8,128)S(1)} %shard_map.114.acc_ref, ...), custom_call_target="tpu_custom_call" | custom-call | flops 2147483648 | bytes 8000000 | tf_op jit(solution)/shard_map/pallas_call | solution.py:309
  116.6 2.7 %collective-permute-start.21 = (bf16[128,512]{1,0:T(8,128)(2,1)S(1)}, bf16[128,512]{1,0:T(8,128)(2,1)S(1)}, u32[]{:S(2)}, u32[]{:S(2)}) collective-permute-start(bf16[128,512]{1,0:T(8,128)(2,1)S(1)} %get-tuple-element.35), channel_id=1, source_target_pairs={{0,6},{2,0},{4,2},{6,4},{1,7},{3,1},{5,3},{7,5},{8,14},{10,8},{12,... | collective-permute-start | bytes 393224 | tf_op jit(solution)/shard_map/ppermute | solution.py:321
  119.4 1.3 collective-permute-start.23
  120.6 3.9 %shard_map.117 = (bf16[128,1024]{1,0:T(8,128)(2,1)S(1)}, bf16[128,1024]{1,0:T(8,128)(2,1)S(1)}, bf16[128,1024]{1,0:T(8,128)(2,1)S(1)}, bf16[128,1024]{1,0:T(8,128)(2,1)S(1)}) custom-call(bf16[512,2048]{1,0:T(8,128)(2,1)S(1)} %get-tuple-element.38.hid_ref, bf16[4,1024,128]{2,1,0:T(8,128)(2,1)S(1)} %collective-permute-done.24.refs_0_, ...), custom_call_target="tpu_custom_call" | custom-call | flops 2147483648 | bytes 6000000 | tf_op jit(solution)/shard_map/pallas_call | solution.py:309
  124.5 1.7 %collective-permute-start.28 = (bf16[128,1024]{1,0:T(8,128)(2,1)S(1)}, bf16[128,1024]{1,0:T(8,128)(2,1)S(1)}, u32[]{:S(2)}, u32[]{:S(2)}) collective-permute-start(bf16[128,1024]{1,0:T(8,128)(2,1)S(1)} %get-tuple-element.40), channel_id=1, source_target_pairs={{0,6},{2,0},{4,2},{6,4},{1,7},{3,1},{5,3},{7,5},{8,14},{10,8},{12,... | collective-permute-start | bytes 786440 | tf_op jit(solution)/shard_map/ppermute | solution.py:321
  126.2 1.7 %shard_map.118 = (bf16[128,512]{1,0:T(8,128)(2,1)S(1)}, bf16[128,512]{1,0:T(8,128)(2,1)S(1)}, bf16[128,512]{1,0:T(8,128)(2,1)S(1)}, bf16[128,512]{1,0:T(8,128)(2,1)S(1)}) custom-call(bf16[512,2048]{1,0:T(8,128)(2,1)S(1)} %get-tuple-element.38.hid_ref, bf16[4,1024,128]{2,1,0:T(8,128)(2,1)S(1)} %collective-permute-done.31.refs_0_, ...), custom_call_target="tpu_custom_call" | custom-call | flops 1073741824 | bytes 3000000 | tf_op jit(solution)/shard_map/pallas_call | solution.py:309
  127.9 0.6 collective-permute-start.33
  128.6 0.9 collective-permute-start.29
  129.5 2.4 %collective-permute-start.30 = (bf16[128,1024]{1,0:T(8,128)(2,1)S(1)}, bf16[128,1024]{1,0:T(8,128)(2,1)S(1)}, u32[]{:S(2)}, u32[]{:S(2)}) collective-permute-start(bf16[128,1024]{1,0:T(8,128)(2,1)S(1)} %get-tuple-element.42), channel_id=1, source_target_pairs={{0,4},{2,6},{4,0},{6,2},{1,5},{3,7},{5,1},{7,3},{8,12},{10,14},{12... | collective-permute-start | bytes 786440 | tf_op jit(solution)/shard_map/ppermute | solution.py:321
  131.8 3.3 %collective-permute-done.33.refs_9_ = bf16[128,512]{1,0:T(8,128)(2,1)S(1)} collective-permute-done((bf16[128,512]{1,0:T(8,128)(2,1)S(1)}, bf16[128,512]{1,0:T(8,128)(2,1)S(1)}, u32[]{:S(2)}, u32[]{:S(2)}) %collective-permute-start.33) | collective-permute-done | bytes 131104 | tf_op jit(solution)/shard_map/ppermute | solution.py:321
  135.2 1.2 collective-permute-start.35
  136.4 6.5 %collective-permute-done.34.refs_10_ = bf16[128,512]{1,0:T(8,128)(2,1)S(1)} collective-permute-done((bf16[128,512]{1,0:T(8,128)(2,1)S(1)}, bf16[128,512]{1,0:T(8,128)(2,1)S(1)}, u32[]{:S(2)}, u32[]{:S(2)}) %collective-permute-start.34) | collective-permute-done | bytes 131104 | tf_op jit(solution)/shard_map/ppermute | solution.py:321
  142.9 4.6 %collective-permute-done.35.refs_11_ = bf16[128,512]{1,0:T(8,128)(2,1)S(1)} collective-permute-done((bf16[128,512]{1,0:T(8,128)(2,1)S(1)}, bf16[128,512]{1,0:T(8,128)(2,1)S(1)}, u32[]{:S(2)}, u32[]{:S(2)}) %collective-permute-start.35) | collective-permute-done | bytes 131104 | tf_op jit(solution)/shard_map/ppermute | solution.py:321
  147.6 1.3 shard_map.119
  (60 shorter events, 3.6 us)
Async XLA Ops:
  0.0 16.0 %copy-start.8 = (bf16[1024,128]{1,0:T(8,128)(2,1)S(1)}, bf16[1024,128]{1,0:T(8,128)(2,1)}, u32[]{:S(2)}) copy-start(bf16[1024,128]{1,0:T(8,128)(2,1)} %refs_0_.3) | copy-start | bytes 786436
  0.0 18.7 %copy-start.2 = (bf16[128,2048]{1,0:T(8,128)(2,1)S(1)}, bf16[128,2048]{1,0:T(8,128)(2,1)}, u32[]{:S(2)}) copy-start(bf16[128,2048]{1,0:T(8,128)(2,1)} %s0.1) | copy-start | bytes 1572868
  0.0 19.9 %collective-permute-start.7 = (bf16[128,1024]{1,0:T(8,128)(2,1)}, bf16[128,1024]{1,0:T(8,128)(2,1)S(1)}, u32[]{:S(2)}, u32[]{:S(2)}) collective-permute-start(bf16[128,1024]{1,0:T(8,128)(2,1)} %refs_0_.2), channel_id=1, source_target_pairs={{0,8},{1,25},{8,16},{9,1},{16,24},{17,9},{24,0},{25,17},{2,10},{3,... | collective-permute-start | bytes 786440 | tf_op jit(solution)/shard_map/ppermute | solution.py:330
  3.6 17.8 %collective-permute-start.8 = (bf16[128,1024]{1,0:T(8,128)(2,1)}, bf16[128,1024]{1,0:T(8,128)(2,1)S(1)}, u32[]{:S(2)}, u32[]{:S(2)}) collective-permute-start(bf16[128,1024]{1,0:T(8,128)(2,1)} %refs_0_.2), channel_id=1, source_target_pairs={{0,24},{1,9},{8,0},{9,17},{16,8},{17,25},{24,16},{25,1},{2,26},{3,... | collective-permute-start | bytes 786440 | tf_op jit(solution)/shard_map/ppermute | solution.py:330
  3.6 30.5 %copy-start.5 = (bf16[128,1024]{1,0:T(8,128)(2,1)S(1)}, bf16[128,1024]{1,0:T(8,128)(2,1)}, u32[]{:S(2)}) copy-start(bf16[128,1024]{1,0:T(8,128)(2,1)} %refs_0_.2) | copy-start | bytes 786436
  8.5 16.5 %all-to-all-start = ((bf16[16,80,128]{2,1,0:T(8,128)(2,1)}), bf16[16,80,128]{2,1,0:T(8,128)(2,1)S(1)}, u32[]{:S(2)}, u32[]{:S(2)}) async-start(bf16[16,80,128]{2,1,0:T(8,128)(2,1)} %get-tuple-element.26), calls=%async_computation | async-start | bytes 655360 | tf_op jit(solution)/shard_map/all_to_all | solution.py:381
  16.0 13.1 %collective-permute-start.17 = (bf16[1024,128]{1,0:T(8,128)(2,1)S(1)}, bf16[1024,128]{1,0:T(8,128)(2,1)}, u32[]{:S(2)}, u32[]{:S(2)}) collective-permute-start(bf16[1024,128]{1,0:T(8,128)(2,1)S(1)} %copy-done.8), channel_id=1, source_target_pairs={{0,32},{1,97},{32,64},{33,1},{64,96},{65,33},{96,0},{97,65},{2,34}... | collective-permute-start | bytes 786440 | tf_op jit(solution)/shard_map/ppermute | solution.py:330
  18.7 11.9 %collective-permute-start.18 = (bf16[1024,128]{1,0:T(8,128)(2,1)S(1)}, bf16[1024,128]{1,0:T(8,128)(2,1)S(1)}, u32[]{:S(2)}, u32[]{:S(2)}) collective-permute-start(bf16[1024,128]{1,0:T(8,128)(2,1)S(1)} %copy-done.8), channel_id=1, source_target_pairs={{0,96},{1,33},{32,0},{33,65},{64,32},{65,97},{96,64},{97,1},{2,98}... | collective-permute-start | bytes 786440 | tf_op jit(solution)/shard_map/ppermute | solution.py:330
  18.7 15.8 %collective-permute-start.4 = (bf16[128,2048]{1,0:T(8,128)(2,1)S(1)}, bf16[128,2048]{1,0:T(8,128)(2,1)S(1)}, u32[]{:S(2)}, u32[]{:S(2)}) collective-permute-start(bf16[128,2048]{1,0:T(8,128)(2,1)S(1)} %copy-done.2), channel_id=1, source_target_pairs={{0,2},{2,4},{4,6},{6,0},{1,3},{3,5},{5,7},{7,1},{8,10},{10,12},{12... | collective-permute-start | bytes 1572872 | tf_op jit(solution)/shard_map/ppermute | solution.py:321
  19.9 15.8 %collective-permute-start.5 = (bf16[128,2048]{1,0:T(8,128)(2,1)S(1)}, bf16[128,2048]{1,0:T(8,128)(2,1)}, u32[]{:S(2)}, u32[]{:S(2)}) collective-permute-start(bf16[128,2048]{1,0:T(8,128)(2,1)S(1)} %copy-done.2), channel_id=1, source_target_pairs={{0,6},{2,0},{4,2},{6,4},{1,7},{3,1},{5,3},{7,5},{8,14},{10,8},{12,... | collective-permute-start | bytes 1572872 | tf_op jit(solution)/shard_map/ppermute | solution.py:321
  21.4 12.0 %collective-permute-start.9 = (bf16[128,1024]{1,0:T(8,128)(2,1)S(1)}, bf16[128,1024]{1,0:T(8,128)(2,1)S(1)}, u32[]{:S(2)}, u32[]{:S(2)}) collective-permute-start(bf16[128,1024]{1,0:T(8,128)(2,1)S(1)} %collective-permute-done.7.refs_1_), channel_id=1, source_target_pairs={{0,8},{1,25},{8,16},{9,1},{16,24},{17,9},{24,0},{25,17},{2,10},{3,... | collective-permute-start | bytes 786440 | tf_op jit(solution)/shard_map/ppermute | solution.py:330
  25.0 0.7 copy-start.7
  29.2 5.0 %collective-permute-start = (bf16[4,128,128]{2,1,0:T(8,128)(2,1)}, bf16[4,128,128]{2,1,0:T(8,128)(2,1)S(1)}, u32[]{:S(2)}, u32[]{:S(2)}) collective-permute-start(bf16[4,128,128]{2,1,0:T(8,128)(2,1)} %get-tuple-element.30), channel_id=1, source_target_pairs={{0,1},{1,0},{2,3},{3,2},{4,5},{5,4},{6,7},{7,6},{8,9},{9,8},{10,11... | collective-permute-start | bytes 393224 | tf_op jit(solution)/shard_map/ppermute | solution.py:325
  30.6 3.9 %copy-start.9 = (bf16[1024,128]{1,0:T(8,128)(2,1)}, bf16[1024,128]{1,0:T(8,128)(2,1)S(1)}, u32[]{:S(2)}) copy-start(bf16[1024,128]{1,0:T(8,128)(2,1)S(1)} %collective-permute-done.18.refs_2_) | copy-start | bytes 786436
  30.6 15.0 %collective-permute-start.6 = (bf16[128,2048]{1,0:T(8,128)(2,1)S(1)}, bf16[128,2048]{1,0:T(8,128)(2,1)}, u32[]{:S(2)}, u32[]{:S(2)}) collective-permute-start(bf16[128,2048]{1,0:T(8,128)(2,1)S(1)} %copy-done.2), channel_id=1, source_target_pairs={{0,4},{2,6},{4,0},{6,2},{1,5},{3,7},{5,1},{7,3},{8,12},{10,14},{12... | collective-permute-start | bytes 1572872 | tf_op jit(solution)/shard_map/ppermute | solution.py:321
  33.3 5.9 %collective-permute-start.19 = (bf16[1024,128]{1,0:T(8,128)(2,1)}, bf16[1024,128]{1,0:T(8,128)(2,1)S(1)}, u32[]{:S(2)}, u32[]{:S(2)}) collective-permute-start(bf16[1024,128]{1,0:T(8,128)(2,1)} %collective-permute-done.17.refs_1_), channel_id=1, source_target_pairs={{0,32},{1,97},{32,64},{33,1},{64,96},{65,33},{96,0},{97,65},{2,34}... | collective-permute-start | bytes 786440 | tf_op jit(solution)/shard_map/ppermute | solution.py:330
  34.2 30.1 %collective-permute-start.11 = (bf16[4,128,1024]{2,1,0:T(8,128)(2,1)S(1)}, bf16[4,128,1024]{2,1,0:T(8,128)(2,1)S(1)}, u32[]{:S(2)}, u32[]{:S(2)}) collective-permute-start(bf16[4,128,1024]{2,1,0:T(8,128)(2,1)S(1)} %shard_map.113.refs_0_), channel_id=1, source_target_pairs={{0,32},{1,97},{32,64},{33,1},{64,96},{65,33},{96,0},{97,65},{2,34}... | collective-permute-start | bytes 3145736 | tf_op jit(solution)/shard_map/ppermute | solution.py:330
  34.5 0.8 copy-start.3
  35.3 40.6 %collective-permute-start.10 = (bf16[4,128,1024]{2,1,0:T(8,128)(2,1)S(1)}, bf16[4,128,1024]{2,1,0:T(8,128)(2,1)S(1)}, u32[]{:S(2)}, u32[]{:S(2)}) collective-permute-start(bf16[4,128,1024]{2,1,0:T(8,128)(2,1)S(1)} %shard_map.113.refs_0_), channel_id=1, source_target_pairs={{0,1},{1,0},{2,3},{3,2},{4,5},{5,4},{6,7},{7,6},{8,9},{9,8},{10,11... | collective-permute-start | bytes 3145736 | tf_op jit(solution)/shard_map/ppermute | solution.py:325
  35.6 29.8 %collective-permute-start.12 = (bf16[4,128,1024]{2,1,0:T(8,128)(2,1)S(1)}, bf16[4,128,1024]{2,1,0:T(8,128)(2,1)}, u32[]{:S(2)}, u32[]{:S(2)}) collective-permute-start(bf16[4,128,1024]{2,1,0:T(8,128)(2,1)S(1)} %shard_map.113.refs_0_), channel_id=1, source_target_pairs={{0,96},{1,33},{32,0},{33,65},{64,32},{65,97},{96,64},{97,1},{2,98}... | collective-permute-start | bytes 3145736 | tf_op jit(solution)/shard_map/ppermute | solution.py:330
  39.3 0.7 copy-start.10
  40.0 8.9 %collective-permute-start.1 = (bf16[2,4,128,128]{3,2,1,0:T(8,128)(2,1)S(1)}, bf16[2,4,128,128]{3,2,1,0:T(8,128)(2,1)}, u32[]{:S(2)}, u32[]{:S(2)}) collective-permute-start(bf16[2,4,128,128]{3,2,1,0:T(8,128)(2,1)S(1)} %pad_maximum_fusion.g0), channel_id=1, source_target_pairs={{0,2},{2,4},{4,6},{6,0},{1,3},{3,5},{5,7},{7,1},{8,10},{10,12},{12... | collective-permute-start | bytes 786440 | tf_op jit(solution)/shard_map/ppermute | solution.py:321
  40.3 62.5 %copy-start.6 = (f32[2048]{0:T(1024)S(1)}, f32[2048]{0:T(1024)}, u32[]{:S(2)}) copy-start(f32[2048]{0:T(1024)} %param.19) | copy-start | bytes 24580
  45.6 30.4 %collective-permute-start.24 = (bf16[4,1024,128]{2,1,0:T(8,128)(2,1)}, bf16[4,1024,128]{2,1,0:T(8,128)(2,1)S(1)}, u32[]{:S(2)}, u32[]{:S(2)}) collective-permute-start(bf16[4,1024,128]{2,1,0:T(8,128)(2,1)} %shard_map.115.d0), channel_id=1, source_target_pairs={{0,8},{1,25},{8,16},{9,1},{16,24},{17,9},{24,0},{25,17},{2,10},{3,... | collective-permute-start | bytes 3145736 | tf_op jit(solution)/shard_map/ppermute | solution.py:330
  48.9 7.1 %collective-permute-start.2 = (bf16[2,4,128,128]{3,2,1,0:T(8,128)(2,1)S(1)}, bf16[2,4,128,128]{3,2,1,0:T(8,128)(2,1)S(1)}, u32[]{:S(2)}, u32[]{:S(2)}) collective-permute-start(bf16[2,4,128,128]{3,2,1,0:T(8,128)(2,1)S(1)} %pad_maximum_fusion.g0), channel_id=1, source_target_pairs={{0,6},{2,0},{4,2},{6,4},{1,7},{3,1},{5,3},{7,5},{8,14},{10,8},{12,... | collective-permute-start | bytes 786440 | tf_op jit(solution)/shard_map/ppermute | solution.py:321
  55.9 7.8 %collective-permute-start.3 = (bf16[2,4,128,128]{3,2,1,0:T(8,128)(2,1)S(1)}, bf16[2,4,128,128]{3,2,1,0:T(8,128)(2,1)S(1)}, u32[]{:S(2)}, u32[]{:S(2)}) collective-permute-start(bf16[2,4,128,128]{3,2,1,0:T(8,128)(2,1)S(1)} %pad_maximum_fusion.g0), channel_id=1, source_target_pairs={{0,4},{2,6},{4,0},{6,2},{1,5},{3,7},{5,1},{7,3},{8,12},{10,14},{12... | collective-permute-start | bytes 786440 | tf_op jit(solution)/shard_map/ppermute | solution.py:321
  63.8 15.1 %collective-permute-start.25 = (bf16[4,1024,128]{2,1,0:T(8,128)(2,1)}, bf16[4,1024,128]{2,1,0:T(8,128)(2,1)S(1)}, u32[]{:S(2)}, u32[]{:S(2)}) collective-permute-start(bf16[4,1024,128]{2,1,0:T(8,128)(2,1)} %shard_map.115.d0), channel_id=1, source_target_pairs={{0,24},{1,9},{8,0},{9,17},{16,8},{17,25},{24,16},{25,1},{2,26},{3,... | collective-permute-start | bytes 3145736 | tf_op jit(solution)/shard_map/ppermute | solution.py:330
  64.3 35.1 %collective-permute-start.15 = (bf16[4,128,1024]{2,1,0:T(8,128)(2,1)S(1)}, bf16[4,128,1024]{2,1,0:T(8,128)(2,1)S(1)}, u32[]{:S(2)}, u32[]{:S(2)}) collective-permute-start(bf16[4,128,1024]{2,1,0:T(8,128)(2,1)S(1)} %collective-permute-done.11.refs_2_), channel_id=1, source_target_pairs={{0,32},{1,97},{32,64},{33,1},{64,96},{65,33},{96,0},{97,65},{2,34}... | collective-permute-start | bytes 3145736 | tf_op jit(solution)/shard_map/ppermute | solution.py:330
  65.5 33.8 %collective-permute-start.13 = (bf16[4,128,1024]{2,1,0:T(8,128)(2,1)}, bf16[4,128,1024]{2,1,0:T(8,128)(2,1)S(1)}, u32[]{:S(2)}, u32[]{:S(2)}) collective-permute-start(bf16[4,128,1024]{2,1,0:T(8,128)(2,1)} %collective-permute-done.12.refs_4_), channel_id=1, source_target_pairs={{0,1},{1,0},{2,3},{3,2},{4,5},{5,4},{6,7},{7,6},{8,9},{9,8},{10,11... | collective-permute-start | bytes 3145736 | tf_op jit(solution)/shard_map/ppermute | solution.py:325
  75.9 24.0 %collective-permute-start.14 = (bf16[4,128,1024]{2,1,0:T(8,128)(2,1)S(1)}, bf16[4,128,1024]{2,1,0:T(8,128)(2,1)S(1)}, u32[]{:S(2)}, u32[]{:S(2)}) collective-permute-start(bf16[4,128,1024]{2,1,0:T(8,128)(2,1)S(1)} %collective-permute-done.11.refs_2_), channel_id=1, source_target_pairs={{0,1},{1,0},{2,3},{3,2},{4,5},{5,4},{6,7},{7,6},{8,9},{9,8},{10,11... | collective-permute-start | bytes 3145736 | tf_op jit(solution)/shard_map/ppermute | solution.py:325
  76.0 24.0 %collective-permute-start.31 = (bf16[4,1024,128]{2,1,0:T(8,128)(2,1)S(1)}, bf16[4,1024,128]{2,1,0:T(8,128)(2,1)S(1)}, u32[]{:S(2)}, u32[]{:S(2)}) collective-permute-start(bf16[4,1024,128]{2,1,0:T(8,128)(2,1)S(1)} %collective-permute-done.24.refs_0_), channel_id=1, source_target_pairs={{0,8},{1,25},{8,16},{9,1},{16,24},{17,9},{24,0},{25,17},{2,10},{3,... | collective-permute-start | bytes 3145736 | tf_op jit(solution)/shard_map/ppermute | solution.py:330
  78.9 34.5 %collective-permute-start.20 = (bf16[4,1024,128]{2,1,0:T(8,128)(2,1)}, bf16[4,1024,128]{2,1,0:T(8,128)(2,1)S(1)}, u32[]{:S(2)}, u32[]{:S(2)}) collective-permute-start(bf16[4,1024,128]{2,1,0:T(8,128)(2,1)} %shard_map.115.d0), channel_id=1, source_target_pairs={{0,1},{1,0},{2,3},{3,2},{4,5},{5,4},{6,7},{7,6},{8,9},{9,8},{10,11... | collective-permute-start | bytes 3145736 | tf_op jit(solution)/shard_map/ppermute | solution.py:325
  99.3 14.1 %collective-permute-start.16 = (bf16[4,128,1024]{2,1,0:T(8,128)(2,1)S(1)}, bf16[4,128,1024]{2,1,0:T(8,128)(2,1)S(1)}, u32[]{:S(2)}, u32[]{:S(2)}) collective-permute-start(bf16[4,128,1024]{2,1,0:T(8,128)(2,1)S(1)} %collective-permute-done.15.u0), channel_id=1, source_target_pairs={{0,1},{1,0},{2,3},{3,2},{4,5},{5,4},{6,7},{7,6},{8,9},{9,8},{10,11... | collective-permute-start | bytes 3145736 | tf_op jit(solution)/shard_map/ppermute | solution.py:325
  99.3 20.0 %collective-permute-start.26 = (bf16[4,1024,128]{2,1,0:T(8,128)(2,1)S(1)}, bf16[4,1024,128]{2,1,0:T(8,128)(2,1)S(1)}, u32[]{:S(2)}, u32[]{:S(2)}) collective-permute-start(bf16[4,1024,128]{2,1,0:T(8,128)(2,1)S(1)} %collective-permute-done.25.refs_2_), channel_id=1, source_target_pairs={{0,1},{1,0},{2,3},{3,2},{4,5},{5,4},{6,7},{7,6},{8,9},{9,8},{10,11... | collective-permute-start | bytes 3145736 | tf_op jit(solution)/shard_map/ppermute | solution.py:325
  99.8 20.8 %collective-permute-start.27 = (bf16[4,1024,128]{2,1,0:T(8,128)(2,1)S(1)}, bf16[4,1024,128]{2,1,0:T(8,128)(2,1)S(1)}, u32[]{:S(2)}, u32[]{:S(2)}) collective-permute-start(bf16[4,1024,128]{2,1,0:T(8,128)(2,1)S(1)} %collective-permute-done.24.refs_0_), channel_id=1, source_target_pairs={{0,1},{1,0},{2,3},{3,2},{4,5},{5,4},{6,7},{7,6},{8,9},{9,8},{10,11... | collective-permute-start | bytes 3145736 | tf_op jit(solution)/shard_map/ppermute | solution.py:325
  99.9 26.3 %collective-permute-start.32 = (bf16[4,1024,128]{2,1,0:T(8,128)(2,1)S(1)}, bf16[4,1024,128]{2,1,0:T(8,128)(2,1)S(1)}, u32[]{:S(2)}, u32[]{:S(2)}) collective-permute-start(bf16[4,1024,128]{2,1,0:T(8,128)(2,1)S(1)} %collective-permute-done.31.refs_0_), channel_id=1, source_target_pairs={{0,1},{1,0},{2,3},{3,2},{4,5},{5,4},{6,7},{7,6},{8,9},{9,8},{10,11... | collective-permute-start | bytes 3145736 | tf_op jit(solution)/shard_map/ppermute | solution.py:325
  100.4 2.2 %copy-start = (bf16[1024,2048]{1,0:T(8,128)(2,1)S(1)}, bf16[1024,2048]{1,0:T(8,128)(2,1)}, u32[]{:S(2)}) copy-start(bf16[1024,2048]{1,0:T(8,128)(2,1)} %w_ref.1) | copy-start | bytes 12582916
  102.5 1.0 copy-start.4
  108.2 5.2 %copy-start.1 = (bf16[4,1024,128]{2,1,0:T(8,128)(2,1)S(1)}, bf16[4,1024,128]{2,1,0:T(8,128)(2,1)}, u32[]{:S(2)}) copy-start(bf16[4,1024,128]{2,1,0:T(8,128)(2,1)} %shard_map.115.d0) | copy-start | bytes 3145732
  116.6 12.0 %collective-permute-start.21 = (bf16[128,512]{1,0:T(8,128)(2,1)S(1)}, bf16[128,512]{1,0:T(8,128)(2,1)S(1)}, u32[]{:S(2)}, u32[]{:S(2)}) collective-permute-start(bf16[128,512]{1,0:T(8,128)(2,1)S(1)} %get-tuple-element.35), channel_id=1, source_target_pairs={{0,6},{2,0},{4,2},{6,4},{1,7},{3,1},{5,3},{7,5},{8,14},{10,8},{12,... | collective-permute-start | bytes 393224 | tf_op jit(solution)/shard_map/ppermute | solution.py:321
  119.4 10.1 %collective-permute-start.22 = (bf16[128,512]{1,0:T(8,128)(2,1)S(1)}, bf16[128,512]{1,0:T(8,128)(2,1)S(1)}, u32[]{:S(2)}, u32[]{:S(2)}) collective-permute-start(bf16[128,512]{1,0:T(8,128)(2,1)S(1)} %get-tuple-element.36), channel_id=1, source_target_pairs={{0,2},{2,4},{4,6},{6,0},{1,3},{3,5},{5,7},{7,1},{8,10},{10,12},{12... | collective-permute-start | bytes 393224 | tf_op jit(solution)/shard_map/ppermute | solution.py:321
  119.4 12.5 %collective-permute-start.23 = (bf16[128,512]{1,0:T(8,128)(2,1)S(1)}, bf16[128,512]{1,0:T(8,128)(2,1)S(1)}, u32[]{:S(2)}, u32[]{:S(2)}) collective-permute-start(bf16[128,512]{1,0:T(8,128)(2,1)S(1)} %get-tuple-element.37), channel_id=1, source_target_pairs={{0,4},{2,6},{4,0},{6,2},{1,5},{3,7},{5,1},{7,3},{8,12},{10,14},{12... | collective-permute-start | bytes 393224 | tf_op jit(solution)/shard_map/ppermute | solution.py:321
  124.5 23.0 %collective-permute-start.28 = (bf16[128,1024]{1,0:T(8,128)(2,1)S(1)}, bf16[128,1024]{1,0:T(8,128)(2,1)S(1)}, u32[]{:S(2)}, u32[]{:S(2)}) collective-permute-start(bf16[128,1024]{1,0:T(8,128)(2,1)S(1)} %get-tuple-element.40), channel_id=1, source_target_pairs={{0,6},{2,0},{4,2},{6,4},{1,7},{3,1},{5,3},{7,5},{8,14},{10,8},{12,... | collective-permute-start | bytes 786440 | tf_op jit(solution)/shard_map/ppermute | solution.py:321
  127.9 7.2 %collective-permute-start.33 = (bf16[128,512]{1,0:T(8,128)(2,1)S(1)}, bf16[128,512]{1,0:T(8,128)(2,1)S(1)}, u32[]{:S(2)}, u32[]{:S(2)}) collective-permute-start(bf16[128,512]{1,0:T(8,128)(2,1)S(1)} %get-tuple-element.44), channel_id=1, source_target_pairs={{0,6},{2,0},{4,2},{6,4},{1,7},{3,1},{5,3},{7,5},{8,14},{10,8},{12,... | collective-permute-start | bytes 393224 | tf_op jit(solution)/shard_map/ppermute | solution.py:321
  128.6 19.0 %collective-permute-start.29 = (bf16[128,1024]{1,0:T(8,128)(2,1)S(1)}, bf16[128,1024]{1,0:T(8,128)(2,1)S(1)}, u32[]{:S(2)}, u32[]{:S(2)}) collective-permute-start(bf16[128,1024]{1,0:T(8,128)(2,1)S(1)} %get-tuple-element.41), channel_id=1, source_target_pairs={{0,2},{2,4},{4,6},{6,0},{1,3},{3,5},{5,7},{7,1},{8,10},{10,12},{12... | collective-permute-start | bytes 786440 | tf_op jit(solution)/shard_map/ppermute | solution.py:321
  129.5 18.1 %collective-permute-start.30 = (bf16[128,1024]{1,0:T(8,128)(2,1)S(1)}, bf16[128,1024]{1,0:T(8,128)(2,1)S(1)}, u32[]{:S(2)}, u32[]{:S(2)}) collective-permute-start(bf16[128,1024]{1,0:T(8,128)(2,1)S(1)} %get-tuple-element.42), channel_id=1, source_target_pairs={{0,4},{2,6},{4,0},{6,2},{1,5},{3,7},{5,1},{7,3},{8,12},{10,14},{12... | collective-permute-start | bytes 786440 | tf_op jit(solution)/shard_map/ppermute | solution.py:321
  131.8 11.1 %collective-permute-start.34 = (bf16[128,512]{1,0:T(8,128)(2,1)S(1)}, bf16[128,512]{1,0:T(8,128)(2,1)S(1)}, u32[]{:S(2)}, u32[]{:S(2)}) collective-permute-start(bf16[128,512]{1,0:T(8,128)(2,1)S(1)} %get-tuple-element.45), channel_id=1, source_target_pairs={{0,2},{2,4},{4,6},{6,0},{1,3},{3,5},{5,7},{7,1},{8,10},{10,12},{12... | collective-permute-start | bytes 393224 | tf_op jit(solution)/shard_map/ppermute | solution.py:321
  135.2 12.4 %collective-permute-start.35 = (bf16[128,512]{1,0:T(8,128)(2,1)S(1)}, bf16[128,512]{1,0:T(8,128)(2,1)S(1)}, u32[]{:S(2)}, u32[]{:S(2)}) collective-permute-start(bf16[128,512]{1,0:T(8,128)(2,1)S(1)} %get-tuple-element.46), channel_id=1, source_target_pairs={{0,4},{2,6},{4,0},{6,2},{1,5},{3,7},{5,1},{7,3},{8,12},{10,14},{12... | collective-permute-start | bytes 393224 | tf_op jit(solution)/shard_map/ppermute | solution.py:321

commit v2 on v1

--- a/solution.py
+++ b/solution.py
@@ -17,7 +17,7 @@
 SP = ("z", "y")
 TP = ("x", "c")
 PEERS = 16
-FOLD = 80
+FOLD = 72
 
 gate_temper = 16.0
 norm_eps = 1e-06
@@ -123,11 +123,11 @@
     bwd = jnp.zeros((half, 2 * HEAD_K), f32)
     for peer in range(PEERS):
         state = got_ref[peer, :half].astype(f32)
-        decay = got_ref[peer, half : half + 16].astype(f32)[:1]
+        decay = got_ref[peer, half : half + 8].astype(f32)[:1]
         fwd = jnp.where(peer < me, fwd * decay + state, fwd)
     for peer in reversed(range(PEERS)):
         state = got_ref[peer, :half].astype(f32)
-        decay = got_ref[peer, half : half + 16].astype(f32)[:1]
+        decay = got_ref[peer, half : half + 8].astype(f32)[:1]
         bwd = jnp.where(peer > me, bwd * decay + state, bwd)
     top = jnp.concatenate([fwd[:, :HEAD_K], bwd[:, :HEAD_K]], axis=1)
     low = jnp.concatenate([fwd[:, HEAD_K:], bwd[:, HEAD_K:]], axis=1)

time: 151 us -> 151 us (level)
  no operation moved by 1% of the time
where the time goes in v2:
time: 151 us; the launch traced here: 149 us
  starting transfers between devices  77.4 us (51%)
  waiting for transfers between devices  34.2 us (23%)
  Pallas kernels  30.6 us (20%)
  local copies, waits for them, and re-layouts  5.18 us (3%)
    ppermute x9, starting transfers between devices, swapped(): return lax.ppermute(v, 'c', [(0, 1), (1, 0)])  33.4 us
    pallas_call x11, Pallas kernels, launched(): pl.pallas_call(kernel, in_specs=ins, out_specs=[spec] * len(outs), out_sh...  30.6 us
    ppermute x15, waiting for transfers between devices, shifted(): return lax.ppermute(v, axis, [(i, (i + by) % n) for i in range(n)])  29.4 us
    ppermute x15, starting transfers between devices, shifted(): return lax.ppermute(v, axis, [(i, (i + by) % n) for i in range(n)])  21.4 us
    ppermute x12, starting transfers between devices, both_ways(): return lax.ppermute(v, (axis, 'c'), pairs)  15.1 us
    all_to_all x1, starting transfers between devices, local(): got = lax.all_to_all(sent, SP, 0, 0, tiled=True)  7.53 us
    unnamed x22, local copies, waits for them, and re-layouts  5.18 us
    ppermute x12, waiting for transfers between devices, both_ways(): return lax.ppermute(v, (axis, 'c'), pairs)  3.91 us
  transfers between devices with their start and end apart: 37, of which 10 were waited for; matrix products, arithmetic and copies ran while one was open for 1% of the time, Pallas kernels for 20%

profile of v2, /device:TPU:1, one launch (start us, length us, event | category | flops | bytes accessed | tf_op | source)
XLA Modules:
  0.0 148.6 jit_solution(7160125242632868499)
XLA Ops:
  0.0 3.6 %collective-permute-start.7 = (bf16[128,1024]{1,0:T(8,128)(2,1)}, bf16[128,1024]{1,0:T(8,128)(2,1)S(1)}, u32[]{:S(2)}, u32[]{:S(2)}) collective-permute-start(bf16[128,1024]{1,0:T(8,128)(2,1)} %refs_0_.2), channel_id=1, source_target_pairs={{0,8},{1,25},{8,16},{9,1},{16,24},{17,9},{24,0},{25,17},{2,10},{3,... | collective-permute-start | bytes 786440 | tf_op jit(solution)/shard_map/ppermute | solution.py:330
  3.6 4.9 %shard_map.109 = (f32[1024,128]{1,0:T(8,128)}, bf16[1024,128]{1,0:T(8,128)(2,1)}, bf16[16,72,128]{2,1,0:T(8,128)(2,1)}) custom-call(bf16[64,1024]{1,0:T(8,128)(2,1)} %bitcast.11, bf16[64,1024]{1,0:T(8,128)(2,1)} %bitcast.12, bf16[1024,128]{1,0:T(8,128)(2,1)} %v_ref.1, f32[2,64,1024]{2,1,0:T(8,128)} %bitcast.10), custom_call_target="tpu_custom_call" | custom-call | flops 2000000000 | bytes 2000000 | tf_op jit(solution)/shard_map/pallas_call | solution.py:309
  8.5 7.5 %all-to-all-start = ((bf16[16,72,128]{2,1,0:T(8,128)(2,1)}), bf16[16,72,128]{2,1,0:T(8,128)(2,1)S(1)}, u32[]{:S(2)}, u32[]{:S(2)}) async-start(bf16[16,72,128]{2,1,0:T(8,128)(2,1)} %get-tuple-element.26), calls=%async_computation | async-start | bytes 589824 | tf_op jit(solution)/shard_map/all_to_all | solution.py:381
  16.0 2.6 %collective-permute-start.17 = (bf16[1024,128]{1,0:T(8,128)(2,1)S(1)}, bf16[1024,128]{1,0:T(8,128)(2,1)}, u32[]{:S(2)}, u32[]{:S(2)}) collective-permute-start(bf16[1024,128]{1,0:T(8,128)(2,1)S(1)} %copy-done.8), channel_id=1, source_target_pairs={{0,32},{1,97},{32,64},{33,1},{64,96},{65,33},{96,0},{97,65},{2,34}... | collective-permute-start | bytes 786440 | tf_op jit(solution)/shard_map/ppermute | solution.py:330
  18.7 1.2 collective-permute-start.4
  19.9 1.5 collective-permute-start.5
  21.4 2.4 %collective-permute-start.9 = (bf16[128,1024]{1,0:T(8,128)(2,1)S(1)}, bf16[128,1024]{1,0:T(8,128)(2,1)S(1)}, u32[]{:S(2)}, u32[]{:S(2)}) collective-permute-start(bf16[128,1024]{1,0:T(8,128)(2,1)S(1)} %collective-permute-done.7.refs_1_), channel_id=1, source_target_pairs={{0,8},{1,25},{8,16},{9,1},{16,24},{17,9},{24,0},{25,17},{2,10},{3,... | collective-permute-start | bytes 786440 | tf_op jit(solution)/shard_map/ppermute | solution.py:330
  23.8 0.9 all-to-all-done.got_ref
  24.7 0.7 copy-done.7
  25.4 3.4 %shard_map.110 = (bf16[4,128,128]{2,1,0:T(8,128)(2,1)}, bf16[4,128,128]{2,1,0:T(8,128)(2,1)}) custom-call(bf16[16,72,128]{2,1,0:T(8,128)(2,1)} %copy-done.7, f32[1024,128]{1,0:T(8,128)} %get-tuple-element.27.local_hbm, bf16[1024,128]{1,0:T(8,128)(2,1)} %get-tuple-element.28.carry_hbm, bf16[1024,128]{1,0:T(8,128)(2,1)} %gate_hbm.1, f32[1,128]{1,0:T(1,128)} %bitcast.13), custom_call_target="tpu_custom_call" | custom-call | flops 1000000000 | bytes 2000000 | tf_op jit(solution)/shard_map/pallas_call | solution.py:309
  28.8 1.4 collective-permute-start
  30.3 2.7 %collective-permute-start.6 = (bf16[128,2048]{1,0:T(8,128)(2,1)S(1)}, bf16[128,2048]{1,0:T(8,128)(2,1)}, u32[]{:S(2)}, u32[]{:S(2)}) collective-permute-start(bf16[128,2048]{1,0:T(8,128)(2,1)S(1)} %copy-done.2), channel_id=1, source_target_pairs={{0,4},{2,6},{4,0},{6,2},{1,5},{3,7},{5,1},{7,3},{8,12},{10,14},{12... | collective-permute-start | bytes 1572872 | tf_op jit(solution)/shard_map/ppermute | solution.py:321
  33.0 0.7 collective-permute-start.19
  34.2 0.8 copy-done.3
  35.3 1.2 collective-permute-start.12
  36.5 0.9 pad_maximum_fusion.g0
  37.4 1.5 %collective-permute-done.19.refs_3_ = bf16[1024,128]{1,0:T(8,128)(2,1)S(1)} collective-permute-done((bf16[1024,128]{1,0:T(8,128)(2,1)}, bf16[1024,128]{1,0:T(8,128)(2,1)S(1)}, u32[]{:S(2)}, u32[]{:S(2)}) %collective-permute-start.19) | collective-permute-done | bytes 262176 | tf_op jit(solution)/shard_map/ppermute | solution.py:330
  38.9 0.7 copy-done.10
  39.9 2.0 %shard_map.115.d0 = bf16[4,1024,128]{2,1,0:T(8,128)(2,1)} custom-call(bf16[1024,128]{1,0:T(8,128)(2,1)} %refs_0_.3, bf16[1024,128]{1,0:T(8,128)(2,1)} %collective-permute-done.17.refs_1_, bf16[1024,128]{1,0:T(8,128)(2,1)} %copy-done.9, bf16[1024,128]{1,0:T(8,128)(2,1)} %copy-done.10), custom_call_target="tpu_custom_call" | custom-call | flops 800000000 | bytes 2000000 | tf_op jit(solution)/shard_map/pallas_call | solution.py:309
  42.0 3.9 %collective-permute-done.6.s3 = bf16[128,2048]{1,0:T(8,128)(2,1)} collective-permute-done((bf16[128,2048]{1,0:T(8,128)(2,1)S(1)}, bf16[128,2048]{1,0:T(8,128)(2,1)}, u32[]{:S(2)}, u32[]{:S(2)}) %collective-permute-start.6) | collective-permute-done | bytes 524320 | tf_op jit(solution)/shard_map/ppermute | solution.py:321
  45.8 1.8 %collective-permute-start.24 = (bf16[4,1024,128]{2,1,0:T(8,128)(2,1)}, bf16[4,1024,128]{2,1,0:T(8,128)(2,1)S(1)}, u32[]{:S(2)}, u32[]{:S(2)}) collective-permute-start(bf16[4,1024,128]{2,1,0:T(8,128)(2,1)} %shard_map.115.d0), channel_id=1, source_target_pairs={{0,8},{1,25},{8,16},{9,1},{16,24},{17,9},{24,0},{25,17},{2,10},{3,... | collective-permute-start | bytes 3145736 | tf_op jit(solution)/shard_map/ppermute | solution.py:330
  47.6 1.3 collective-permute-done.1.g1
  48.9 0.7 collective-permute-start.2
  49.6 6.0 %collective-permute-done.2.g2 = bf16[2,4,128,128]{3,2,1,0:T(8,128)(2,1)S(1)} collective-permute-done((bf16[2,4,128,128]{3,2,1,0:T(8,128)(2,1)S(1)}, bf16[2,4,128,128]{3,2,1,0:T(8,128)(2,1)S(1)}, u32[]{:S(2)}, u32[]{:S(2)}) %collective-permute-start.2) | collective-permute-done | bytes 262176 | tf_op jit(solution)/shard_map/ppermute | solution.py:321
  55.6 4.1 %collective-permute-start.3 = (bf16[2,4,128,128]{3,2,1,0:T(8,128)(2,1)S(1)}, bf16[2,4,128,128]{3,2,1,0:T(8,128)(2,1)S(1)}, u32[]{:S(2)}, u32[]{:S(2)}) collective-permute-start(bf16[2,4,128,128]{3,2,1,0:T(8,128)(2,1)S(1)} %pad_maximum_fusion.g0), channel_id=1, source_target_pairs={{0,4},{2,6},{4,0},{6,2},{1,5},{3,7},{5,1},{7,3},{8,12},{10,14},{12... | collective-permute-start | bytes 786440 | tf_op jit(solution)/shard_map/ppermute | solution.py:321
  59.7 3.8 %collective-permute-done.3.g3 = bf16[2,4,128,128]{3,2,1,0:T(8,128)(2,1)S(1)} collective-permute-done((bf16[2,4,128,128]{3,2,1,0:T(8,128)(2,1)S(1)}, bf16[2,4,128,128]{3,2,1,0:T(8,128)(2,1)S(1)}, u32[]{:S(2)}, u32[]{:S(2)}) %collective-permute-start.3) | collective-permute-done | bytes 262176 | tf_op jit(solution)/shard_map/ppermute | solution.py:321
  63.8 1.7 %collective-permute-start.15 = (bf16[4,128,1024]{2,1,0:T(8,128)(2,1)S(1)}, bf16[4,128,1024]{2,1,0:T(8,128)(2,1)S(1)}, u32[]{:S(2)}, u32[]{:S(2)}) collective-permute-start(bf16[4,128,1024]{2,1,0:T(8,128)(2,1)S(1)} %collective-permute-done.11.refs_2_), channel_id=1, source_target_pairs={{0,32},{1,97},{32,64},{33,1},{64,96},{65,33},{96,0},{97,65},{2,34}... | collective-permute-start | bytes 3145736 | tf_op jit(solution)/shard_map/ppermute | solution.py:330
  65.5 10.0 %collective-permute-start.13 = (bf16[4,128,1024]{2,1,0:T(8,128)(2,1)}, bf16[4,128,1024]{2,1,0:T(8,128)(2,1)S(1)}, u32[]{:S(2)}, u32[]{:S(2)}) collective-permute-start(bf16[4,128,1024]{2,1,0:T(8,128)(2,1)} %collective-permute-done.12.refs_4_), channel_id=1, source_target_pairs={{0,1},{1,0},{2,3},{3,2},{4,5},{5,4},{6,7},{7,6},{8,9},{9,8},{10,11... | collective-permute-start | bytes 3145736 | tf_op jit(solution)/shard_map/ppermute | solution.py:325
  76.1 2.4 %collective-permute-done.25.refs_2_ = bf16[4,1024,128]{2,1,0:T(8,128)(2,1)S(1)} collective-permute-done((bf16[4,1024,128]{2,1,0:T(8,128)(2,1)}, bf16[4,1024,128]{2,1,0:T(8,128)(2,1)S(1)}, u32[]{:S(2)}, u32[]{:S(2)}) %collective-permute-start.25) | collective-permute-done | bytes 1048608 | tf_op jit(solution)/shard_map/ppermute | solution.py:330
  78.5 20.5 %collective-permute-start.20 = (bf16[4,1024,128]{2,1,0:T(8,128)(2,1)}, bf16[4,1024,128]{2,1,0:T(8,128)(2,1)S(1)}, u32[]{:S(2)}, u32[]{:S(2)}) collective-permute-start(bf16[4,1024,128]{2,1,0:T(8,128)(2,1)} %shard_map.115.d0), channel_id=1, source_target_pairs={{0,1},{1,0},{2,3},{3,2},{4,5},{5,4},{6,7},{7,6},{8,9},{9,8},{10,11... | collective-permute-start | bytes 3145736 | tf_op jit(solution)/shard_map/ppermute | solution.py:325
  100.1 2.2 %copy-done = bf16[1024,2048]{1,0:T(8,128)(2,1)S(1)} copy-done((bf16[1024,2048]{1,0:T(8,128)(2,1)S(1)}, bf16[1024,2048]{1,0:T(8,128)(2,1)}, u32[]{:S(2)}) %copy-start) | copy-done | bytes 4194328
  102.6 0.7 copy-done.4
  103.3 4.6 %shard_map.112 = (bf16[512,1536]{1,0:T(8,128)(2,1)S(1)}, bf16[512,512]{1,0:T(8,128)(2,1)S(1)}, bf16[128,2048]{1,0:T(8,128)(2,1)S(1)}) custom-call(bf16[2,4,128,128]{3,2,1,0:T(8,128)(2,1)S(1)} %pad_maximum_fusion.g0, bf16[2,4,128,128]{3,2,1,0:T(8,128)(2,1)} %collective-permute-done.1.g1, bf16[2,4,128,128]{3,2,1,0:T(8,128)(2,1)S(1)} %collective-permute-done.2.g2, ...), custom_call_target="tpu_custom_call" | custom-call | flops 2147483648 | bytes 12000000 | tf_op jit(solution)/shard_map/pallas_call | solution.py:309
  107.9 5.1 %shard_map.114.acc_ref = f32[512,2048]{1,0:T(8,128)S(1)} custom-call(bf16[512,1536]{1,0:T(8,128)(2,1)S(1)} %get-tuple-element.33.x_ref, bf16[4,128,1024]{2,1,0:T(8,128)(2,1)S(1)} %shard_map.113.refs_0_, bf16[4,128,1024]{2,1,0:T(8,128)(2,1)S(1)} %collective-permute-done.10.refs_1_, bf16[4,128,1024]{2,1,0:T(8,128)(2,1)S(1)} %collective-permute-done.11.refs_2_, ...), custom_call_target="tpu_custom_call" | custom-call | flops 3221225472 | bytes 10000000 | tf_op jit(solution)/shard_map/pallas_call | solution.py:309
  113.1 3.2 %shard_map.116 = (bf16[512,2048]{1,0:T(8,128)(2,1)S(1)}, bf16[128,512]{1,0:T(8,128)(2,1)S(1)}, bf16[128,512]{1,0:T(8,128)(2,1)S(1)}, bf16[128,512]{1,0:T(8,128)(2,1)S(1)}, bf16[128,512]{1,0:T(8,128)(2,1)S(1)}) custom-call(bf16[512,512]{1,0:T(8,128)(2,1)S(1)} %get-tuple-element.32.x_ref, f32[512,2048]{1,0:T(8,128)S(1)} %shard_map.114.acc_ref, ...), custom_call_target="tpu_custom_call" | custom-call | flops 2147483648 | bytes 8000000 | tf_op jit(solution)/shard_map/pallas_call | solution.py:309
  116.3 2.7 %collective-permute-start.21 = (bf16[128,512]{1,0:T(8,128)(2,1)S(1)}, bf16[128,512]{1,0:T(8,128)(2,1)S(1)}, u32[]{:S(2)}, u32[]{:S(2)}) collective-permute-start(bf16[128,512]{1,0:T(8,128)(2,1)S(1)} %get-tuple-element.35), channel_id=1, source_target_pairs={{0,6},{2,0},{4,2},{6,4},{1,7},{3,1},{5,3},{7,5},{8,14},{10,8},{12,... | collective-permute-start | bytes 393224 | tf_op jit(solution)/shard_map/ppermute | solution.py:321
  119.1 1.6 %collective-permute-start.23 = (bf16[128,512]{1,0:T(8,128)(2,1)S(1)}, bf16[128,512]{1,0:T(8,128)(2,1)S(1)}, u32[]{:S(2)}, u32[]{:S(2)}) collective-permute-start(bf16[128,512]{1,0:T(8,128)(2,1)S(1)} %get-tuple-element.37), channel_id=1, source_target_pairs={{0,4},{2,6},{4,0},{6,2},{1,5},{3,7},{5,1},{7,3},{8,12},{10,14},{12... | collective-permute-start | bytes 393224 | tf_op jit(solution)/shard_map/ppermute | solution.py:321
  120.6 3.9 %shard_map.117 = (bf16[128,1024]{1,0:T(8,128)(2,1)S(1)}, bf16[128,1024]{1,0:T(8,128)(2,1)S(1)}, bf16[128,1024]{1,0:T(8,128)(2,1)S(1)}, bf16[128,1024]{1,0:T(8,128)(2,1)S(1)}) custom-call(bf16[512,2048]{1,0:T(8,128)(2,1)S(1)} %get-tuple-element.38.hid_ref, bf16[4,1024,128]{2,1,0:T(8,128)(2,1)S(1)} %collective-permute-done.24.refs_0_, ...), custom_call_target="tpu_custom_call" | custom-call | flops 2147483648 | bytes 6000000 | tf_op jit(solution)/shard_map/pallas_call | solution.py:309
  124.5 1.4 collective-permute-start.28
  125.9 1.7 %shard_map.118 = (bf16[128,512]{1,0:T(8,128)(2,1)S(1)}, bf16[128,512]{1,0:T(8,128)(2,1)S(1)}, bf16[128,512]{1,0:T(8,128)(2,1)S(1)}, bf16[128,512]{1,0:T(8,128)(2,1)S(1)}) custom-call(bf16[512,2048]{1,0:T(8,128)(2,1)S(1)} %get-tuple-element.38.hid_ref, bf16[4,1024,128]{2,1,0:T(8,128)(2,1)S(1)} %collective-permute-done.31.refs_0_, ...), custom_call_target="tpu_custom_call" | custom-call | flops 1073741824 | bytes 3000000 | tf_op jit(solution)/shard_map/pallas_call | solution.py:309
  127.6 0.6 collective-permute-start.33
  128.3 0.9 collective-permute-start.29
  129.2 2.4 %collective-permute-start.30 = (bf16[128,1024]{1,0:T(8,128)(2,1)S(1)}, bf16[128,1024]{1,0:T(8,128)(2,1)S(1)}, u32[]{:S(2)}, u32[]{:S(2)}) collective-permute-start(bf16[128,1024]{1,0:T(8,128)(2,1)S(1)} %get-tuple-element.42), channel_id=1, source_target_pairs={{0,4},{2,6},{4,0},{6,2},{1,5},{3,7},{5,1},{7,3},{8,12},{10,14},{12... | collective-permute-start | bytes 786440 | tf_op jit(solution)/shard_map/ppermute | solution.py:321
  131.5 3.3 %collective-permute-done.33.refs_9_ = bf16[128,512]{1,0:T(8,128)(2,1)S(1)} collective-permute-done((bf16[128,512]{1,0:T(8,128)(2,1)S(1)}, bf16[128,512]{1,0:T(8,128)(2,1)S(1)}, u32[]{:S(2)}, u32[]{:S(2)}) %collective-permute-start.33) | collective-permute-done | bytes 131104 | tf_op jit(solution)/shard_map/ppermute | solution.py:321
  134.8 1.2 collective-permute-start.35
  136.1 6.5 %collective-permute-done.34.refs_10_ = bf16[128,512]{1,0:T(8,128)(2,1)S(1)} collective-permute-done((bf16[128,512]{1,0:T(8,128)(2,1)S(1)}, bf16[128,512]{1,0:T(8,128)(2,1)S(1)}, u32[]{:S(2)}, u32[]{:S(2)}) %collective-permute-start.34) | collective-permute-done | bytes 131104 | tf_op jit(solution)/shard_map/ppermute | solution.py:321
  142.6 4.6 %collective-permute-done.35.refs_11_ = bf16[128,512]{1,0:T(8,128)(2,1)S(1)} collective-permute-done((bf16[128,512]{1,0:T(8,128)(2,1)S(1)}, bf16[128,512]{1,0:T(8,128)(2,1)S(1)}, u32[]{:S(2)}, u32[]{:S(2)}) %collective-permute-start.35) | collective-permute-done | bytes 131104 | tf_op jit(solution)/shard_map/ppermute | solution.py:321
  147.3 1.3 shard_map.119
  (60 shorter events, 3.5 us)
Async XLA Ops:
  0.0 16.0 %copy-start.8 = (bf16[1024,128]{1,0:T(8,128)(2,1)S(1)}, bf16[1024,128]{1,0:T(8,128)(2,1)}, u32[]{:S(2)}) copy-start(bf16[1024,128]{1,0:T(8,128)(2,1)} %refs_0_.3) | copy-start | bytes 786436
  0.0 18.7 %copy-start.2 = (bf16[128,2048]{1,0:T(8,128)(2,1)S(1)}, bf16[128,2048]{1,0:T(8,128)(2,1)}, u32[]{:S(2)}) copy-start(bf16[128,2048]{1,0:T(8,128)(2,1)} %s0.1) | copy-start | bytes 1572868
  0.0 19.9 %collective-permute-start.7 = (bf16[128,1024]{1,0:T(8,128)(2,1)}, bf16[128,1024]{1,0:T(8,128)(2,1)S(1)}, u32[]{:S(2)}, u32[]{:S(2)}) collective-permute-start(bf16[128,1024]{1,0:T(8,128)(2,1)} %refs_0_.2), channel_id=1, source_target_pairs={{0,8},{1,25},{8,16},{9,1},{16,24},{17,9},{24,0},{25,17},{2,10},{3,... | collective-permute-start | bytes 786440 | tf_op jit(solution)/shard_map/ppermute | solution.py:330
  3.6 17.8 %collective-permute-start.8 = (bf16[128,1024]{1,0:T(8,128)(2,1)}, bf16[128,1024]{1,0:T(8,128)(2,1)S(1)}, u32[]{:S(2)}, u32[]{:S(2)}) collective-permute-start(bf16[128,1024]{1,0:T(8,128)(2,1)} %refs_0_.2), channel_id=1, source_target_pairs={{0,24},{1,9},{8,0},{9,17},{16,8},{17,25},{24,16},{25,1},{2,26},{3,... | collective-permute-start | bytes 786440 | tf_op jit(solution)/shard_map/ppermute | solution.py:330
  3.6 30.1 %copy-start.5 = (bf16[128,1024]{1,0:T(8,128)(2,1)S(1)}, bf16[128,1024]{1,0:T(8,128)(2,1)}, u32[]{:S(2)}) copy-start(bf16[128,1024]{1,0:T(8,128)(2,1)} %refs_0_.2) | copy-start | bytes 786436
  8.5 16.2 %all-to-all-start = ((bf16[16,72,128]{2,1,0:T(8,128)(2,1)}), bf16[16,72,128]{2,1,0:T(8,128)(2,1)S(1)}, u32[]{:S(2)}, u32[]{:S(2)}) async-start(bf16[16,72,128]{2,1,0:T(8,128)(2,1)} %get-tuple-element.26), calls=%async_computation | async-start | bytes 589824 | tf_op jit(solution)/shard_map/all_to_all | solution.py:381
  16.0 12.8 %collective-permute-start.17 = (bf16[1024,128]{1,0:T(8,128)(2,1)S(1)}, bf16[1024,128]{1,0:T(8,128)(2,1)}, u32[]{:S(2)}, u32[]{:S(2)}) collective-permute-start(bf16[1024,128]{1,0:T(8,128)(2,1)S(1)} %copy-done.8), channel_id=1, source_target_pairs={{0,32},{1,97},{32,64},{33,1},{64,96},{65,33},{96,0},{97,65},{2,34}... | collective-permute-start | bytes 786440 | tf_op jit(solution)/shard_map/ppermute | solution.py:330
  18.7 11.6 %collective-permute-start.18 = (bf16[1024,128]{1,0:T(8,128)(2,1)S(1)}, bf16[1024,128]{1,0:T(8,128)(2,1)S(1)}, u32[]{:S(2)}, u32[]{:S(2)}) collective-permute-start(bf16[1024,128]{1,0:T(8,128)(2,1)S(1)} %copy-done.8), channel_id=1, source_target_pairs={{0,96},{1,33},{32,0},{33,65},{64,32},{65,97},{96,64},{97,1},{2,98}... | collective-permute-start | bytes 786440 | tf_op jit(solution)/shard_map/ppermute | solution.py:330
  18.7 15.5 %collective-permute-start.4 = (bf16[128,2048]{1,0:T(8,128)(2,1)S(1)}, bf16[128,2048]{1,0:T(8,128)(2,1)S(1)}, u32[]{:S(2)}, u32[]{:S(2)}) collective-permute-start(bf16[128,2048]{1,0:T(8,128)(2,1)S(1)} %copy-done.2), channel_id=1, source_target_pairs={{0,2},{2,4},{4,6},{6,0},{1,3},{3,5},{5,7},{7,1},{8,10},{10,12},{12... | collective-permute-start | bytes 1572872 | tf_op jit(solution)/shard_map/ppermute | solution.py:321
  19.9 15.4 %collective-permute-start.5 = (bf16[128,2048]{1,0:T(8,128)(2,1)S(1)}, bf16[128,2048]{1,0:T(8,128)(2,1)}, u32[]{:S(2)}, u32[]{:S(2)}) collective-permute-start(bf16[128,2048]{1,0:T(8,128)(2,1)S(1)} %copy-done.2), channel_id=1, source_target_pairs={{0,6},{2,0},{4,2},{6,4},{1,7},{3,1},{5,3},{7,5},{8,14},{10,8},{12,... | collective-permute-start | bytes 1572872 | tf_op jit(solution)/shard_map/ppermute | solution.py:321
  21.4 11.6 %collective-permute-start.9 = (bf16[128,1024]{1,0:T(8,128)(2,1)S(1)}, bf16[128,1024]{1,0:T(8,128)(2,1)S(1)}, u32[]{:S(2)}, u32[]{:S(2)}) collective-permute-start(bf16[128,1024]{1,0:T(8,128)(2,1)S(1)} %collective-permute-done.7.refs_1_), channel_id=1, source_target_pairs={{0,8},{1,25},{8,16},{9,1},{16,24},{17,9},{24,0},{25,17},{2,10},{3,... | collective-permute-start | bytes 786440 | tf_op jit(solution)/shard_map/ppermute | solution.py:330
  24.7 0.7 copy-start.7
  28.8 5.0 %collective-permute-start = (bf16[4,128,128]{2,1,0:T(8,128)(2,1)}, bf16[4,128,128]{2,1,0:T(8,128)(2,1)S(1)}, u32[]{:S(2)}, u32[]{:S(2)}) collective-permute-start(bf16[4,128,128]{2,1,0:T(8,128)(2,1)} %get-tuple-element.30), channel_id=1, source_target_pairs={{0,1},{1,0},{2,3},{3,2},{4,5},{5,4},{6,7},{7,6},{8,9},{9,8},{10,11... | collective-permute-start | bytes 393224 | tf_op jit(solution)/shard_map/ppermute | solution.py:325
  30.2 3.9 %copy-start.9 = (bf16[1024,128]{1,0:T(8,128)(2,1)}, bf16[1024,128]{1,0:T(8,128)(2,1)S(1)}, u32[]{:S(2)}) copy-start(bf16[1024,128]{1,0:T(8,128)(2,1)S(1)} %collective-permute-done.18.refs_2_) | copy-start | bytes 786436
  30.3 15.6 %collective-permute-start.6 = (bf16[128,2048]{1,0:T(8,128)(2,1)S(1)}, bf16[128,2048]{1,0:T(8,128)(2,1)}, u32[]{:S(2)}, u32[]{:S(2)}) collective-permute-start(bf16[128,2048]{1,0:T(8,128)(2,1)S(1)} %copy-done.2), channel_id=1, source_target_pairs={{0,4},{2,6},{4,0},{6,2},{1,5},{3,7},{5,1},{7,3},{8,12},{10,14},{12... | collective-permute-start | bytes 1572872 | tf_op jit(solution)/shard_map/ppermute | solution.py:321
  33.0 5.9 %collective-permute-start.19 = (bf16[1024,128]{1,0:T(8,128)(2,1)}, bf16[1024,128]{1,0:T(8,128)(2,1)S(1)}, u32[]{:S(2)}, u32[]{:S(2)}) collective-permute-start(bf16[1024,128]{1,0:T(8,128)(2,1)} %collective-permute-done.17.refs_1_), channel_id=1, source_target_pairs={{0,32},{1,97},{32,64},{33,1},{64,96},{65,33},{96,0},{97,65},{2,34}... | collective-permute-start | bytes 786440 | tf_op jit(solution)/shard_map/ppermute | solution.py:330
  33.8 30.0 %collective-permute-start.11 = (bf16[4,128,1024]{2,1,0:T(8,128)(2,1)S(1)}, bf16[4,128,1024]{2,1,0:T(8,128)(2,1)S(1)}, u32[]{:S(2)}, u32[]{:S(2)}) collective-permute-start(bf16[4,128,1024]{2,1,0:T(8,128)(2,1)S(1)} %shard_map.113.refs_0_), channel_id=1, source_target_pairs={{0,32},{1,97},{32,64},{33,1},{64,96},{65,33},{96,0},{97,65},{2,34}... | collective-permute-start | bytes 3145736 | tf_op jit(solution)/shard_map/ppermute | solution.py:330
  34.2 0.8 copy-start.3
  35.0 40.6 %collective-permute-start.10 = (bf16[4,128,1024]{2,1,0:T(8,128)(2,1)S(1)}, bf16[4,128,1024]{2,1,0:T(8,128)(2,1)S(1)}, u32[]{:S(2)}, u32[]{:S(2)}) collective-permute-start(bf16[4,128,1024]{2,1,0:T(8,128)(2,1)S(1)} %shard_map.113.refs_0_), channel_id=1, source_target_pairs={{0,1},{1,0},{2,3},{3,2},{4,5},{5,4},{6,7},{7,6},{8,9},{9,8},{10,11... | collective-permute-start | bytes 3145736 | tf_op jit(solution)/shard_map/ppermute | solution.py:325
  35.3 30.2 %collective-permute-start.12 = (bf16[4,128,1024]{2,1,0:T(8,128)(2,1)S(1)}, bf16[4,128,1024]{2,1,0:T(8,128)(2,1)}, u32[]{:S(2)}, u32[]{:S(2)}) collective-permute-start(bf16[4,128,1024]{2,1,0:T(8,128)(2,1)S(1)} %shard_map.113.refs_0_), channel_id=1, source_target_pairs={{0,96},{1,33},{32,0},{33,65},{64,32},{65,97},{96,64},{97,1},{2,98}... | collective-permute-start | bytes 3145736 | tf_op jit(solution)/shard_map/ppermute | solution.py:330
  38.9 0.7 copy-start.10
  39.6 9.2 %collective-permute-start.1 = (bf16[2,4,128,128]{3,2,1,0:T(8,128)(2,1)S(1)}, bf16[2,4,128,128]{3,2,1,0:T(8,128)(2,1)}, u32[]{:S(2)}, u32[]{:S(2)}) collective-permute-start(bf16[2,4,128,128]{3,2,1,0:T(8,128)(2,1)S(1)} %pad_maximum_fusion.g0), channel_id=1, source_target_pairs={{0,2},{2,4},{4,6},{6,0},{1,3},{3,5},{5,7},{7,1},{8,10},{10,12},{12... | collective-permute-start | bytes 786440 | tf_op jit(solution)/shard_map/ppermute | solution.py:321
  39.9 62.6 %copy-start.6 = (f32[2048]{0:T(1024)S(1)}, f32[2048]{0:T(1024)}, u32[]{:S(2)}) copy-start(f32[2048]{0:T(1024)} %param.19) | copy-start | bytes 24580
  45.8 29.8 %collective-permute-start.24 = (bf16[4,1024,128]{2,1,0:T(8,128)(2,1)}, bf16[4,1024,128]{2,1,0:T(8,128)(2,1)S(1)}, u32[]{:S(2)}, u32[]{:S(2)}) collective-permute-start(bf16[4,1024,128]{2,1,0:T(8,128)(2,1)} %shard_map.115.d0), channel_id=1, source_target_pairs={{0,8},{1,25},{8,16},{9,1},{16,24},{17,9},{24,0},{25,17},{2,10},{3,... | collective-permute-start | bytes 3145736 | tf_op jit(solution)/shard_map/ppermute | solution.py:330
  48.9 6.7 %collective-permute-start.2 = (bf16[2,4,128,128]{3,2,1,0:T(8,128)(2,1)S(1)}, bf16[2,4,128,128]{3,2,1,0:T(8,128)(2,1)S(1)}, u32[]{:S(2)}, u32[]{:S(2)}) collective-permute-start(bf16[2,4,128,128]{3,2,1,0:T(8,128)(2,1)S(1)} %pad_maximum_fusion.g0), channel_id=1, source_target_pairs={{0,6},{2,0},{4,2},{6,4},{1,7},{3,1},{5,3},{7,5},{8,14},{10,8},{12,... | collective-permute-start | bytes 786440 | tf_op jit(solution)/shard_map/ppermute | solution.py:321
  55.6 7.8 %collective-permute-start.3 = (bf16[2,4,128,128]{3,2,1,0:T(8,128)(2,1)S(1)}, bf16[2,4,128,128]{3,2,1,0:T(8,128)(2,1)S(1)}, u32[]{:S(2)}, u32[]{:S(2)}) collective-permute-start(bf16[2,4,128,128]{3,2,1,0:T(8,128)(2,1)S(1)} %pad_maximum_fusion.g0), channel_id=1, source_target_pairs={{0,4},{2,6},{4,0},{6,2},{1,5},{3,7},{5,1},{7,3},{8,12},{10,14},{12... | collective-permute-start | bytes 786440 | tf_op jit(solution)/shard_map/ppermute | solution.py:321
  63.4 15.1 %collective-permute-start.25 = (bf16[4,1024,128]{2,1,0:T(8,128)(2,1)}, bf16[4,1024,128]{2,1,0:T(8,128)(2,1)S(1)}, u32[]{:S(2)}, u32[]{:S(2)}) collective-permute-start(bf16[4,1024,128]{2,1,0:T(8,128)(2,1)} %shard_map.115.d0), channel_id=1, source_target_pairs={{0,24},{1,9},{8,0},{9,17},{16,8},{17,25},{24,16},{25,1},{2,26},{3,... | collective-permute-start | bytes 3145736 | tf_op jit(solution)/shard_map/ppermute | solution.py:330
  63.8 35.2 %collective-permute-start.15 = (bf16[4,128,1024]{2,1,0:T(8,128)(2,1)S(1)}, bf16[4,128,1024]{2,1,0:T(8,128)(2,1)S(1)}, u32[]{:S(2)}, u32[]{:S(2)}) collective-permute-start(bf16[4,128,1024]{2,1,0:T(8,128)(2,1)S(1)} %collective-permute-done.11.refs_2_), channel_id=1, source_target_pairs={{0,32},{1,97},{32,64},{33,1},{64,96},{65,33},{96,0},{97,65},{2,34}... | collective-permute-start | bytes 3145736 | tf_op jit(solution)/shard_map/ppermute | solution.py:330
  65.5 33.5 %collective-permute-start.13 = (bf16[4,128,1024]{2,1,0:T(8,128)(2,1)}, bf16[4,128,1024]{2,1,0:T(8,128)(2,1)S(1)}, u32[]{:S(2)}, u32[]{:S(2)}) collective-permute-start(bf16[4,128,1024]{2,1,0:T(8,128)(2,1)} %collective-permute-done.12.refs_4_), channel_id=1, source_target_pairs={{0,1},{1,0},{2,3},{3,2},{4,5},{5,4},{6,7},{7,6},{8,9},{9,8},{10,11... | collective-permute-start | bytes 3145736 | tf_op jit(solution)/shard_map/ppermute | solution.py:325
  75.5 24.0 %collective-permute-start.14 = (bf16[4,128,1024]{2,1,0:T(8,128)(2,1)S(1)}, bf16[4,128,1024]{2,1,0:T(8,128)(2,1)S(1)}, u32[]{:S(2)}, u32[]{:S(2)}) collective-permute-start(bf16[4,128,1024]{2,1,0:T(8,128)(2,1)S(1)} %collective-permute-done.11.refs_2_), channel_id=1, source_target_pairs={{0,1},{1,0},{2,3},{3,2},{4,5},{5,4},{6,7},{7,6},{8,9},{9,8},{10,11... | collective-permute-start | bytes 3145736 | tf_op jit(solution)/shard_map/ppermute | solution.py:325
  75.6 24.0 %collective-permute-start.31 = (bf16[4,1024,128]{2,1,0:T(8,128)(2,1)S(1)}, bf16[4,1024,128]{2,1,0:T(8,128)(2,1)S(1)}, u32[]{:S(2)}, u32[]{:S(2)}) collective-permute-start(bf16[4,1024,128]{2,1,0:T(8,128)(2,1)S(1)} %collective-permute-done.24.refs_0_), channel_id=1, source_target_pairs={{0,8},{1,25},{8,16},{9,1},{16,24},{17,9},{24,0},{25,17},{2,10},{3,... | collective-permute-start | bytes 3145736 | tf_op jit(solution)/shard_map/ppermute | solution.py:330
  78.5 34.6 %collective-permute-start.20 = (bf16[4,1024,128]{2,1,0:T(8,128)(2,1)}, bf16[4,1024,128]{2,1,0:T(8,128)(2,1)S(1)}, u32[]{:S(2)}, u32[]{:S(2)}) collective-permute-start(bf16[4,1024,128]{2,1,0:T(8,128)(2,1)} %shard_map.115.d0), channel_id=1, source_target_pairs={{0,1},{1,0},{2,3},{3,2},{4,5},{5,4},{6,7},{7,6},{8,9},{9,8},{10,11... | collective-permute-start | bytes 3145736 | tf_op jit(solution)/shard_map/ppermute | solution.py:325
  99.0 14.1 %collective-permute-start.16 = (bf16[4,128,1024]{2,1,0:T(8,128)(2,1)S(1)}, bf16[4,128,1024]{2,1,0:T(8,128)(2,1)S(1)}, u32[]{:S(2)}, u32[]{:S(2)}) collective-permute-start(bf16[4,128,1024]{2,1,0:T(8,128)(2,1)S(1)} %collective-permute-done.15.u0), channel_id=1, source_target_pairs={{0,1},{1,0},{2,3},{3,2},{4,5},{5,4},{6,7},{7,6},{8,9},{9,8},{10,11... | collective-permute-start | bytes 3145736 | tf_op jit(solution)/shard_map/ppermute | solution.py:325
  99.0 20.0 %collective-permute-start.26 = (bf16[4,1024,128]{2,1,0:T(8,128)(2,1)S(1)}, bf16[4,1024,128]{2,1,0:T(8,128)(2,1)S(1)}, u32[]{:S(2)}, u32[]{:S(2)}) collective-permute-start(bf16[4,1024,128]{2,1,0:T(8,128)(2,1)S(1)} %collective-permute-done.25.refs_2_), channel_id=1, source_target_pairs={{0,1},{1,0},{2,3},{3,2},{4,5},{5,4},{6,7},{7,6},{8,9},{9,8},{10,11... | collective-permute-start | bytes 3145736 | tf_op jit(solution)/shard_map/ppermute | solution.py:325
  99.5 21.1 %collective-permute-start.27 = (bf16[4,1024,128]{2,1,0:T(8,128)(2,1)S(1)}, bf16[4,1024,128]{2,1,0:T(8,128)(2,1)S(1)}, u32[]{:S(2)}, u32[]{:S(2)}) collective-permute-start(bf16[4,1024,128]{2,1,0:T(8,128)(2,1)S(1)} %collective-permute-done.24.refs_0_), channel_id=1, source_target_pairs={{0,1},{1,0},{2,3},{3,2},{4,5},{5,4},{6,7},{7,6},{8,9},{9,8},{10,11... | collective-permute-start | bytes 3145736 | tf_op jit(solution)/shard_map/ppermute | solution.py:325
  99.6 26.3 %collective-permute-start.32 = (bf16[4,1024,128]{2,1,0:T(8,128)(2,1)S(1)}, bf16[4,1024,128]{2,1,0:T(8,128)(2,1)S(1)}, u32[]{:S(2)}, u32[]{:S(2)}) collective-permute-start(bf16[4,1024,128]{2,1,0:T(8,128)(2,1)S(1)} %collective-permute-done.31.refs_0_), channel_id=1, source_target_pairs={{0,1},{1,0},{2,3},{3,2},{4,5},{5,4},{6,7},{7,6},{8,9},{9,8},{10,11... | collective-permute-start | bytes 3145736 | tf_op jit(solution)/shard_map/ppermute | solution.py:325
  100.1 2.2 %copy-start = (bf16[1024,2048]{1,0:T(8,128)(2,1)S(1)}, bf16[1024,2048]{1,0:T(8,128)(2,1)}, u32[]{:S(2)}) copy-start(bf16[1024,2048]{1,0:T(8,128)(2,1)} %w_ref.1) | copy-start | bytes 12582916
  102.2 1.0 copy-start.4
  107.9 5.2 %copy-start.1 = (bf16[4,1024,128]{2,1,0:T(8,128)(2,1)S(1)}, bf16[4,1024,128]{2,1,0:T(8,128)(2,1)}, u32[]{:S(2)}) copy-start(bf16[4,1024,128]{2,1,0:T(8,128)(2,1)} %shard_map.115.d0) | copy-start | bytes 3145732
  116.3 12.0 %collective-permute-start.21 = (bf16[128,512]{1,0:T(8,128)(2,1)S(1)}, bf16[128,512]{1,0:T(8,128)(2,1)S(1)}, u32[]{:S(2)}, u32[]{:S(2)}) collective-permute-start(bf16[128,512]{1,0:T(8,128)(2,1)S(1)} %get-tuple-element.35), channel_id=1, source_target_pairs={{0,6},{2,0},{4,2},{6,4},{1,7},{3,1},{5,3},{7,5},{8,14},{10,8},{12,... | collective-permute-start | bytes 393224 | tf_op jit(solution)/shard_map/ppermute | solution.py:321
  119.1 10.1 %collective-permute-start.22 = (bf16[128,512]{1,0:T(8,128)(2,1)S(1)}, bf16[128,512]{1,0:T(8,128)(2,1)S(1)}, u32[]{:S(2)}, u32[]{:S(2)}) collective-permute-start(bf16[128,512]{1,0:T(8,128)(2,1)S(1)} %get-tuple-element.36), channel_id=1, source_target_pairs={{0,2},{2,4},{4,6},{6,0},{1,3},{3,5},{5,7},{7,1},{8,10},{10,12},{12... | collective-permute-start | bytes 393224 | tf_op jit(solution)/shard_map/ppermute | solution.py:321
  119.1 12.5 %collective-permute-start.23 = (bf16[128,512]{1,0:T(8,128)(2,1)S(1)}, bf16[128,512]{1,0:T(8,128)(2,1)S(1)}, u32[]{:S(2)}, u32[]{:S(2)}) collective-permute-start(bf16[128,512]{1,0:T(8,128)(2,1)S(1)} %get-tuple-element.37), channel_id=1, source_target_pairs={{0,4},{2,6},{4,0},{6,2},{1,5},{3,7},{5,1},{7,3},{8,12},{10,14},{12... | collective-permute-start | bytes 393224 | tf_op jit(solution)/shard_map/ppermute | solution.py:321
  124.5 22.7 %collective-permute-start.28 = (bf16[128,1024]{1,0:T(8,128)(2,1)S(1)}, bf16[128,1024]{1,0:T(8,128)(2,1)S(1)}, u32[]{:S(2)}, u32[]{:S(2)}) collective-permute-start(bf16[128,1024]{1,0:T(8,128)(2,1)S(1)} %get-tuple-element.40), channel_id=1, source_target_pairs={{0,6},{2,0},{4,2},{6,4},{1,7},{3,1},{5,3},{7,5},{8,14},{10,8},{12,... | collective-permute-start | bytes 786440 | tf_op jit(solution)/shard_map/ppermute | solution.py:321
  127.6 7.2 %collective-permute-start.33 = (bf16[128,512]{1,0:T(8,128)(2,1)S(1)}, bf16[128,512]{1,0:T(8,128)(2,1)S(1)}, u32[]{:S(2)}, u32[]{:S(2)}) collective-permute-start(bf16[128,512]{1,0:T(8,128)(2,1)S(1)} %get-tuple-element.44), channel_id=1, source_target_pairs={{0,6},{2,0},{4,2},{6,4},{1,7},{3,1},{5,3},{7,5},{8,14},{10,8},{12,... | collective-permute-start | bytes 393224 | tf_op jit(solution)/shard_map/ppermute | solution.py:321
  128.3 19.0 %collective-permute-start.29 = (bf16[128,1024]{1,0:T(8,128)(2,1)S(1)}, bf16[128,1024]{1,0:T(8,128)(2,1)S(1)}, u32[]{:S(2)}, u32[]{:S(2)}) collective-permute-start(bf16[128,1024]{1,0:T(8,128)(2,1)S(1)} %get-tuple-element.41), channel_id=1, source_target_pairs={{0,2},{2,4},{4,6},{6,0},{1,3},{3,5},{5,7},{7,1},{8,10},{10,12},{12... | collective-permute-start | bytes 786440 | tf_op jit(solution)/shard_map/ppermute | solution.py:321
  129.2 18.1 %collective-permute-start.30 = (bf16[128,1024]{1,0:T(8,128)(2,1)S(1)}, bf16[128,1024]{1,0:T(8,128)(2,1)S(1)}, u32[]{:S(2)}, u32[]{:S(2)}) collective-permute-start(bf16[128,1024]{1,0:T(8,128)(2,1)S(1)} %get-tuple-element.42), channel_id=1, source_target_pairs={{0,4},{2,6},{4,0},{6,2},{1,5},{3,7},{5,1},{7,3},{8,12},{10,14},{12... | collective-permute-start | bytes 786440 | tf_op jit(solution)/shard_map/ppermute | solution.py:321
  131.5 11.1 %collective-permute-start.34 = (bf16[128,512]{1,0:T(8,128)(2,1)S(1)}, bf16[128,512]{1,0:T(8,128)(2,1)S(1)}, u32[]{:S(2)}, u32[]{:S(2)}) collective-permute-start(bf16[128,512]{1,0:T(8,128)(2,1)S(1)} %get-tuple-element.45), channel_id=1, source_target_pairs={{0,2},{2,4},{4,6},{6,0},{1,3},{3,5},{5,7},{7,1},{8,10},{10,12},{12... | collective-permute-start | bytes 393224 | tf_op jit(solution)/shard_map/ppermute | solution.py:321
  134.8 12.4 %collective-permute-start.35 = (bf16[128,512]{1,0:T(8,128)(2,1)S(1)}, bf16[128,512]{1,0:T(8,128)(2,1)S(1)}, u32[]{:S(2)}, u32[]{:S(2)}) collective-permute-start(bf16[128,512]{1,0:T(8,128)(2,1)S(1)} %get-tuple-element.46), channel_id=1, source_target_pairs={{0,4},{2,6},{4,0},{6,2},{1,5},{3,7},{5,1},{7,3},{8,12},{10,14},{12... | collective-permute-start | bytes 393224 | tf_op jit(solution)/shard_map/ppermute | solution.py:321

commit v3 on v2

--- a/solution.py
+++ b/solution.py
@@ -266,7 +266,7 @@
         for i in range(4):
             sp = lax.rem(pos[0] + steps[i] + 4, 4) * 4 + lax.rem(pos[1] + steps[j] + 4, 4)
             at = pl.ds(pl.multiple_of(sp * 128, 128), 128)
-            src, off = ((parts[0], 0), (parts[1], 0), (parts[1], 512), (parts[2], 0))[j]
+            src, off = ((parts[0], 0), (parts[1], 0), (parts[2], 0), (parts[2], 512))[j]
             cols = slice(off + i * 128, off + (i + 1) * 128)
             total = src[0][:, cols].astype(f32) + src[1][:, cols].astype(f32)
             total = total + src[2][:, cols].astype(f32) + src[3][:, cols].astype(f32)
@@ -470,8 +470,8 @@
         return [parts[0]] + [shifted(parts[k], "x", NEAR[k]) for k in (1, 2, 3)]
 
     first = sent_back(first)
-    second = sent_back(down((1, 2)))
-    third = sent_back(down((3,)))
+    second = sent_back(down((1,)))
+    third = sent_back(down((2, 3)))
     return call(
         end_kernel,
         [VMEM] * 13,

time: 151 us -> 149 us (0.987)
  the two profiles are of different devices: /device:TPU:1 before, /device:TPU:96 now
where the time goes in v3:
time: 149 us
  waiting for transfers between devices  63.8 us (43%)
  starting transfers between devices  48.2 us (32%)
  Pallas kernels  30.4 us (20%)
  local copies, waits for them, and re-layouts  5.18 us (3%)
    ppermute x15, waiting for transfers between devices, shifted(): return lax.ppermute(v, axis, [(i, (i + by) % n) for i in range(n)])  34.8 us
    pallas_call x11, Pallas kernels, launched(): pl.pallas_call(kernel, in_specs=ins, out_specs=[spec] * len(outs), out_sh...  30.4 us
    ppermute x12, waiting for transfers between devices, both_ways(): return lax.ppermute(v, (axis, 'c'), pairs)  28.9 us
    ppermute x15, starting transfers between devices, shifted(): return lax.ppermute(v, axis, [(i, (i + by) % n) for i in range(n)])  23.1 us
    ppermute x12, starting transfers between devices, both_ways(): return lax.ppermute(v, (axis, 'c'), pairs)  12.6 us
    ppermute x9, starting transfers between devices, swapped(): return lax.ppermute(v, 'c', [(0, 1), (1, 0)])  6.51 us
    all_to_all x1, starting transfers between devices, local(): got = lax.all_to_all(sent, SP, 0, 0, tiled=True)  5.95 us
    unnamed x22, local copies, waits for them, and re-layouts  5.18 us
  transfers between devices with their start and end apart: 37, of which 8 were waited for; matrix products, arithmetic and copies ran while one was open for 1% of the time, Pallas kernels for 20%

profile of v3, /device:TPU:96, one launch (start us, length us, event | category | flops | bytes accessed | tf_op | source)
XLA Modules:
  0.0 148.8 jit_solution(12789576066910507774)
XLA Ops:
  0.0 1.6 %collective-permute-start.7 = (bf16[128,1024]{1,0:T(8,128)(2,1)}, bf16[128,1024]{1,0:T(8,128)(2,1)S(1)}, u32[]{:S(2)}, u32[]{:S(2)}) collective-permute-start(bf16[128,1024]{1,0:T(8,128)(2,1)} %refs_0_.2), channel_id=1, source_target_pairs={{0,8},{1,25},{8,16},{9,1},{16,24},{17,9},{24,0},{25,17},{2,10},{3,... | collective-permute-start | bytes 786440 | tf_op jit(solution)/shard_map/ppermute | solution.py:330
  1.6 1.7 %collective-permute-start.8 = (bf16[128,1024]{1,0:T(8,128)(2,1)}, bf16[128,1024]{1,0:T(8,128)(2,1)S(1)}, u32[]{:S(2)}, u32[]{:S(2)}) collective-permute-start(bf16[128,1024]{1,0:T(8,128)(2,1)} %refs_0_.2), channel_id=1, source_target_pairs={{0,24},{1,9},{8,0},{9,17},{16,8},{17,25},{24,16},{25,1},{2,26},{3,... | collective-permute-start | bytes 786440 | tf_op jit(solution)/shard_map/ppermute | solution.py:330
  3.2 4.9 %shard_map.109 = (f32[1024,128]{1,0:T(8,128)}, bf16[1024,128]{1,0:T(8,128)(2,1)}, bf16[16,72,128]{2,1,0:T(8,128)(2,1)}) custom-call(bf16[64,1024]{1,0:T(8,128)(2,1)} %bitcast.11, bf16[64,1024]{1,0:T(8,128)(2,1)} %bitcast.12, bf16[1024,128]{1,0:T(8,128)(2,1)} %v_ref.1, f32[2,64,1024]{2,1,0:T(8,128)} %bitcast.10), custom_call_target="tpu_custom_call" | custom-call | flops 2000000000 | bytes 2000000 | tf_op jit(solution)/shard_map/pallas_call | solution.py:309
  8.2 6.0 %all-to-all-start = ((bf16[16,72,128]{2,1,0:T(8,128)(2,1)}), bf16[16,72,128]{2,1,0:T(8,128)(2,1)S(1)}, u32[]{:S(2)}, u32[]{:S(2)}) async-start(bf16[16,72,128]{2,1,0:T(8,128)(2,1)} %get-tuple-element.26), calls=%async_computation | async-start | bytes 589824 | tf_op jit(solution)/shard_map/all_to_all | solution.py:381
  14.3 1.5 %collective-permute-start.4 = (bf16[128,2048]{1,0:T(8,128)(2,1)S(1)}, bf16[128,2048]{1,0:T(8,128)(2,1)S(1)}, u32[]{:S(2)}, u32[]{:S(2)}) collective-permute-start(bf16[128,2048]{1,0:T(8,128)(2,1)S(1)} %copy-done.2), channel_id=1, source_target_pairs={{0,2},{2,4},{4,6},{6,0},{1,3},{3,5},{5,7},{7,1},{8,10},{10,12},{12... | collective-permute-start | bytes 1572872 | tf_op jit(solution)/shard_map/ppermute | solution.py:321
  15.8 1.9 %collective-permute-start.18 = (bf16[1024,128]{1,0:T(8,128)(2,1)S(1)}, bf16[1024,128]{1,0:T(8,128)(2,1)S(1)}, u32[]{:S(2)}, u32[]{:S(2)}) collective-permute-start(bf16[1024,128]{1,0:T(8,128)(2,1)S(1)} %copy-done.8), channel_id=1, source_target_pairs={{0,96},{1,33},{32,0},{33,65},{64,32},{65,97},{96,64},{97,1},{2,98}... | collective-permute-start | bytes 786440 | tf_op jit(solution)/shard_map/ppermute | solution.py:330
  17.7 1.5 collective-permute-start.9
  19.2 1.7 %collective-permute-start.5 = (bf16[128,2048]{1,0:T(8,128)(2,1)S(1)}, bf16[128,2048]{1,0:T(8,128)(2,1)}, u32[]{:S(2)}, u32[]{:S(2)}) collective-permute-start(bf16[128,2048]{1,0:T(8,128)(2,1)S(1)} %copy-done.2), channel_id=1, source_target_pairs={{0,6},{2,0},{4,2},{6,4},{1,7},{3,1},{5,3},{7,5},{8,14},{10,8},{12,... | collective-permute-start | bytes 1572872 | tf_op jit(solution)/shard_map/ppermute | solution.py:321
  20.9 4.3 %collective-permute-done.17.refs_1_ = bf16[1024,128]{1,0:T(8,128)(2,1)} collective-permute-done((bf16[1024,128]{1,0:T(8,128)(2,1)S(1)}, bf16[1024,128]{1,0:T(8,128)(2,1)}, u32[]{:S(2)}, u32[]{:S(2)}) %collective-permute-start.17) | collective-permute-done | bytes 262176 | tf_op jit(solution)/shard_map/ppermute | solution.py:330
  25.2 3.0 %collective-permute-start.6 = (bf16[128,2048]{1,0:T(8,128)(2,1)S(1)}, bf16[128,2048]{1,0:T(8,128)(2,1)}, u32[]{:S(2)}, u32[]{:S(2)}) collective-permute-start(bf16[128,2048]{1,0:T(8,128)(2,1)S(1)} %copy-done.2), channel_id=1, source_target_pairs={{0,4},{2,6},{4,0},{6,2},{1,5},{3,7},{5,1},{7,3},{8,12},{10,14},{12... | collective-permute-start | bytes 1572872 | tf_op jit(solution)/shard_map/ppermute | solution.py:321
  28.3 0.7 copy-done.7
  29.0 3.4 %shard_map.110 = (bf16[4,128,128]{2,1,0:T(8,128)(2,1)}, bf16[4,128,128]{2,1,0:T(8,128)(2,1)}) custom-call(bf16[16,72,128]{2,1,0:T(8,128)(2,1)} %copy-done.7, f32[1024,128]{1,0:T(8,128)} %get-tuple-element.27.local_hbm, bf16[1024,128]{1,0:T(8,128)(2,1)} %get-tuple-element.28.carry_hbm, bf16[1024,128]{1,0:T(8,128)(2,1)} %gate_hbm.1, f32[1,128]{1,0:T(1,128)} %bitcast.13), custom_call_target="tpu_custom_call" | custom-call | flops 1000000000 | bytes 2000000 | tf_op jit(solution)/shard_map/pallas_call | solution.py:309
  32.5 1.6 %collective-permute-start.19 = (bf16[1024,128]{1,0:T(8,128)(2,1)}, bf16[1024,128]{1,0:T(8,128)(2,1)S(1)}, u32[]{:S(2)}, u32[]{:S(2)}) collective-permute-start(bf16[1024,128]{1,0:T(8,128)(2,1)} %collective-permute-done.17.refs_1_), channel_id=1, source_target_pairs={{0,32},{1,97},{32,64},{33,1},{64,96},{65,33},{96,0},{97,65},{2,34}... | collective-permute-start | bytes 786440 | tf_op jit(solution)/shard_map/ppermute | solution.py:330
  34.3 1.3 collective-permute-start.11
  35.6 0.8 copy-done.3
  36.4 0.8 collective-permute-start.12
  37.2 0.9 pad_maximum_fusion.g0
  38.1 0.8 collective-permute-start.1
  38.9 1.2 collective-permute-done.19.refs_3_
  40.1 0.7 copy-done.10
  40.8 4.6 %collective-permute-start.10 = (bf16[4,128,1024]{2,1,0:T(8,128)(2,1)S(1)}, bf16[4,128,1024]{2,1,0:T(8,128)(2,1)}, u32[]{:S(2)}, u32[]{:S(2)}) collective-permute-start(bf16[4,128,1024]{2,1,0:T(8,128)(2,1)S(1)} %shard_map.113.refs_0_), channel_id=1, source_target_pairs={{0,1},{1,0},{2,3},{3,2},{4,5},{5,4},{6,7},{7,6},{8,9},{9,8},{10,11... | collective-permute-start | bytes 3145736 | tf_op jit(solution)/shard_map/ppermute | solution.py:325
  45.4 2.0 %shard_map.115.d0 = bf16[4,1024,128]{2,1,0:T(8,128)(2,1)} custom-call(bf16[1024,128]{1,0:T(8,128)(2,1)} %refs_0_.3, bf16[1024,128]{1,0:T(8,128)(2,1)} %collective-permute-done.17.refs_1_, bf16[1024,128]{1,0:T(8,128)(2,1)} %copy-done.9, bf16[1024,128]{1,0:T(8,128)(2,1)} %copy-done.10), custom_call_target="tpu_custom_call" | custom-call | flops 800000000 | bytes 2000000 | tf_op jit(solution)/shard_map/pallas_call | solution.py:309
  47.5 7.4 %collective-permute-done.1.g1 = bf16[2,4,128,128]{3,2,1,0:T(8,128)(2,1)} collective-permute-done((bf16[2,4,128,128]{3,2,1,0:T(8,128)(2,1)S(1)}, bf16[2,4,128,128]{3,2,1,0:T(8,128)(2,1)}, u32[]{:S(2)}, u32[]{:S(2)}) %collective-permute-start.1) | collective-permute-done | bytes 262176 | tf_op jit(solution)/shard_map/ppermute | solution.py:321
  54.9 1.7 %collective-permute-start.2 = (bf16[2,4,128,128]{3,2,1,0:T(8,128)(2,1)S(1)}, bf16[2,4,128,128]{3,2,1,0:T(8,128)(2,1)S(1)}, u32[]{:S(2)}, u32[]{:S(2)}) collective-permute-start(bf16[2,4,128,128]{3,2,1,0:T(8,128)(2,1)S(1)} %pad_maximum_fusion.g0), channel_id=1, source_target_pairs={{0,6},{2,0},{4,2},{6,4},{1,7},{3,1},{5,3},{7,5},{8,14},{10,8},{12,... | collective-permute-start | bytes 786440 | tf_op jit(solution)/shard_map/ppermute | solution.py:321
  56.6 6.0 %collective-permute-done.2.g2 = bf16[2,4,128,128]{3,2,1,0:T(8,128)(2,1)S(1)} collective-permute-done((bf16[2,4,128,128]{3,2,1,0:T(8,128)(2,1)S(1)}, bf16[2,4,128,128]{3,2,1,0:T(8,128)(2,1)S(1)}, u32[]{:S(2)}, u32[]{:S(2)}) %collective-permute-start.2) | collective-permute-done | bytes 262176 | tf_op jit(solution)/shard_map/ppermute | solution.py:321
  62.6 1.2 collective-permute-start.3
  63.8 7.2 %collective-permute-done.3.g3 = bf16[2,4,128,128]{3,2,1,0:T(8,128)(2,1)S(1)} collective-permute-done((bf16[2,4,128,128]{3,2,1,0:T(8,128)(2,1)S(1)}, bf16[2,4,128,128]{3,2,1,0:T(8,128)(2,1)S(1)}, u32[]{:S(2)}, u32[]{:S(2)}) %collective-permute-start.3) | collective-permute-done | bytes 262176 | tf_op jit(solution)/shard_map/ppermute | solution.py:321
  71.2 0.5 collective-permute-start.14
  71.7 2.0 %collective-permute-start.31 = (bf16[4,1024,128]{2,1,0:T(8,128)(2,1)S(1)}, bf16[4,1024,128]{2,1,0:T(8,128)(2,1)S(1)}, u32[]{:S(2)}, u32[]{:S(2)}) collective-permute-start(bf16[4,1024,128]{2,1,0:T(8,128)(2,1)S(1)} %collective-permute-done.24.refs_0_), channel_id=1, source_target_pairs={{0,8},{1,25},{8,16},{9,1},{16,24},{17,9},{24,0},{25,17},{2,10},{3,... | collective-permute-start | bytes 3145736 | tf_op jit(solution)/shard_map/ppermute | solution.py:330
  73.7 23.4 %collective-permute-done.25.refs_0_ = bf16[4,1024,128]{2,1,0:T(8,128)(2,1)S(1)} collective-permute-done((bf16[4,1024,128]{2,1,0:T(8,128)(2,1)}, bf16[4,1024,128]{2,1,0:T(8,128)(2,1)S(1)}, u32[]{:S(2)}, u32[]{:S(2)}) %collective-permute-start.25) | collective-permute-done | bytes 1048608 | tf_op jit(solution)/shard_map/ppermute | solution.py:330
  97.1 0.5 collective-permute-start.16
  98.4 2.2 %copy-done = bf16[1024,2048]{1,0:T(8,128)(2,1)S(1)} copy-done((bf16[1024,2048]{1,0:T(8,128)(2,1)S(1)}, bf16[1024,2048]{1,0:T(8,128)(2,1)}, u32[]{:S(2)}) %copy-start) | copy-done | bytes 4194328
  100.9 0.7 copy-done.4
  101.6 4.6 %shard_map.112 = (bf16[512,1536]{1,0:T(8,128)(2,1)S(1)}, bf16[512,512]{1,0:T(8,128)(2,1)S(1)}, bf16[128,2048]{1,0:T(8,128)(2,1)S(1)}) custom-call(bf16[2,4,128,128]{3,2,1,0:T(8,128)(2,1)S(1)} %pad_maximum_fusion.g0, bf16[2,4,128,128]{3,2,1,0:T(8,128)(2,1)} %collective-permute-done.1.g1, bf16[2,4,128,128]{3,2,1,0:T(8,128)(2,1)S(1)} %collective-permute-done.2.g2, ...), custom_call_target="tpu_custom_call" | custom-call | flops 2147483648 | bytes 12000000 | tf_op jit(solution)/shard_map/pallas_call | solution.py:309
  106.3 5.0 %shard_map.114.acc_ref = f32[512,2048]{1,0:T(8,128)S(1)} custom-call(bf16[512,1536]{1,0:T(8,128)(2,1)S(1)} %get-tuple-element.33.x_ref, bf16[4,128,1024]{2,1,0:T(8,128)(2,1)S(1)} %shard_map.113.refs_0_, bf16[4,128,1024]{2,1,0:T(8,128)(2,1)} %collective-permute-done.10.refs_1_, bf16[4,128,1024]{2,1,0:T(8,128)(2,1)S(1)} %collective-permute-done.11.refs_2_, ...), custom_call_target="tpu_custom_call" | custom-call | flops 3221225472 | bytes 10000000 | tf_op jit(solution)/shard_map/pallas_call | solution.py:309
  111.3 3.2 %shard_map.116 = (bf16[512,2048]{1,0:T(8,128)(2,1)S(1)}, bf16[128,512]{1,0:T(8,128)(2,1)S(1)}, bf16[128,512]{1,0:T(8,128)(2,1)S(1)}, bf16[128,512]{1,0:T(8,128)(2,1)S(1)}, bf16[128,512]{1,0:T(8,128)(2,1)S(1)}) custom-call(bf16[512,512]{1,0:T(8,128)(2,1)S(1)} %get-tuple-element.32.x_ref, f32[512,2048]{1,0:T(8,128)S(1)} %shard_map.114.acc_ref, ...), custom_call_target="tpu_custom_call" | custom-call | flops 2147483648 | bytes 8000000 | tf_op jit(solution)/shard_map/pallas_call | solution.py:309
  114.5 2.5 %collective-permute-start.21 = (bf16[128,512]{1,0:T(8,128)(2,1)S(1)}, bf16[128,512]{1,0:T(8,128)(2,1)S(1)}, u32[]{:S(2)}, u32[]{:S(2)}) collective-permute-start(bf16[128,512]{1,0:T(8,128)(2,1)S(1)} %get-tuple-element.35), channel_id=1, source_target_pairs={{0,6},{2,0},{4,2},{6,4},{1,7},{3,1},{5,3},{7,5},{8,14},{10,8},{12,... | collective-permute-start | bytes 393224 | tf_op jit(solution)/shard_map/ppermute | solution.py:321
  117.0 1.5 %collective-permute-start.23 = (bf16[128,512]{1,0:T(8,128)(2,1)S(1)}, bf16[128,512]{1,0:T(8,128)(2,1)S(1)}, u32[]{:S(2)}, u32[]{:S(2)}) collective-permute-start(bf16[128,512]{1,0:T(8,128)(2,1)S(1)} %get-tuple-element.37), channel_id=1, source_target_pairs={{0,4},{2,6},{4,0},{6,2},{1,5},{3,7},{5,1},{7,3},{8,12},{10,14},{12... | collective-permute-start | bytes 393224 | tf_op jit(solution)/shard_map/ppermute | solution.py:321
  118.5 1.7 %shard_map.117 = (bf16[128,512]{1,0:T(8,128)(2,1)S(1)}, bf16[128,512]{1,0:T(8,128)(2,1)S(1)}, bf16[128,512]{1,0:T(8,128)(2,1)S(1)}, bf16[128,512]{1,0:T(8,128)(2,1)S(1)}) custom-call(bf16[512,2048]{1,0:T(8,128)(2,1)S(1)} %get-tuple-element.38.hid_ref, bf16[4,1024,128]{2,1,0:T(8,128)(2,1)S(1)} %collective-permute-done.24.refs_0_, ...), custom_call_target="tpu_custom_call" | custom-call | flops 1073741824 | bytes 3000000 | tf_op jit(solution)/shard_map/pallas_call | solution.py:309
  120.2 2.0 %collective-permute-start.27 = (bf16[128,512]{1,0:T(8,128)(2,1)S(1)}, bf16[128,512]{1,0:T(8,128)(2,1)S(1)}, u32[]{:S(2)}, u32[]{:S(2)}) collective-permute-start(bf16[128,512]{1,0:T(8,128)(2,1)S(1)} %get-tuple-element.40), channel_id=1, source_target_pairs={{0,6},{2,0},{4,2},{6,4},{1,7},{3,1},{5,3},{7,5},{8,14},{10,8},{12,... | collective-permute-start | bytes 393224 | tf_op jit(solution)/shard_map/ppermute | solution.py:321
  122.2 3.9 %shard_map.118 = (bf16[128,1024]{1,0:T(8,128)(2,1)S(1)}, bf16[128,1024]{1,0:T(8,128)(2,1)S(1)}, bf16[128,1024]{1,0:T(8,128)(2,1)S(1)}, bf16[128,1024]{1,0:T(8,128)(2,1)S(1)}) custom-call(bf16[512,2048]{1,0:T(8,128)(2,1)S(1)} %get-tuple-element.38.hid_ref, bf16[4,1024,128]{2,1,0:T(8,128)(2,1)S(1)} %collective-permute-done.25.refs_0_, ...), custom_call_target="tpu_custom_call" | custom-call | flops 2147483648 | bytes 6000000 | tf_op jit(solution)/shard_map/pallas_call | solution.py:309
  126.1 0.9 collective-permute-start.33
  127.0 1.2 collective-permute-start.34
  128.2 2.9 %collective-permute-start.35 = (bf16[128,1024]{1,0:T(8,128)(2,1)S(1)}, bf16[128,1024]{1,0:T(8,128)(2,1)S(1)}, u32[]{:S(2)}, u32[]{:S(2)}) collective-permute-start(bf16[128,1024]{1,0:T(8,128)(2,1)S(1)} %get-tuple-element.46), channel_id=1, source_target_pairs={{0,4},{2,6},{4,0},{6,2},{1,5},{3,7},{5,1},{7,3},{8,12},{10,14},{12... | collective-permute-start | bytes 786440 | tf_op jit(solution)/shard_map/ppermute | solution.py:321
  131.1 2.2 %collective-permute-start.29 = (bf16[128,512]{1,0:T(8,128)(2,1)S(1)}, bf16[128,512]{1,0:T(8,128)(2,1)S(1)}, u32[]{:S(2)}, u32[]{:S(2)}) collective-permute-start(bf16[128,512]{1,0:T(8,128)(2,1)S(1)} %get-tuple-element.42), channel_id=1, source_target_pairs={{0,4},{2,6},{4,0},{6,2},{1,5},{3,7},{5,1},{7,3},{8,12},{10,14},{12... | collective-permute-start | bytes 393224 | tf_op jit(solution)/shard_map/ppermute | solution.py:321
  133.3 12.1 %collective-permute-done.28.refs_6_ = bf16[128,512]{1,0:T(8,128)(2,1)S(1)} collective-permute-done((bf16[128,512]{1,0:T(8,128)(2,1)S(1)}, bf16[128,512]{1,0:T(8,128)(2,1)S(1)}, u32[]{:S(2)}, u32[]{:S(2)}) %collective-permute-start.28) | collective-permute-done | bytes 131104 | tf_op jit(solution)/shard_map/ppermute | solution.py:321
  145.4 2.0 %collective-permute-done.29.refs_7_ = bf16[128,512]{1,0:T(8,128)(2,1)S(1)} collective-permute-done((bf16[128,512]{1,0:T(8,128)(2,1)S(1)}, bf16[128,512]{1,0:T(8,128)(2,1)S(1)}, u32[]{:S(2)}, u32[]{:S(2)}) %collective-permute-start.29) | collective-permute-done | bytes 131104 | tf_op jit(solution)/shard_map/ppermute | solution.py:321
  147.4 1.3 shard_map.119
  (60 shorter events, 1.7 us)
Async XLA Ops:
  0.0 14.1 %copy-start.8 = (bf16[1024,128]{1,0:T(8,128)(2,1)S(1)}, bf16[1024,128]{1,0:T(8,128)(2,1)}, u32[]{:S(2)}) copy-start(bf16[1024,128]{1,0:T(8,128)(2,1)} %refs_0_.3) | copy-start | bytes 786436
  0.0 14.3 %copy-start.2 = (bf16[128,2048]{1,0:T(8,128)(2,1)S(1)}, bf16[128,2048]{1,0:T(8,128)(2,1)}, u32[]{:S(2)}) copy-start(bf16[128,2048]{1,0:T(8,128)(2,1)} %s0.1) | copy-start | bytes 1572868
  0.0 17.7 %collective-permute-start.7 = (bf16[128,1024]{1,0:T(8,128)(2,1)}, bf16[128,1024]{1,0:T(8,128)(2,1)S(1)}, u32[]{:S(2)}, u32[]{:S(2)}) collective-permute-start(bf16[128,1024]{1,0:T(8,128)(2,1)} %refs_0_.2), channel_id=1, source_target_pairs={{0,8},{1,25},{8,16},{9,1},{16,24},{17,9},{24,0},{25,17},{2,10},{3,... | collective-permute-start | bytes 786440 | tf_op jit(solution)/shard_map/ppermute | solution.py:330
  1.6 17.6 %collective-permute-start.8 = (bf16[128,1024]{1,0:T(8,128)(2,1)}, bf16[128,1024]{1,0:T(8,128)(2,1)S(1)}, u32[]{:S(2)}, u32[]{:S(2)}) collective-permute-start(bf16[128,1024]{1,0:T(8,128)(2,1)} %refs_0_.2), channel_id=1, source_target_pairs={{0,24},{1,9},{8,0},{9,17},{16,8},{17,25},{24,16},{25,1},{2,26},{3,... | collective-permute-start | bytes 786440 | tf_op jit(solution)/shard_map/ppermute | solution.py:330
  3.2 30.9 %copy-start.5 = (bf16[128,1024]{1,0:T(8,128)(2,1)S(1)}, bf16[128,1024]{1,0:T(8,128)(2,1)}, u32[]{:S(2)}) copy-start(bf16[128,1024]{1,0:T(8,128)(2,1)} %refs_0_.2) | copy-start | bytes 786436
  8.2 20.1 %all-to-all-start = ((bf16[16,72,128]{2,1,0:T(8,128)(2,1)}), bf16[16,72,128]{2,1,0:T(8,128)(2,1)S(1)}, u32[]{:S(2)}, u32[]{:S(2)}) async-start(bf16[16,72,128]{2,1,0:T(8,128)(2,1)} %get-tuple-element.26), calls=%async_computation | async-start | bytes 589824 | tf_op jit(solution)/shard_map/all_to_all | solution.py:381
  14.1 11.1 %collective-permute-start.17 = (bf16[1024,128]{1,0:T(8,128)(2,1)S(1)}, bf16[1024,128]{1,0:T(8,128)(2,1)}, u32[]{:S(2)}, u32[]{:S(2)}) collective-permute-start(bf16[1024,128]{1,0:T(8,128)(2,1)S(1)} %copy-done.8), channel_id=1, source_target_pairs={{0,32},{1,97},{32,64},{33,1},{64,96},{65,33},{96,0},{97,65},{2,34}... | collective-permute-start | bytes 786440 | tf_op jit(solution)/shard_map/ppermute | solution.py:330
  14.3 21.3 %collective-permute-start.4 = (bf16[128,2048]{1,0:T(8,128)(2,1)S(1)}, bf16[128,2048]{1,0:T(8,128)(2,1)S(1)}, u32[]{:S(2)}, u32[]{:S(2)}) collective-permute-start(bf16[128,2048]{1,0:T(8,128)(2,1)S(1)} %copy-done.2), channel_id=1, source_target_pairs={{0,2},{2,4},{4,6},{6,0},{1,3},{3,5},{5,7},{7,1},{8,10},{10,12},{12... | collective-permute-start | bytes 1572872 | tf_op jit(solution)/shard_map/ppermute | solution.py:321
  15.8 16.6 %collective-permute-start.18 = (bf16[1024,128]{1,0:T(8,128)(2,1)S(1)}, bf16[1024,128]{1,0:T(8,128)(2,1)S(1)}, u32[]{:S(2)}, u32[]{:S(2)}) collective-permute-start(bf16[1024,128]{1,0:T(8,128)(2,1)S(1)} %copy-done.8), channel_id=1, source_target_pairs={{0,96},{1,33},{32,0},{33,65},{64,32},{65,97},{96,64},{97,1},{2,98}... | collective-permute-start | bytes 786440 | tf_op jit(solution)/shard_map/ppermute | solution.py:330
  17.7 14.8 %collective-permute-start.9 = (bf16[128,1024]{1,0:T(8,128)(2,1)S(1)}, bf16[128,1024]{1,0:T(8,128)(2,1)S(1)}, u32[]{:S(2)}, u32[]{:S(2)}) collective-permute-start(bf16[128,1024]{1,0:T(8,128)(2,1)S(1)} %collective-permute-done.7.refs_1_), channel_id=1, source_target_pairs={{0,8},{1,25},{8,16},{9,1},{16,24},{17,9},{24,0},{25,17},{2,10},{3,... | collective-permute-start | bytes 786440 | tf_op jit(solution)/shard_map/ppermute | solution.py:330
  19.2 18.9 %collective-permute-start.5 = (bf16[128,2048]{1,0:T(8,128)(2,1)S(1)}, bf16[128,2048]{1,0:T(8,128)(2,1)}, u32[]{:S(2)}, u32[]{:S(2)}) collective-permute-start(bf16[128,2048]{1,0:T(8,128)(2,1)S(1)} %copy-done.2), channel_id=1, source_target_pairs={{0,6},{2,0},{4,2},{6,4},{1,7},{3,1},{5,3},{7,5},{8,14},{10,8},{12,... | collective-permute-start | bytes 1572872 | tf_op jit(solution)/shard_map/ppermute | solution.py:321
  25.2 22.2 %collective-permute-start.6 = (bf16[128,2048]{1,0:T(8,128)(2,1)S(1)}, bf16[128,2048]{1,0:T(8,128)(2,1)}, u32[]{:S(2)}, u32[]{:S(2)}) collective-permute-start(bf16[128,2048]{1,0:T(8,128)(2,1)S(1)} %copy-done.2), channel_id=1, source_target_pairs={{0,4},{2,6},{4,0},{6,2},{1,5},{3,7},{5,1},{7,3},{8,12},{10,14},{12... | collective-permute-start | bytes 1572872 | tf_op jit(solution)/shard_map/ppermute | solution.py:321
  28.3 0.7 copy-start.7
  32.4 3.2 %copy-start.9 = (bf16[1024,128]{1,0:T(8,128)(2,1)}, bf16[1024,128]{1,0:T(8,128)(2,1)S(1)}, u32[]{:S(2)}) copy-start(bf16[1024,128]{1,0:T(8,128)(2,1)S(1)} %collective-permute-done.18.refs_2_) | copy-start | bytes 786436
  32.4 1.9 %collective-permute-start = (bf16[4,128,128]{2,1,0:T(8,128)(2,1)}, bf16[4,128,128]{2,1,0:T(8,128)(2,1)S(1)}, u32[]{:S(2)}, u32[]{:S(2)}) collective-permute-start(bf16[4,128,128]{2,1,0:T(8,128)(2,1)} %get-tuple-element.30), channel_id=1, source_target_pairs={{0,1},{1,0},{2,3},{3,2},{4,5},{5,4},{6,7},{7,6},{8,9},{9,8},{10,11... | collective-permute-start | bytes 393224 | tf_op jit(solution)/shard_map/ppermute | solution.py:325
  32.5 7.6 %collective-permute-start.19 = (bf16[1024,128]{1,0:T(8,128)(2,1)}, bf16[1024,128]{1,0:T(8,128)(2,1)S(1)}, u32[]{:S(2)}, u32[]{:S(2)}) collective-permute-start(bf16[1024,128]{1,0:T(8,128)(2,1)} %collective-permute-done.17.refs_1_), channel_id=1, source_target_pairs={{0,32},{1,97},{32,64},{33,1},{64,96},{65,33},{96,0},{97,65},{2,34}... | collective-permute-start | bytes 786440 | tf_op jit(solution)/shard_map/ppermute | solution.py:330
  34.3 36.8 %collective-permute-start.11 = (bf16[4,128,1024]{2,1,0:T(8,128)(2,1)S(1)}, bf16[4,128,1024]{2,1,0:T(8,128)(2,1)S(1)}, u32[]{:S(2)}, u32[]{:S(2)}) collective-permute-start(bf16[4,128,1024]{2,1,0:T(8,128)(2,1)S(1)} %shard_map.113.refs_0_), channel_id=1, source_target_pairs={{0,32},{1,97},{32,64},{33,1},{64,96},{65,33},{96,0},{97,65},{2,34}... | collective-permute-start | bytes 3145736 | tf_op jit(solution)/shard_map/ppermute | solution.py:330
  35.6 0.8 copy-start.3
  36.4 34.7 %collective-permute-start.12 = (bf16[4,128,1024]{2,1,0:T(8,128)(2,1)S(1)}, bf16[4,128,1024]{2,1,0:T(8,128)(2,1)S(1)}, u32[]{:S(2)}, u32[]{:S(2)}) collective-permute-start(bf16[4,128,1024]{2,1,0:T(8,128)(2,1)S(1)} %shard_map.113.refs_0_), channel_id=1, source_target_pairs={{0,96},{1,33},{32,0},{33,65},{64,32},{65,97},{96,64},{97,1},{2,98}... | collective-permute-start | bytes 3145736 | tf_op jit(solution)/shard_map/ppermute | solution.py:330
  38.1 16.8 %collective-permute-start.1 = (bf16[2,4,128,128]{3,2,1,0:T(8,128)(2,1)S(1)}, bf16[2,4,128,128]{3,2,1,0:T(8,128)(2,1)}, u32[]{:S(2)}, u32[]{:S(2)}) collective-permute-start(bf16[2,4,128,128]{3,2,1,0:T(8,128)(2,1)S(1)} %pad_maximum_fusion.g0), channel_id=1, source_target_pairs={{0,2},{2,4},{4,6},{6,0},{1,3},{3,5},{5,7},{7,1},{8,10},{10,12},{12... | collective-permute-start | bytes 786440 | tf_op jit(solution)/shard_map/ppermute | solution.py:321
  40.1 0.7 copy-start.10
  40.8 30.4 %collective-permute-start.10 = (bf16[4,128,1024]{2,1,0:T(8,128)(2,1)S(1)}, bf16[4,128,1024]{2,1,0:T(8,128)(2,1)}, u32[]{:S(2)}, u32[]{:S(2)}) collective-permute-start(bf16[4,128,1024]{2,1,0:T(8,128)(2,1)S(1)} %shard_map.113.refs_0_), channel_id=1, source_target_pairs={{0,1},{1,0},{2,3},{3,2},{4,5},{5,4},{6,7},{7,6},{8,9},{9,8},{10,11... | collective-permute-start | bytes 3145736 | tf_op jit(solution)/shard_map/ppermute | solution.py:325
  45.4 55.5 %copy-start.6 = (f32[2048]{0:T(1024)S(1)}, f32[2048]{0:T(1024)}, u32[]{:S(2)}) copy-start(f32[2048]{0:T(1024)} %param.19) | copy-start | bytes 24580
  47.4 24.3 %collective-permute-start.24 = (bf16[4,1024,128]{2,1,0:T(8,128)(2,1)}, bf16[4,1024,128]{2,1,0:T(8,128)(2,1)S(1)}, u32[]{:S(2)}, u32[]{:S(2)}) collective-permute-start(bf16[4,1024,128]{2,1,0:T(8,128)(2,1)} %shard_map.115.d0), channel_id=1, source_target_pairs={{0,8},{1,25},{8,16},{9,1},{16,24},{17,9},{24,0},{25,17},{2,10},{3,... | collective-permute-start | bytes 3145736 | tf_op jit(solution)/shard_map/ppermute | solution.py:330
  54.9 7.8 %collective-permute-start.2 = (bf16[2,4,128,128]{3,2,1,0:T(8,128)(2,1)S(1)}, bf16[2,4,128,128]{3,2,1,0:T(8,128)(2,1)S(1)}, u32[]{:S(2)}, u32[]{:S(2)}) collective-permute-start(bf16[2,4,128,128]{3,2,1,0:T(8,128)(2,1)S(1)} %pad_maximum_fusion.g0), channel_id=1, source_target_pairs={{0,6},{2,0},{4,2},{6,4},{1,7},{3,1},{5,3},{7,5},{8,14},{10,8},{12,... | collective-permute-start | bytes 786440 | tf_op jit(solution)/shard_map/ppermute | solution.py:321
  62.6 8.4 %collective-permute-start.3 = (bf16[2,4,128,128]{3,2,1,0:T(8,128)(2,1)S(1)}, bf16[2,4,128,128]{3,2,1,0:T(8,128)(2,1)S(1)}, u32[]{:S(2)}, u32[]{:S(2)}) collective-permute-start(bf16[2,4,128,128]{3,2,1,0:T(8,128)(2,1)S(1)} %pad_maximum_fusion.g0), channel_id=1, source_target_pairs={{0,4},{2,6},{4,0},{6,2},{1,5},{3,7},{5,1},{7,3},{8,12},{10,14},{12... | collective-permute-start | bytes 786440 | tf_op jit(solution)/shard_map/ppermute | solution.py:321
  71.0 26.1 %collective-permute-start.25 = (bf16[4,1024,128]{2,1,0:T(8,128)(2,1)}, bf16[4,1024,128]{2,1,0:T(8,128)(2,1)S(1)}, u32[]{:S(2)}, u32[]{:S(2)}) collective-permute-start(bf16[4,1024,128]{2,1,0:T(8,128)(2,1)} %shard_map.115.d0), channel_id=1, source_target_pairs={{0,24},{1,9},{8,0},{9,17},{16,8},{17,25},{24,16},{25,1},{2,26},{3,... | collective-permute-start | bytes 3145736 | tf_op jit(solution)/shard_map/ppermute | solution.py:330
  71.1 26.1 %collective-permute-start.15 = (bf16[4,128,1024]{2,1,0:T(8,128)(2,1)S(1)}, bf16[4,128,1024]{2,1,0:T(8,128)(2,1)S(1)}, u32[]{:S(2)}, u32[]{:S(2)}) collective-permute-start(bf16[4,128,1024]{2,1,0:T(8,128)(2,1)S(1)} %collective-permute-done.11.refs_2_), channel_id=1, source_target_pairs={{0,32},{1,97},{32,64},{33,1},{64,96},{65,33},{96,0},{97,65},{2,34}... | collective-permute-start | bytes 3145736 | tf_op jit(solution)/shard_map/ppermute | solution.py:330
  71.1 26.5 %collective-permute-start.13 = (bf16[4,128,1024]{2,1,0:T(8,128)(2,1)S(1)}, bf16[4,128,1024]{2,1,0:T(8,128)(2,1)S(1)}, u32[]{:S(2)}, u32[]{:S(2)}) collective-permute-start(bf16[4,128,1024]{2,1,0:T(8,128)(2,1)S(1)} %collective-permute-done.12.refs_4_), channel_id=1, source_target_pairs={{0,1},{1,0},{2,3},{3,2},{4,5},{5,4},{6,7},{7,6},{8,9},{9,8},{10,11... | collective-permute-start | bytes 3145736 | tf_op jit(solution)/shard_map/ppermute | solution.py:325
  71.2 26.5 %collective-permute-start.14 = (bf16[4,128,1024]{2,1,0:T(8,128)(2,1)S(1)}, bf16[4,128,1024]{2,1,0:T(8,128)(2,1)S(1)}, u32[]{:S(2)}, u32[]{:S(2)}) collective-permute-start(bf16[4,128,1024]{2,1,0:T(8,128)(2,1)S(1)} %collective-permute-done.11.refs_2_), channel_id=1, source_target_pairs={{0,1},{1,0},{2,3},{3,2},{4,5},{5,4},{6,7},{7,6},{8,9},{9,8},{10,11... | collective-permute-start | bytes 3145736 | tf_op jit(solution)/shard_map/ppermute | solution.py:325
  71.7 26.5 %collective-permute-start.31 = (bf16[4,1024,128]{2,1,0:T(8,128)(2,1)S(1)}, bf16[4,1024,128]{2,1,0:T(8,128)(2,1)S(1)}, u32[]{:S(2)}, u32[]{:S(2)}) collective-permute-start(bf16[4,1024,128]{2,1,0:T(8,128)(2,1)S(1)} %collective-permute-done.24.refs_0_), channel_id=1, source_target_pairs={{0,8},{1,25},{8,16},{9,1},{16,24},{17,9},{24,0},{25,17},{2,10},{3,... | collective-permute-start | bytes 3145736 | tf_op jit(solution)/shard_map/ppermute | solution.py:330
  97.1 14.2 %collective-permute-start.20 = (bf16[4,1024,128]{2,1,0:T(8,128)(2,1)}, bf16[4,1024,128]{2,1,0:T(8,128)(2,1)S(1)}, u32[]{:S(2)}, u32[]{:S(2)}) collective-permute-start(bf16[4,1024,128]{2,1,0:T(8,128)(2,1)} %shard_map.115.d0), channel_id=1, source_target_pairs={{0,1},{1,0},{2,3},{3,2},{4,5},{5,4},{6,7},{7,6},{8,9},{9,8},{10,11... | collective-permute-start | bytes 3145736 | tf_op jit(solution)/shard_map/ppermute | solution.py:325
  97.1 14.2 %collective-permute-start.16 = (bf16[4,128,1024]{2,1,0:T(8,128)(2,1)S(1)}, bf16[4,128,1024]{2,1,0:T(8,128)(2,1)S(1)}, u32[]{:S(2)}, u32[]{:S(2)}) collective-permute-start(bf16[4,128,1024]{2,1,0:T(8,128)(2,1)S(1)} %collective-permute-done.15.u0), channel_id=1, source_target_pairs={{0,1},{1,0},{2,3},{3,2},{4,5},{5,4},{6,7},{7,6},{8,9},{9,8},{10,11... | collective-permute-start | bytes 3145736 | tf_op jit(solution)/shard_map/ppermute | solution.py:325
  97.6 19.3 %collective-permute-start.26 = (bf16[4,1024,128]{2,1,0:T(8,128)(2,1)S(1)}, bf16[4,1024,128]{2,1,0:T(8,128)(2,1)S(1)}, u32[]{:S(2)}, u32[]{:S(2)}) collective-permute-start(bf16[4,1024,128]{2,1,0:T(8,128)(2,1)S(1)} %collective-permute-done.25.refs_0_), channel_id=1, source_target_pairs={{0,1},{1,0},{2,3},{3,2},{4,5},{5,4},{6,7},{7,6},{8,9},{9,8},{10,11... | collective-permute-start | bytes 3145736 | tf_op jit(solution)/shard_map/ppermute | solution.py:325
  97.7 22.5 %collective-permute-start.30 = (bf16[4,1024,128]{2,1,0:T(8,128)(2,1)S(1)}, bf16[4,1024,128]{2,1,0:T(8,128)(2,1)S(1)}, u32[]{:S(2)}, u32[]{:S(2)}) collective-permute-start(bf16[4,1024,128]{2,1,0:T(8,128)(2,1)S(1)} %collective-permute-done.24.refs_0_), channel_id=1, source_target_pairs={{0,1},{1,0},{2,3},{3,2},{4,5},{5,4},{6,7},{7,6},{8,9},{9,8},{10,11... | collective-permute-start | bytes 3145736 | tf_op jit(solution)/shard_map/ppermute | solution.py:325
  98.1 24.1 %collective-permute-start.32 = (bf16[4,1024,128]{2,1,0:T(8,128)(2,1)S(1)}, bf16[4,1024,128]{2,1,0:T(8,128)(2,1)S(1)}, u32[]{:S(2)}, u32[]{:S(2)}) collective-permute-start(bf16[4,1024,128]{2,1,0:T(8,128)(2,1)S(1)} %collective-permute-done.31.refs_2_), channel_id=1, source_target_pairs={{0,1},{1,0},{2,3},{3,2},{4,5},{5,4},{6,7},{7,6},{8,9},{9,8},{10,11... | collective-permute-start | bytes 3145736 | tf_op jit(solution)/shard_map/ppermute | solution.py:325
  98.4 2.2 %copy-start = (bf16[1024,2048]{1,0:T(8,128)(2,1)S(1)}, bf16[1024,2048]{1,0:T(8,128)(2,1)}, u32[]{:S(2)}) copy-start(bf16[1024,2048]{1,0:T(8,128)(2,1)} %w_ref.1) | copy-start | bytes 12582916
  100.6 1.0 copy-start.4
  106.3 5.0 %copy-start.1 = (bf16[4,1024,128]{2,1,0:T(8,128)(2,1)S(1)}, bf16[4,1024,128]{2,1,0:T(8,128)(2,1)}, u32[]{:S(2)}) copy-start(bf16[4,1024,128]{2,1,0:T(8,128)(2,1)} %shard_map.115.d0) | copy-start | bytes 3145732
  114.5 12.5 %collective-permute-start.21 = (bf16[128,512]{1,0:T(8,128)(2,1)S(1)}, bf16[128,512]{1,0:T(8,128)(2,1)S(1)}, u32[]{:S(2)}, u32[]{:S(2)}) collective-permute-start(bf16[128,512]{1,0:T(8,128)(2,1)S(1)} %get-tuple-element.35), channel_id=1, source_target_pairs={{0,6},{2,0},{4,2},{6,4},{1,7},{3,1},{5,3},{7,5},{8,14},{10,8},{12,... | collective-permute-start | bytes 393224 | tf_op jit(solution)/shard_map/ppermute | solution.py:321
  117.0 11.2 %collective-permute-start.22 = (bf16[128,512]{1,0:T(8,128)(2,1)S(1)}, bf16[128,512]{1,0:T(8,128)(2,1)S(1)}, u32[]{:S(2)}, u32[]{:S(2)}) collective-permute-start(bf16[128,512]{1,0:T(8,128)(2,1)S(1)} %get-tuple-element.36), channel_id=1, source_target_pairs={{0,2},{2,4},{4,6},{6,0},{1,3},{3,5},{5,7},{7,1},{8,10},{10,12},{12... | collective-permute-start | bytes 393224 | tf_op jit(solution)/shard_map/ppermute | solution.py:321
  117.0 14.2 %collective-permute-start.23 = (bf16[128,512]{1,0:T(8,128)(2,1)S(1)}, bf16[128,512]{1,0:T(8,128)(2,1)S(1)}, u32[]{:S(2)}, u32[]{:S(2)}) collective-permute-start(bf16[128,512]{1,0:T(8,128)(2,1)S(1)} %get-tuple-element.37), channel_id=1, source_target_pairs={{0,4},{2,6},{4,0},{6,2},{1,5},{3,7},{5,1},{7,3},{8,12},{10,14},{12... | collective-permute-start | bytes 393224 | tf_op jit(solution)/shard_map/ppermute | solution.py:321
  120.2 10.9 %collective-permute-start.27 = (bf16[128,512]{1,0:T(8,128)(2,1)S(1)}, bf16[128,512]{1,0:T(8,128)(2,1)S(1)}, u32[]{:S(2)}, u32[]{:S(2)}) collective-permute-start(bf16[128,512]{1,0:T(8,128)(2,1)S(1)} %get-tuple-element.40), channel_id=1, source_target_pairs={{0,6},{2,0},{4,2},{6,4},{1,7},{3,1},{5,3},{7,5},{8,14},{10,8},{12,... | collective-permute-start | bytes 393224 | tf_op jit(solution)/shard_map/ppermute | solution.py:321
  126.1 21.3 %collective-permute-start.33 = (bf16[128,1024]{1,0:T(8,128)(2,1)S(1)}, bf16[128,1024]{1,0:T(8,128)(2,1)S(1)}, u32[]{:S(2)}, u32[]{:S(2)}) collective-permute-start(bf16[128,1024]{1,0:T(8,128)(2,1)S(1)} %get-tuple-element.44), channel_id=1, source_target_pairs={{0,6},{2,0},{4,2},{6,4},{1,7},{3,1},{5,3},{7,5},{8,14},{10,8},{12,... | collective-permute-start | bytes 786440 | tf_op jit(solution)/shard_map/ppermute | solution.py:321
  127.0 20.4 %collective-permute-start.34 = (bf16[128,1024]{1,0:T(8,128)(2,1)S(1)}, bf16[128,1024]{1,0:T(8,128)(2,1)S(1)}, u32[]{:S(2)}, u32[]{:S(2)}) collective-permute-start(bf16[128,1024]{1,0:T(8,128)(2,1)S(1)} %get-tuple-element.45), channel_id=1, source_target_pairs={{0,2},{2,4},{4,6},{6,0},{1,3},{3,5},{5,7},{7,1},{8,10},{10,12},{12... | collective-permute-start | bytes 786440 | tf_op jit(solution)/shard_map/ppermute | solution.py:321
  128.2 19.2 %collective-permute-start.35 = (bf16[128,1024]{1,0:T(8,128)(2,1)S(1)}, bf16[128,1024]{1,0:T(8,128)(2,1)S(1)}, u32[]{:S(2)}, u32[]{:S(2)}) collective-permute-start(bf16[128,1024]{1,0:T(8,128)(2,1)S(1)} %get-tuple-element.46), channel_id=1, source_target_pairs={{0,4},{2,6},{4,0},{6,2},{1,5},{3,7},{5,1},{7,3},{8,12},{10,14},{12... | collective-permute-start | bytes 786440 | tf_op jit(solution)/shard_map/ppermute | solution.py:321
  131.1 14.3 %collective-permute-start.28 = (bf16[128,512]{1,0:T(8,128)(2,1)S(1)}, bf16[128,512]{1,0:T(8,128)(2,1)S(1)}, u32[]{:S(2)}, u32[]{:S(2)}) collective-permute-start(bf16[128,512]{1,0:T(8,128)(2,1)S(1)} %get-tuple-element.41), channel_id=1, source_target_pairs={{0,2},{2,4},{4,6},{6,0},{1,3},{3,5},{5,7},{7,1},{8,10},{10,12},{12... | collective-permute-start | bytes 393224 | tf_op jit(solution)/shard_map/ppermute | solution.py:321
  131.1 16.3 %collective-permute-start.29 = (bf16[128,512]{1,0:T(8,128)(2,1)S(1)}, bf16[128,512]{1,0:T(8,128)(2,1)S(1)}, u32[]{:S(2)}, u32[]{:S(2)}) collective-permute-start(bf16[128,512]{1,0:T(8,128)(2,1)S(1)} %get-tuple-element.42), channel_id=1, source_target_pairs={{0,4},{2,6},{4,0},{6,2},{1,5},{3,7},{5,1},{7,3},{8,12},{10,14},{12... | collective-permute-start | bytes 393224 | tf_op jit(solution)/shard_map/ppermute | solution.py:321
